TPU v7x, 32 devices: a whole 2x2x4 slice. The times are simulated.
32 devices in a mesh: ep: 8 (over z, x), tp: 4 (over y, core).
Axes of the slice: x: 2, y: 2, z: 4, core: 2. Of those that a mesh axis runs over, the one named last changes fastest.
Arguments:
- receptance: bfloat16 [4096, 1024], P('ep', 'tp'), may hold values from -6 to 6
- key_matrix: bfloat16 [4096, 1024], P('ep', 'tp'), may hold values from -6 to 6
- value_matrix: bfloat16 [4096, 1024], P('ep', 'tp'), may hold values from -6 to 6
- decay_data_term: bfloat16 [4096, 1024], P('ep', 'tp'), may hold values from -3.5 to 3.5
- correction_rate_data: bfloat16 [4096, 1024], P('ep', 'tp'), may hold values from -6 to 6
- output_gate_input: bfloat16 [4096, 1024], P('ep', 'tp'), may hold values from -6 to 6
- decay_channel_offset: float32 [1024], P('tp'), may hold values from -12 to -2
- correction_rate_offset: float32 [1024], P('tp'), may hold values from -12 to 1
- extra_head_log_decay: float32 [4096, 16], P('ep', 'tp'), may hold values from -2.1 to 0, as said below
- head_norm_gain: float32 [1024], P('tp'), may hold values from 0.1 to 1.9
- mixer_output_weight: bfloat16 [1024, 2048], P('tp'), may hold values from -0.1875 to 0.1875
- expert_layer_input: bfloat16 [1024, 2048], P('ep'), may hold values from -6 to 6
- feedforward_norm_gain: float32 [2048], replicated, may hold values from 0.1 to 1.9
- group_router_weight: bfloat16 [2048, 4], replicated, may hold values from -0.125 to 0.125
- expert_router_weight: bfloat16 [2048, 8], replicated, may hold values from -0.125 to 0.125
- routes: int32 [1024, 2], P('ep'), may hold values from 0 to 7, all different within a row; in each aligned block of 128 rows (0 to 127, 128 to 255, ...) at most 64 rows name the same one
- expert_gate_weight: bfloat16 [8, 2048, 4096], P('ep', None, 'tp'), may hold values from -0.125 to 0.125
- expert_up_weight: bfloat16 [8, 2048, 4096], P('ep', None, 'tp'), may hold values from -0.125 to 0.125
- expert_down_weight: bfloat16 [8, 4096, 2048], P('ep', 'tp'), may hold values from -0.09375 to 0.09375
Outputs:
- token_mixer_output: bfloat16 [4096, 2048], P(('ep', 'tp'))
- expert_out: bfloat16 [1024, 2048], P('ep', 'tp')
Inputs may be any that keep to these rules, and one draw needn't show every extreme that they name: A token's routes are distinct. Within the rows of one index of ep, no expert is named by more than 64 rows, a bound that some block reaches. `extra_head_log_decay`: entries are zero or negative; each head has a few nonzero positions.
All inputs are finite; a program needn't handle non-finite values.
Results may differ from a plain program's by a relative error of at most 0.022.
Values may be sent and summed in bfloat16 or wider, within the bound.
No kernel may reach another device: no remote copies, remote signals or barrier semaphores. Data moves between devices by JAX's collectives and lax.ppermute only.
A program may use at most 128 MiB of HBM per device.

v0:
```python
import jax
import jax.numpy as jnp
from jax import lax
from jax.sharding import PartitionSpec as P

HEAD_DIM = 64
GROUPS = 4


key_eps = 1e-06
group_eps = 0.00064
norm_eps = 1e-06
highest = lax.Precision.HIGHEST


def carried_in(value, axis, combine, identity):
    devices, place = (lax.axis_size(axis), lax.axis_index(axis))
    everything = jax.tree.map(
        lambda part, kind: lax.all_gather(part.astype(kind), axis),
        value,
        (jnp.bfloat16, jnp.bfloat16),
    )
    start = jax.tree.map(
        lambda part, zero: jnp.broadcast_to(jnp.asarray(zero, part.dtype), part.shape),
        value,
        identity,
    )

    def hop(k, before):
        reached = k < place
        new = combine(
            before, jax.tree.map(lambda part, own: part[k].astype(own.dtype), everything, value)
        )
        return jax.tree.map(lambda a, b: jnp.where(reached, a, b), new, before)

    return lax.fori_loop(0, devices, hop, start)


def chain_join(earlier, later):
    joined_map = jnp.einsum("hvk,hkj->hvj", earlier[0], later[0], precision=highest)
    joined_state = jnp.einsum("hvk,hkj->hvj", earlier[1], later[0], precision=highest) + later[1]
    return (joined_map, joined_state)


def pair_decay(upper, lower, keep):
    gap = upper[:, None] - lower[None, :]
    mask = keep[:, :, None, None]
    return jnp.where(mask, jnp.exp(jnp.where(mask, gap, 0.0)), 0.0)


def block_advance(stacked, inputs):
    recept_b, log_b, unit_b, removal_b, key_b, value_b = inputs
    block_len = recept_b.shape[0]
    cumul = jnp.cumsum(log_b, axis=0)
    before = cumul - log_b
    places = jnp.arange(block_len)
    strict = places[:, None] > places[None, :]
    upto = places[:, None] >= places[None, :]
    strict_decay = pair_decay(before, cumul, strict)
    upto_decay = pair_decay(cumul, cumul, upto)
    key_pairs = jnp.einsum("jhk,ihk,jihk->hji", unit_b, key_b, strict_decay, precision=highest)
    removal_pairs = jnp.einsum(
        "jhk,ihk,jihk->hji", unit_b, removal_b, strict_decay, precision=highest
    )
    read_keys = jnp.einsum("thk,ihk,tihk->hti", recept_b, key_b, upto_decay, precision=highest)
    read_removal = jnp.einsum(
        "thk,ihk,tihk->hti", recept_b, removal_b, upto_decay, precision=highest
    )
    value_padded = jnp.concatenate([value_b, jnp.zeros_like(value_b)], axis=-1)
    right_side = jnp.einsum(
        "jhk,hrk->hjr", unit_b * jnp.exp(before), stacked, precision=highest
    ) + jnp.einsum("hji,ihr->hjr", key_pairs, value_padded, precision=highest)
    left_side = jnp.eye(block_len, dtype=jnp.float32)[None] + removal_pairs
    corrected = jax.scipy.linalg.solve_triangular(
        left_side, right_side, lower=True, unit_diagonal=True
    )
    outputs = (
        jnp.einsum("thk,hrk->thr", recept_b * jnp.exp(cumul), stacked, precision=highest)
        + jnp.einsum("hti,ihr->thr", read_keys, value_padded, precision=highest)
        - jnp.einsum("hti,hir->thr", read_removal, corrected, precision=highest)
    )
    tail = jnp.exp(cumul[-1][None] - cumul)
    stacked = (
        stacked * jnp.exp(cumul[-1])[:, None, :]
        + jnp.einsum("ihr,ihk->hrk", value_padded, key_b * tail, precision=highest)
        - jnp.einsum("hir,ihk->hrk", corrected, removal_b * tail, precision=highest)
    )
    return (stacked, outputs)


def mixer_part(
    receptance,
    key_matrix,
    value_matrix,
    decay_data_term,
    correction_rate_data,
    output_gate_input,
    decay_channel_offset,
    correction_rate_offset,
    extra_head_log_decay,
    head_norm_gain,
    mixer_output_weight,
):
    positions = receptance.shape[0]
    head_count = receptance.shape[1] // HEAD_DIM

    def head_view(tensor_in):
        return tensor_in.astype(jnp.float32).reshape(positions, head_count, HEAD_DIM)

    recept = head_view(receptance)
    keyed = head_view(key_matrix)
    valued = head_view(value_matrix)
    unit_keys = keyed * lax.rsqrt(jnp.sum(keyed * keyed, axis=-1, keepdims=True) + key_eps)
    learn_rate = jax.nn.sigmoid(
        head_view(correction_rate_data) + correction_rate_offset.reshape(head_count, HEAD_DIM)
    )
    decay_preactivation = head_view(decay_data_term) + decay_channel_offset.reshape(
        head_count, HEAD_DIM
    )
    decay_logarithm = (
        -jnp.exp(-jax.nn.softplus(-decay_preactivation) - 0.5) + extra_head_log_decay[:, :, None]
    )
    removal = unit_keys * learn_rate
    block_len = min(64, positions)
    block_count = positions // block_len

    def blocked(tensor_in):
        return tensor_in.reshape(block_count, block_len, head_count, HEAD_DIM)

    eye_maps = jnp.broadcast_to(
        jnp.eye(HEAD_DIM, dtype=jnp.float32), (head_count, HEAD_DIM, HEAD_DIM)
    )
    zero_state = jnp.zeros((head_count, HEAD_DIM, HEAD_DIM), jnp.float32)
    start = jnp.concatenate([zero_state, eye_maps], axis=1)
    final, outputs = lax.scan(
        block_advance,
        start,
        (
            blocked(recept),
            blocked(decay_logarithm),
            blocked(unit_keys),
            blocked(removal),
            blocked(keyed),
            blocked(valued),
        ),
    )
    outputs = outputs.reshape(positions, head_count, 2 * HEAD_DIM)
    local_read = outputs[:, :, :HEAD_DIM]
    reached = outputs[:, :, HEAD_DIM:]
    state_end = final[:, :HEAD_DIM]
    transfer_end = final[:, HEAD_DIM:]
    prefix = carried_in((transfer_end, state_end), "ep", chain_join, (eye_maps, zero_state))
    head_out = local_read + jnp.einsum("hvk,thk->thv", prefix[1], reached, precision=highest)
    centre = jnp.mean(head_out, axis=-1, keepdims=True)
    spread = jnp.mean(jnp.square(head_out - centre), axis=-1, keepdims=True)
    normed = (head_out - centre) * lax.rsqrt(spread + group_eps)
    gated = (
        normed
        * head_norm_gain.reshape(head_count, HEAD_DIM)
        * jax.nn.sigmoid(head_view(output_gate_input))
    )
    mixed_hidden = gated.reshape(positions, head_count * HEAD_DIM).astype(jnp.bfloat16)
    return lax.psum_scatter(
        jnp.dot(mixed_hidden, mixer_output_weight, preferred_element_type=jnp.float32).astype(
            jnp.bfloat16
        ),
        "tp",
        scatter_dimension=0,
        tiled=True,
    )


def finish_experts(gate_val, up_val, expert_down_weight):
    expert_hidden = (jax.nn.silu(gate_val) * up_val).astype(jnp.bfloat16)
    return lax.psum_scatter(
        jnp.einsum(
            "sxcf,xfd->dsxc", expert_hidden, expert_down_weight, preferred_element_type=jnp.float32
        ).astype(jnp.bfloat16),
        "tp",
        scatter_dimension=0,
        tiled=True,
    )


def expert_part(
    expert_layer_input,
    feedforward_norm_gain,
    group_router_weight,
    expert_router_weight,
    routes,
    expert_gate_weight,
    expert_up_weight,
    expert_down_weight,
):
    token_rows = expert_layer_input.shape[0]
    route_count = routes.shape[1]
    ep_count = lax.axis_size("ep")
    expert_total = expert_router_weight.shape[1]
    per_group = expert_total // GROUPS
    capacity = 4 * token_rows // ep_count
    widened = expert_layer_input.astype(jnp.float32)
    normed_input = (
        widened
        * lax.rsqrt(jnp.mean(widened * widened, axis=-1, keepdims=True) + norm_eps)
        * feedforward_norm_gain
    ).astype(jnp.bfloat16)
    group_logit = jnp.dot(normed_input, group_router_weight, preferred_element_type=jnp.float32)
    group_exp = jnp.exp(group_logit)
    group_prob = group_exp / jnp.sum(group_exp, axis=-1, keepdims=True)
    expert_logit = jnp.dot(normed_input, expert_router_weight, preferred_element_type=jnp.float32)
    expert_range = jnp.arange(expert_total, dtype=jnp.int32)
    matched = routes[:, :, None] == expert_range[None, None, :]
    chosen_logit = jnp.sum(jnp.where(matched, expert_logit[:, None, :], 0.0), axis=-1)
    group_match = (routes // per_group)[:, :, None] == jnp.arange(GROUPS, dtype=jnp.int32)[
        None, None, :
    ]
    chosen_group = jnp.sum(jnp.where(group_match, group_prob[:, None, :], 0.0), axis=-1)
    route_weight = chosen_group * jax.nn.sigmoid(chosen_logit - chosen_logit[:, ::-1])
    flat_match = matched.reshape(token_rows * route_count, expert_total).astype(jnp.int32)
    before = jnp.cumsum(flat_match, axis=0) - flat_match
    placed = jnp.sum(before * flat_match, axis=1)
    slot_ids = routes.reshape(-1) * capacity + placed
    slot_range = jnp.arange(expert_total * capacity, dtype=jnp.int32)
    struck = (slot_range[:, None] == slot_ids[None, :]).reshape(
        expert_total * capacity, token_rows, route_count
    )
    dispatch_matrix = jnp.any(struck, axis=-1).astype(jnp.bfloat16)
    combine_matrix = jnp.sum(jnp.where(struck, route_weight[None, :, :], 0.0), axis=-1)
    outgoing = jnp.dot(dispatch_matrix, normed_input, preferred_element_type=jnp.float32).astype(
        jnp.bfloat16
    )
    outgoing = outgoing.reshape(ep_count, expert_total // ep_count, capacity, outgoing.shape[1])
    width_share = outgoing.shape[3] // lax.axis_size("tp")
    own_columns = lax.dynamic_slice_in_dim(
        outgoing, lax.axis_index("tp") * width_share, width_share, 3
    )
    piece = lax.all_gather(
        lax.all_to_all(own_columns, "ep", split_axis=0, concat_axis=0, tiled=True),
        "tp",
        axis=3,
        tiled=True,
    )
    gate_val = jnp.einsum(
        "sxcd,xdf->sxcf", piece, expert_gate_weight, preferred_element_type=jnp.float32
    )
    up_val = jnp.einsum(
        "sxcd,xdf->sxcf", piece, expert_up_weight, preferred_element_type=jnp.float32
    )
    expert_rows = finish_experts(gate_val, up_val, expert_down_weight)
    homebound = lax.all_to_all(expert_rows, "ep", split_axis=1, concat_axis=1, tiled=True)
    homebound = homebound.reshape(homebound.shape[0], expert_total * capacity)
    combined = jnp.dot(homebound.astype(jnp.float32), combine_matrix, precision=highest)
    return combined.T.astype(jnp.bfloat16)


def local(
    receptance,
    key_matrix,
    value_matrix,
    decay_data_term,
    correction_rate_data,
    output_gate_input,
    decay_channel_offset,
    correction_rate_offset,
    extra_head_log_decay,
    head_norm_gain,
    mixer_output_weight,
    expert_layer_input,
    feedforward_norm_gain,
    group_router_weight,
    expert_router_weight,
    routes,
    expert_gate_weight,
    expert_up_weight,
    expert_down_weight,
):
    token_mixer_output = mixer_part(
        receptance,
        key_matrix,
        value_matrix,
        decay_data_term,
        correction_rate_data,
        output_gate_input,
        decay_channel_offset,
        correction_rate_offset,
        extra_head_log_decay,
        head_norm_gain,
        mixer_output_weight,
    )
    expert_out = expert_part(
        expert_layer_input,
        feedforward_norm_gain,
        group_router_weight,
        expert_router_weight,
        routes,
        expert_gate_weight,
        expert_up_weight,
        expert_down_weight,
    )
    return (token_mixer_output, expert_out)


def solution(mesh):
    in_specs = (
        P("ep", "tp"),
        P("ep", "tp"),
        P("ep", "tp"),
        P("ep", "tp"),
        P("ep", "tp"),
        P("ep", "tp"),
        P("tp"),
        P("tp"),
        P("ep", "tp"),
        P("tp"),
        P("tp", None),
        P("ep", None),
        P(),
        P(),
        P(),
        P("ep", None),
        P("ep", None, "tp"),
        P("ep", None, "tp"),
        P("ep", "tp", None),
    )
    out_specs = (P(("ep", "tp"), None), P("ep", "tp"))
    return jax.shard_map(local, mesh=mesh, in_specs=in_specs, out_specs=out_specs, check_vma=False)
```

profile of v0, /device:TPU:0, one launch (start us, length us, event | category | flops | bytes accessed | tf_op | source)
XLA Modules:
  0.0 763.8 jit_solution(9080496010554632357)
XLA Ops:
  11.6 1.9 convolution_convert_fusion.1
  14.3 7.4 all-to-all-start
  22.2 1.4 copy.152
  24.9 1.4 reshape.221
  27.4 2.4 reshape.222
  29.8 2.4 reshape.241
  32.3 5.1 divide_multiply_fusion
  37.6 566.0 %while.26 = (s32[]{:T(128)}, f32[4,128,64]{1,2,0:T(8,128)S(1)}, f32[8,64,4,128]{3,1,0,2:T(8,128)}, f32[8,64,4,64]{3,2,1,0:T(4,128)}, f32[8,64,4,64]{3,2,1,0:T(4,...) while((s32[]{:T(128)}, f32[4,128,64]{1,2,0:T(8,128)S(1)}, ...), condition=%wide.region_3.4_spmd, body=%wide.region_1.3_spmd.sunk | while | flops 221540416 | bytes 39878260 | solution.py:135
  38.6 1.3 bitcast_multiply_fusion.11
  40.0 12.8 %select_bitcast_fusion.3 = (f32[4,64,64,64]{3,0,2,1:T(4,128)}, f32[4,64,64,64]{3,0,2,1:T(4,128)}) fusion(f32[64,4,64]{2,1,0:T(4,128)S(1)} %fusion.151, pred[64,64]{1,0:T(8,128)(4,1)S(1)} %get-tuple-element.380, f32[64,4,64]{2,1,0:T(4,128)S(1)} %get-tuple-element.381, pred[64,64]{1,0:T(8,128)(4,1)S(1)} %get-tuple-element.382), kind=kLoop, calls=%fused_computation.19.clone.1 | loop fusion | flops 6291456 | bytes 8527872 | tf_op jit(solution)/shard_map/while
  52.8 10.7 %copy.249 = f32[4,64,64,64]{1,2,3,0:T(8,128)} copy(f32[4,64,64,64]{3,0,2,1:T(4,128)} %get-tuple-element.383) | data formatting | bytes 8388608 | tf_op jit(solution)/shard_map/while
  63.5 10.6 %copy.253 = f32[4,64,64,64]{1,2,3,0:T(8,128)} copy(f32[4,64,64,64]{3,0,2,1:T(4,128)} %get-tuple-element.387) | data formatting | bytes 8388608 | tf_op jit(solution)/shard_map/while
  76.6 7.5 fusion.154
  84.3 19.7 %custom-call.7 = f32[4,1,64,64]{2,3,1,0:T(8,128)S(1)} custom-call(f32[4,1,64,64]{3,2,1,0:T(8,128)S(1)} %add_bitcast_fusion.2), custom_call_target="InvertDiagBlocksLowerTriangular" | custom-call | tf_op jit(solution)/shard_map/while/body/eval_jaxpr/jit(_solve_triangular)/vmap()/triangular_solve | solution.py:74
  110.8 12.8 %select_bitcast_fusion.3 = (f32[4,64,64,64]{3,0,2,1:T(4,128)}, f32[4,64,64,64]{3,0,2,1:T(4,128)}) fusion(f32[64,4,64]{2,1,0:T(4,128)S(1)} %fusion.151, pred[64,64]{1,0:T(8,128)(4,1)S(1)} %get-tuple-element.380, f32[64,4,64]{2,1,0:T(4,128)S(1)} %get-tuple-element.381, pred[64,64]{1,0:T(8,128)(4,1)S(1)} %get-tuple-element.382), kind=kLoop, calls=%fused_computation.19.clone.1 | loop fusion | flops 6291456 | bytes 8527872 | tf_op jit(solution)/shard_map/while
  123.6 10.7 %copy.249 = f32[4,64,64,64]{1,2,3,0:T(8,128)} copy(f32[4,64,64,64]{3,0,2,1:T(4,128)} %get-tuple-element.383) | data formatting | bytes 8388608 | tf_op jit(solution)/shard_map/while
  134.2 10.6 %copy.253 = f32[4,64,64,64]{1,2,3,0:T(8,128)} copy(f32[4,64,64,64]{3,0,2,1:T(4,128)} %get-tuple-element.387) | data formatting | bytes 8388608 | tf_op jit(solution)/shard_map/while
  147.3 7.5 fusion.154
  155.0 19.7 %custom-call.7 = f32[4,1,64,64]{2,3,1,0:T(8,128)S(1)} custom-call(f32[4,1,64,64]{3,2,1,0:T(8,128)S(1)} %add_bitcast_fusion.2), custom_call_target="InvertDiagBlocksLowerTriangular" | custom-call | tf_op jit(solution)/shard_map/while/body/eval_jaxpr/jit(_solve_triangular)/vmap()/triangular_solve | solution.py:74
  180.2 1.3 bitcast_multiply_fusion.11
  181.5 12.8 %select_bitcast_fusion.3 = (f32[4,64,64,64]{3,0,2,1:T(4,128)}, f32[4,64,64,64]{3,0,2,1:T(4,128)}) fusion(f32[64,4,64]{2,1,0:T(4,128)S(1)} %fusion.151, pred[64,64]{1,0:T(8,128)(4,1)S(1)} %get-tuple-element.380, f32[64,4,64]{2,1,0:T(4,128)S(1)} %get-tuple-element.381, pred[64,64]{1,0:T(8,128)(4,1)S(1)} %get-tuple-element.382), kind=kLoop, calls=%fused_computation.19.clone.1 | loop fusion | flops 6291456 | bytes 8527872 | tf_op jit(solution)/shard_map/while
  194.3 10.7 %copy.249 = f32[4,64,64,64]{1,2,3,0:T(8,128)} copy(f32[4,64,64,64]{3,0,2,1:T(4,128)} %get-tuple-element.383) | data formatting | bytes 8388608 | tf_op jit(solution)/shard_map/while
  205.0 10.6 %copy.253 = f32[4,64,64,64]{1,2,3,0:T(8,128)} copy(f32[4,64,64,64]{3,0,2,1:T(4,128)} %get-tuple-element.387) | data formatting | bytes 8388608 | tf_op jit(solution)/shard_map/while
  218.0 7.5 fusion.154
  225.7 19.7 %custom-call.7 = f32[4,1,64,64]{2,3,1,0:T(8,128)S(1)} custom-call(f32[4,1,64,64]{3,2,1,0:T(8,128)S(1)} %add_bitcast_fusion.2), custom_call_target="InvertDiagBlocksLowerTriangular" | custom-call | tf_op jit(solution)/shard_map/while/body/eval_jaxpr/jit(_solve_triangular)/vmap()/triangular_solve | solution.py:74
  250.9 1.3 bitcast_multiply_fusion.11
  252.3 12.8 %select_bitcast_fusion.3 = (f32[4,64,64,64]{3,0,2,1:T(4,128)}, f32[4,64,64,64]{3,0,2,1:T(4,128)}) fusion(f32[64,4,64]{2,1,0:T(4,128)S(1)} %fusion.151, pred[64,64]{1,0:T(8,128)(4,1)S(1)} %get-tuple-element.380, f32[64,4,64]{2,1,0:T(4,128)S(1)} %get-tuple-element.381, pred[64,64]{1,0:T(8,128)(4,1)S(1)} %get-tuple-element.382), kind=kLoop, calls=%fused_computation.19.clone.1 | loop fusion | flops 6291456 | bytes 8527872 | tf_op jit(solution)/shard_map/while
  265.1 10.7 %copy.249 = f32[4,64,64,64]{1,2,3,0:T(8,128)} copy(f32[4,64,64,64]{3,0,2,1:T(4,128)} %get-tuple-element.383) | data formatting | bytes 8388608 | tf_op jit(solution)/shard_map/while
  275.7 10.6 %copy.253 = f32[4,64,64,64]{1,2,3,0:T(8,128)} copy(f32[4,64,64,64]{3,0,2,1:T(4,128)} %get-tuple-element.387) | data formatting | bytes 8388608 | tf_op jit(solution)/shard_map/while
  288.8 7.5 fusion.154
  296.5 19.7 %custom-call.7 = f32[4,1,64,64]{2,3,1,0:T(8,128)S(1)} custom-call(f32[4,1,64,64]{3,2,1,0:T(8,128)S(1)} %add_bitcast_fusion.2), custom_call_target="InvertDiagBlocksLowerTriangular" | custom-call | tf_op jit(solution)/shard_map/while/body/eval_jaxpr/jit(_solve_triangular)/vmap()/triangular_solve | solution.py:74
  321.6 1.3 bitcast_multiply_fusion.11
  323.0 12.8 %select_bitcast_fusion.3 = (f32[4,64,64,64]{3,0,2,1:T(4,128)}, f32[4,64,64,64]{3,0,2,1:T(4,128)}) fusion(f32[64,4,64]{2,1,0:T(4,128)S(1)} %fusion.151, pred[64,64]{1,0:T(8,128)(4,1)S(1)} %get-tuple-element.380, f32[64,4,64]{2,1,0:T(4,128)S(1)} %get-tuple-element.381, pred[64,64]{1,0:T(8,128)(4,1)S(1)} %get-tuple-element.382), kind=kLoop, calls=%fused_computation.19.clone.1 | loop fusion | flops 6291456 | bytes 8527872 | tf_op jit(solution)/shard_map/while
  335.8 10.7 %copy.249 = f32[4,64,64,64]{1,2,3,0:T(8,128)} copy(f32[4,64,64,64]{3,0,2,1:T(4,128)} %get-tuple-element.383) | data formatting | bytes 8388608 | tf_op jit(solution)/shard_map/while
  346.5 10.6 %copy.253 = f32[4,64,64,64]{1,2,3,0:T(8,128)} copy(f32[4,64,64,64]{3,0,2,1:T(4,128)} %get-tuple-element.387) | data formatting | bytes 8388608 | tf_op jit(solution)/shard_map/while
  359.5 7.5 fusion.154
  367.2 19.7 %custom-call.7 = f32[4,1,64,64]{2,3,1,0:T(8,128)S(1)} custom-call(f32[4,1,64,64]{3,2,1,0:T(8,128)S(1)} %add_bitcast_fusion.2), custom_call_target="InvertDiagBlocksLowerTriangular" | custom-call | tf_op jit(solution)/shard_map/while/body/eval_jaxpr/jit(_solve_triangular)/vmap()/triangular_solve | solution.py:74
  393.7 12.8 %select_bitcast_fusion.3 = (f32[4,64,64,64]{3,0,2,1:T(4,128)}, f32[4,64,64,64]{3,0,2,1:T(4,128)}) fusion(f32[64,4,64]{2,1,0:T(4,128)S(1)} %fusion.151, pred[64,64]{1,0:T(8,128)(4,1)S(1)} %get-tuple-element.380, f32[64,4,64]{2,1,0:T(4,128)S(1)} %get-tuple-element.381, pred[64,64]{1,0:T(8,128)(4,1)S(1)} %get-tuple-element.382), kind=kLoop, calls=%fused_computation.19.clone.1 | loop fusion | flops 6291456 | bytes 8527872 | tf_op jit(solution)/shard_map/while
  406.5 10.7 %copy.249 = f32[4,64,64,64]{1,2,3,0:T(8,128)} copy(f32[4,64,64,64]{3,0,2,1:T(4,128)} %get-tuple-element.383) | data formatting | bytes 8388608 | tf_op jit(solution)/shard_map/while
  417.2 10.6 %copy.253 = f32[4,64,64,64]{1,2,3,0:T(8,128)} copy(f32[4,64,64,64]{3,0,2,1:T(4,128)} %get-tuple-element.387) | data formatting | bytes 8388608 | tf_op jit(solution)/shard_map/while
  430.3 7.5 fusion.154
  438.0 19.7 %custom-call.7 = f32[4,1,64,64]{2,3,1,0:T(8,128)S(1)} custom-call(f32[4,1,64,64]{3,2,1,0:T(8,128)S(1)} %add_bitcast_fusion.2), custom_call_target="InvertDiagBlocksLowerTriangular" | custom-call | tf_op jit(solution)/shard_map/while/body/eval_jaxpr/jit(_solve_triangular)/vmap()/triangular_solve | solution.py:74
  464.5 12.8 %select_bitcast_fusion.3 = (f32[4,64,64,64]{3,0,2,1:T(4,128)}, f32[4,64,64,64]{3,0,2,1:T(4,128)}) fusion(f32[64,4,64]{2,1,0:T(4,128)S(1)} %fusion.151, pred[64,64]{1,0:T(8,128)(4,1)S(1)} %get-tuple-element.380, f32[64,4,64]{2,1,0:T(4,128)S(1)} %get-tuple-element.381, pred[64,64]{1,0:T(8,128)(4,1)S(1)} %get-tuple-element.382), kind=kLoop, calls=%fused_computation.19.clone.1 | loop fusion | flops 6291456 | bytes 8527872 | tf_op jit(solution)/shard_map/while
  477.3 10.7 %copy.249 = f32[4,64,64,64]{1,2,3,0:T(8,128)} copy(f32[4,64,64,64]{3,0,2,1:T(4,128)} %get-tuple-element.383) | data formatting | bytes 8388608 | tf_op jit(solution)/shard_map/while
  487.9 10.6 %copy.253 = f32[4,64,64,64]{1,2,3,0:T(8,128)} copy(f32[4,64,64,64]{3,0,2,1:T(4,128)} %get-tuple-element.387) | data formatting | bytes 8388608 | tf_op jit(solution)/shard_map/while
  501.0 7.5 fusion.154
  508.7 19.7 %custom-call.7 = f32[4,1,64,64]{2,3,1,0:T(8,128)S(1)} custom-call(f32[4,1,64,64]{3,2,1,0:T(8,128)S(1)} %add_bitcast_fusion.2), custom_call_target="InvertDiagBlocksLowerTriangular" | custom-call | tf_op jit(solution)/shard_map/while/body/eval_jaxpr/jit(_solve_triangular)/vmap()/triangular_solve | solution.py:74
  535.2 12.8 %select_bitcast_fusion.3 = (f32[4,64,64,64]{3,0,2,1:T(4,128)}, f32[4,64,64,64]{3,0,2,1:T(4,128)}) fusion(f32[64,4,64]{2,1,0:T(4,128)S(1)} %fusion.151, pred[64,64]{1,0:T(8,128)(4,1)S(1)} %get-tuple-element.380, f32[64,4,64]{2,1,0:T(4,128)S(1)} %get-tuple-element.381, pred[64,64]{1,0:T(8,128)(4,1)S(1)} %get-tuple-element.382), kind=kLoop, calls=%fused_computation.19.clone.1 | loop fusion | flops 6291456 | bytes 8527872 | tf_op jit(solution)/shard_map/while
  548.0 10.7 %copy.249 = f32[4,64,64,64]{1,2,3,0:T(8,128)} copy(f32[4,64,64,64]{3,0,2,1:T(4,128)} %get-tuple-element.383) | data formatting | bytes 8388608 | tf_op jit(solution)/shard_map/while
  558.7 10.6 %copy.253 = f32[4,64,64,64]{1,2,3,0:T(8,128)} copy(f32[4,64,64,64]{3,0,2,1:T(4,128)} %get-tuple-element.387) | data formatting | bytes 8388608 | tf_op jit(solution)/shard_map/while
  571.7 7.5 fusion.154
  579.4 19.7 %custom-call.7 = f32[4,1,64,64]{2,3,1,0:T(8,128)S(1)} custom-call(f32[4,1,64,64]{3,2,1,0:T(8,128)S(1)} %add_bitcast_fusion.2), custom_call_target="InvertDiagBlocksLowerTriangular" | custom-call | tf_op jit(solution)/shard_map/while/body/eval_jaxpr/jit(_solve_triangular)/vmap()/triangular_solve | solution.py:74
  603.7 1.5 copy.210
  605.8 33.9 %all-gather = bf16[32,64,64]{2,1,0:T(8,128)(2,1)} all-gather(bf16[4,64,64]{2,1,0:T(8,128)(2,1)S(1)} %get-tuple-element.270), channel_id=2, replica_groups=mesh['ep'=8,'tp'=4] {'ep'}, dimensions={0}, use_global_device_ids=true | all-gather | bytes 294912 | tf_op jit(solution)/shard_map/all_gather | solution.py:19
  639.7 33.5 %all-gather.1 = bf16[32,64,64]{2,1,0:T(8,128)(2,1)} all-gather(bf16[4,64,64]{2,1,0:T(8,128)(2,1)S(1)} %get-tuple-element.269), channel_id=3, replica_groups=mesh['ep'=8,'tp'=4] {'ep'}, dimensions={0}, use_global_device_ids=true | all-gather | bytes 294912 | tf_op jit(solution)/shard_map/all_gather | solution.py:19
  673.2 6.4 fusion.39
  679.6 10.7 %fusion.46 = bf16[2048,8,1,64]{0,3,1,2:T(8,128)(2,1)} fusion(bf16[1,1024,2048]{2,1,0:T(8,128)(2,1)} %param.41, f32[8,64,1024]{2,1,0:T(8,128)} %fusion.39, bf16[1,2048,1024]{2,1,0:T(8,128)(2,1)} %param.39, bf16[8,1,64,2048]{3,2,0,1:T(8,128)(2,1)} %all-gather.4.cloned.1.call-done), kind=kOutput, calls=%fused_computation.81 | convolution fusion | flops 4299161600 | bytes 14680064 | tf_op jit(solution)/shard_map/sxcf,xfd->dsxc/dot_general | solution.py:176
  690.6 17.0 %while.27 = (s32[]{:T(128)}, f32[4,64,64]{1,2,0:T(8,128)S(1)}, s32[]{:T(128)}, bf16[8,4,64,64]{3,2,1,0:T(8,128)(2,1)}, bf16[8,4,64,64]{3,2,1,0:T(8,128)(2,1)}, /*index=5*/s32[]{:T(128)}, s32[]{:T(128)}) while((s32[]{:T(128)}, f32[4,64,64]{1,2,0:T(8,128)S(1)}, s32[]{:T(128)}, bf16[8,4,64,64]{3,2,1,0:T(8,128)(2,1)}, ...), condition=%wide.region_5.6_spmd.clone, body=%wide.region_4.5_spmd.clone.sunk | while | flops 12664836 | bytes 723043 | solution.py:36
  707.6 1.5 fusion.89
  709.5 2.0 convolution_convert_fusion
  712.0 10.9 %reduce-scatter.5.cloned.1.call-done = bf16[512,8,1,64]{0,3,1,2:T(8,128)(2,1)} async-done(((bf16[2048,8,1,64]{0,3,1,2:T(8,128)(2,1)}), bf16[512,8,1,64]{0,3,1,2:T(8,128)(2,1)}) %reduce-scatter.5.cloned.1.call-update) | async-done | bytes 524304 | tf_op jit(solution)/shard_map/reduce_scatter | solution.py:175
  722.9 5.5 all-to-all-start.1
  728.9 13.8 %all-to-all-done.1 = bf16[512,8,1,64]{0,3,2,1:T(8,128)(2,1)S(1)} async-done(((bf16[512,8,1,64]{0,3,2,1:T(8,128)(2,1)}), bf16[512,8,1,64]{0,3,2,1:T(8,128)(2,1)S(1)}, u32[]{:S(2)}, u32[]{:S(2)}) %all-to-all-start.1) | async-done | bytes 524320 | tf_op jit(solution)/shard_map/all_to_all | solution.py:250
  743.8 13.4 %reduce-scatter.3.cloned.1.call-done = bf16[128,2048]{1,0:T(8,128)(2,1)} async-done(((bf16[512,2048]{1,0:T(8,128)(2,1)}), bf16[128,2048]{1,0:T(8,128)(2,1)}) %reduce-scatter.3.cloned.1.call-update) | async-done | bytes 524304 | tf_op jit(solution)/shard_map/reduce_scatter | solution.py:163
  (324 shorter events, 97.4 us)
Async XLA Ops:
  7.2 702.3 %copy-start = (bf16[256,2048]{1,0:T(8,128)(2,1)S(1)}, bf16[256,2048]{1,0:T(8,128)(2,1)}, u32[]{:S(2)}) copy-start(bf16[256,2048]{1,0:T(8,128)(2,1)} %param.33) | copy-start | bytes 3145732
  7.2 14.6 %copy-start.5 = (bf16[512,256]{1,0:T(8,128)(2,1)S(1)}, bf16[512,256]{1,0:T(8,128)(2,1)}, u32[]{:S(2)}) copy-start(bf16[512,256]{1,0:T(8,128)(2,1)} %param.24) | copy-start | bytes 786436
  11.5 1.9 copy-start.12
  11.5 12.9 %copy-start.3 = (bf16[512,256]{1,0:T(8,128)(2,1)S(1)}, bf16[512,256]{1,0:T(8,128)(2,1)}, u32[]{:S(2)}) copy-start(bf16[512,256]{1,0:T(8,128)(2,1)} %param.26) | copy-start | bytes 786436
  14.3 12.0 %copy-start.8 = (f32[512,4]{0,1:T(4,128)S(1)}, f32[512,4]{0,1:T(4,128)}, u32[]{:S(2)}) copy-start(f32[512,4]{0,1:T(4,128)} %param.31) | copy-start | bytes 24580
  14.3 12.9 %copy-start.9 = (f32[256]{0:T(256)S(1)}, f32[256]{0:T(256)}, u32[]{:S(2)}) copy-start(f32[256]{0:T(256)} %param.29) | copy-start | bytes 3076
  14.3 13.0 %copy-start.10 = (f32[256]{0:T(256)S(1)}, f32[256]{0:T(256)}, u32[]{:S(2)}) copy-start(f32[256]{0:T(256)} %param.30) | copy-start | bytes 3076
  14.3 23.0 %all-to-all-start = ((bf16[8,1,64,512]{3,2,1,0:T(8,128)(2,1)}), bf16[8,1,64,512]{3,2,1,0:T(8,128)(2,1)}, u32[]{:S(2)}, u32[]{:S(2)}) async-start(bf16[8,1,64,512]{3,2,1,0:T(8,128)(2,1)} %constant_dynamic-slice_fusion.2), calls=%async_computation.1 | async-start | bytes 1048576 | tf_op jit(solution)/shard_map/all_to_all | solution.py:238
  21.7 651.5 %all-gather.4.cloned.1.call-start = ((), (), s32[]{:S(2)}) async-start(), calls=%async_computation.5 | async-start | bytes 2621440 | tf_op jit(solution)/shard_map/all_gather | solution.py:237
  37.4 685.6 %reduce-scatter.5.cloned.1.call-start = ((), (), s32[]{:S(2)}) async-start(), calls=%async_computation.6 | async-start | bytes 2621440 | tf_op jit(solution)/shard_map/reduce_scatter | solution.py:175
  37.6 567.7 %copy-start.4 = (bf16[512,256]{1,0:T(8,128)(2,1)S(1)}, bf16[512,256]{1,0:T(8,128)(2,1)}, u32[]{:S(2)}) copy-start(bf16[512,256]{1,0:T(8,128)(2,1)} %param.28) | copy-start | bytes 786436
  37.6 568.1 %copy-start.11 = (f32[256]{0:T(256)S(1)}, f32[256]{0:T(256)}, u32[]{:S(2)}) copy-start(f32[256]{0:T(256)} %param.32) | copy-start | bytes 3076
  690.3 17.3 %copy-start.1 = (f32[8,64,4,128]{3,1,0,2:T(8,128)S(1)}, f32[8,64,4,128]{3,1,0,2:T(8,128)}, u32[]{:S(2)}) copy-start(f32[8,64,4,128]{3,1,0,2:T(8,128)} %get-tuple-element.144) | copy-start | bytes 3145732
  690.4 66.9 %reduce-scatter.3.cloned.1.call-start = ((), (), s32[]{:S(2)}) async-start(), calls=%async_computation.4 | async-start | bytes 2621440 | tf_op jit(solution)/shard_map/reduce_scatter | solution.py:163
  709.2 2.4 copy-start.2
  709.2 2.4 copy-start.7
  709.2 2.4 copy-start.13
  709.2 2.4 copy-start.14
  709.3 2.6 copy-start.6
  709.5 18.9 %copy-start.15 = (bf16[2048,4]{0,1:T(4,128)(2,1)S(1)}, bf16[2048,4]{0,1:T(4,128)(2,1)}, u32[]{:S(2)}) copy-start(bf16[2048,4]{0,1:T(4,128)(2,1)} %param.36) | copy-start | bytes 49156
  722.9 19.8 %all-to-all-start.1 = ((bf16[512,8,1,64]{0,3,2,1:T(8,128)(2,1)}), bf16[512,8,1,64]{0,3,2,1:T(8,128)(2,1)S(1)}, u32[]{:S(2)}, u32[]{:S(2)}) async-start(bf16[512,8,1,64]{0,3,2,1:T(8,128)(2,1)} %bitcast.285), calls=%async_computation.3 | async-start | bytes 1048576 | tf_op jit(solution)/shard_map/all_to_all | solution.py:250
Sparse Core Ops, SparseCore 0:
  37.5 23.9 all-gather.3
  690.5 32.3 reduce-scatter.4
  726.0 31.1 reduce-scatter.2
where the time goes:
time: 769 us; the launch traced here: 764 us
  other arithmetic  347 us (45%)
  local copies, waits for them, and re-layouts  220 us (29%)
  blocking collectives  67.4 us (9%)
  matrix products  61.2 us (8%)
  waiting for transfers between devices  38.2 us (5%)
  between operations  14.2 us (2%)
  starting transfers between devices  13.5 us (2%)
    while x24, local copies, waits for them, and re-layouts  171 us
    while x16, other arithmetic  162 us
    another operation x40, other arithmetic, block_advance(): jax.scipy.linalg.solve_triangular(left_side, right_side, lower=True, unit...  158 us
    all_gather x2, blocking collectives, carried_in(): lax.all_gather(part.astype(kind), axis)  67.4 us
    squeeze x48, local copies, waits for them, and re-layouts, mixer_part(): lax.scan(block_advance, start, (blocked(recept), blocked(decay_logarithm)...  19 us
  transfers between devices with their start and end apart: 5, of which 3 were waited for; matrix products, arithmetic and copies ran while one was open for 79% of the time, Pallas kernels for 0%

commit v1 on v0

v1 whole, which is shorter than its diff:
```python
import functools
import jax
import jax.numpy as jnp
from jax import lax
from jax.experimental import pallas as pl
from jax.experimental.pallas import tpu as pltpu
from jax.sharding import PartitionSpec as P

HEAD_DIM = 64
GROUPS = 4
PARTS = 1
key_eps = 1e-06
group_eps = 0.00064
norm_eps = 1e-06
BASE = 16

f32, bf16 = jnp.float32, jnp.bfloat16
NN = (((1,), (0,)), ((), ()))
NT = (((1,), (1,)), ((), ()))
TN = (((0,), (0,)), ((), ()))


def mm(a, b, dims=NN):
    return lax.dot_general(a, b, dims, preferred_element_type=f32)


def halves(x):
    high = x.astype(bf16)
    return high, (x - high.astype(f32)).astype(bf16)


def thirds(x):
    high = x.astype(bf16)
    rest = x - high.astype(f32)
    mid = rest.astype(bf16)
    return high, mid, (rest - mid.astype(f32)).astype(bf16)


def exact_right(x, ones, parts):
    return sum(mm(p, ones) for p in parts(x))


def exact_left(ones, x, parts):
    return sum(mm(ones, p) for p in parts(x))


def iota(shape, axis):
    return lax.broadcasted_iota(jnp.int32, shape, axis)


def head_mask(lanes):
    return iota((lanes, lanes), 0) // HEAD_DIM == iota((lanes, lanes), 1) // HEAD_DIM


def spread(x, mask):
    rep = mask.shape[0] // HEAD_DIM
    return jnp.where(mask, jnp.concatenate([x] * rep, axis=0), jnp.zeros((), x.dtype))


def fold(x):
    pieces = [x[i : i + HEAD_DIM] for i in range(0, x.shape[0], HEAD_DIM)]
    return functools.reduce(jnp.add, pieces)


def mixer_kernel(
    q_ref, k_ref, v_ref, w_ref, a_ref, wo_ref, ao_ref, ex_ref,
    local_ref, reach_ref, end_ref,
    u_s, r_s, c_s, ld_s, pair_s, diag_s, tri_s, ue_s, qe_s, kh_s, rh_s, up_s, qp_s, g_s, et_s,
):
    rows, lanes = q_ref.shape
    C = HEAD_DIM
    chunks = rows // C
    heads = lanes // HEAD_DIM
    hm = head_mask(lanes)
    ones_bd = hm.astype(bf16)

    k = k_ref[...].astype(f32)
    u = k * lax.rsqrt(exact_right(k * k, ones_bd, halves) + key_eps)
    u_s[...] = u
    r_s[...] = u * jax.nn.sigmoid(a_ref[...].astype(f32) + ao_ref[...])
    owner = (iota((heads, lanes), 1) // HEAD_DIM == iota((heads, lanes), 0)).astype(bf16)
    exb = sum(mm(p, owner, TN) for p in thirds(ex_ref[...]))
    pre = w_ref[...].astype(f32) + wo_ref[...]
    ld_s[...] = exb - jax.nn.sigmoid(pre) * 0.6065306597126334

    tri = (iota((C, C), 0) >= iota((C, C), 1)).astype(bf16)
    same = head_mask(lanes)
    rr, cc = iota((lanes, lanes), 0), iota((lanes, lanes), 1)
    strict = jnp.logical_and(same, rr > cc)
    upto = jnp.logical_and(same, rr >= cc)
    base_mask = rr // BASE == cc // BASE

    def first(i, _):
        at = pl.ds(pl.multiple_of(i * C, C), C)
        ld = ld_s[at, :]
        c = exact_left(tri, ld, thirds)
        tot = c[C - 1 : C, :]
        mid = 0.5 * tot
        em = jnp.exp(mid)
        eq = jnp.exp(c - mid)
        eu = jnp.exp(c - ld - mid)
        ek = jnp.exp(mid - c)
        ut, qt = u_s[at, :] * eu, q_ref[at, :].astype(f32) * eq
        kt, rt = k_ref[at, :].astype(f32) * ek, r_s[at, :] * ek
        ue_s[at, :] = (ut * em).astype(bf16)
        qe_s[at, :] = qt * em
        kh_s[at, :] = (kt * em).astype(bf16)
        rh_s[at, :] = (rt * em).astype(bf16)
        et_s[pl.ds(i, 1), :] = em * em
        left = jnp.concatenate([spread(ut.astype(bf16), hm), spread(qt.astype(bf16), hm)], axis=0)
        right = jnp.concatenate([spread(kt.astype(bf16), hm), spread(rt.astype(bf16), hm)], axis=0)
        pairs = mm(left, right, NT)
        uk = jnp.where(strict, pairs[:lanes, :lanes], 0.0)
        ur = jnp.where(strict, pairs[:lanes, lanes:], 0.0)
        qk = jnp.where(upto, pairs[lanes:, :lanes], 0.0)
        qr = jnp.where(upto, pairs[lanes:, lanes:], 0.0)
        pair_s[i, 0] = uk.astype(bf16)
        pair_s[i, 1] = ur.astype(bf16)
        pair_s[i, 2] = qk.astype(bf16)
        pair_s[i, 3] = qr.astype(bf16)
        dg = jnp.where(base_mask, ur, 0.0)
        diag_s[i] = functools.reduce(
            jnp.add, [dg[p : p + BASE] for p in range(0, lanes, BASE)]
        )
        return 0

    lax.fori_loop(0, chunks, first, 0, unroll=2)

    dparts = thirds(diag_s[...].reshape(chunks * BASE, lanes))
    t = jnp.where(
        iota((chunks, BASE, lanes), 1) == iota((chunks, BASE, lanes), 2) % BASE, 1.0, 0.0
    ).astype(f32)
    for j in range(BASE - 1):
        pick = jnp.logical_and(base_mask, rr % BASE == j).astype(bf16)
        col = sum(mm(p, pick) for p in dparts).reshape(chunks, BASE, lanes)
        t = t - col * t[:, j : j + 1, :]
    tri_s[...] = t

    m32 = jnp.logical_and(rr // (2 * BASE) == cc // (2 * BASE), jnp.logical_not(base_mask))
    m64 = rr // (2 * BASE) != cc // (2 * BASE)
    pickv = (iota((HEAD_DIM, lanes), 0) == iota((HEAD_DIM, lanes), 1) % HEAD_DIM).astype(bf16)
    zero = jnp.zeros((), bf16)

    def second(i, _):
        at = pl.ds(pl.multiple_of(i * C, C), C)
        uk, ur, qk, qr = pair_s[i, 0], pair_s[i, 1], pair_s[i, 2], pair_s[i, 3]
        td = tri_s[i]
        t16 = jnp.where(base_mask, jnp.concatenate([td] * (lanes // BASE), axis=0), 0.0)
        t16b = t16.astype(bf16)
        p1 = mm(jnp.where(m32, ur, zero), t16b).astype(bf16)
        t32 = t16 - mm(t16b, p1)
        t32b = t32.astype(bf16)
        p2 = mm(jnp.where(m64, ur, zero), t32b).astype(bf16)
        t64 = (t32 - mm(t32b, p2)).astype(bf16)
        ubd = spread(ue_s[at, :], hm)
        ta = mm(t64, uk).astype(bf16)
        up = mm(t64, ubd).astype(bf16)
        up_s[i] = up
        vbd = spread(v_ref[at, :], hm)
        za = mm(ta, vbd)
        o = mm(qk, vbd) - mm(qr, za.astype(bf16))
        local_ref[at, :] = fold(o)
        qp_s[at, :] = (qe_s[at, :] - fold(mm(qr, up))).astype(bf16)
        vt = mm(pickv, vbd, NT).astype(bf16)
        zat = mm(vt, ta, NT).astype(bf16)
        g_s[i] = mm(vt, spread(kh_s[at, :], hm)) - mm(zat, spread(rh_s[at, :], hm))
        return 0

    lax.fori_loop(0, chunks, second, 0, unroll=2)

    def third(i, x):
        at = pl.ds(pl.multiple_of(i * C, C), C)
        xb = x.astype(bf16)
        xs, xm = xb[:HEAD_DIM], xb[HEAD_DIM:]
        qp = qp_s[at, :]
        local_ref[at, :] += mm(qp, spread(xs, hm), NT)
        reach_ref[at, :] = mm(qp, spread(xm, hm), NT).astype(bf16)
        at_ = mm(xb, up_s[i], NT).astype(bf16)
        corr = mm(at_, spread(rh_s[at, :], hm))
        g = g_s[i]
        return x * et_s[pl.ds(i, 1), :] + jnp.concatenate([g, jnp.zeros_like(g)], axis=0) - corr

    x0 = jnp.concatenate([jnp.zeros((HEAD_DIM, lanes), f32), pickv.astype(f32)], axis=0)
    x = lax.fori_loop(0, chunks, third, x0, unroll=2)
    end_ref[...] = x.astype(bf16)


def mixer_local(q, k, v, w, a, wo, ao, ex):
    rows, lanes = q.shape
    chunks = rows // HEAD_DIM
    V = pltpu.VMEM
    return pl.pallas_call(
        mixer_kernel,
        out_shape=(
            jax.ShapeDtypeStruct((rows, lanes), f32),
            jax.ShapeDtypeStruct((rows, lanes), bf16),
            jax.ShapeDtypeStruct((2 * HEAD_DIM, lanes), bf16),
        ),
        scratch_shapes=[
            V((rows, lanes), f32), V((rows, lanes), f32), V((8, 128), f32), V((rows, lanes), f32),
            V((chunks, 4, lanes, lanes), bf16), V((chunks, BASE, lanes), f32), V((chunks, BASE, lanes), f32),
            V((rows, lanes), bf16), V((rows, lanes), f32), V((rows, lanes), bf16), V((rows, lanes), bf16),
            V((chunks, lanes, lanes), bf16), V((rows, lanes), bf16), V((chunks, HEAD_DIM, lanes), f32),
            V((chunks, lanes), f32),
        ],
        compiler_params=pltpu.CompilerParams(vmem_limit_bytes=40 * 1024 * 1024),
        cost_estimate=pl.CostEstimate(flops=30_000_000_000, bytes_accessed=4_000_000, transcendentals=0),
        name="mixer_local",
    )(q, k, v, w, a, wo.reshape(1, -1), ao.reshape(1, -1), ex)


def finish_kernel(place_ref, ends_ref, local_ref, reach_ref, gate_ref, gain_ref, out_ref, mixed_s):
    devices, _, lanes = ends_ref.shape
    hm = head_mask(lanes)
    ones_bd = hm.astype(bf16)
    place = place_ref[0]

    def hop(e, s):
        pbd = spread(ends_ref[e, HEAD_DIM:, :], hm)
        new = sum(mm(p, pbd) for p in halves(s)) + ends_ref[e, :HEAD_DIM, :].astype(f32)
        return jnp.where(e < place, new, s)

    s = lax.fori_loop(0, devices - 1, hop, jnp.zeros((HEAD_DIM, lanes), f32), unroll=True)
    head_out = local_ref[...] + mm(reach_ref[...], spread(s.astype(bf16), hm), NT)
    centred = head_out - exact_right(head_out, ones_bd, halves) * (1.0 / HEAD_DIM)
    var = exact_right(centred * centred, ones_bd, halves) * (1.0 / HEAD_DIM)
    gate = jax.nn.sigmoid(gate_ref[...].astype(f32))
    mixed_s[...] = centred * lax.rsqrt(var + group_eps) * gain_ref[...] * gate
    count, rows, _ = out_ref.shape
    for m in range(count):
        at = pl.multiple_of(lax.bitwise_xor(place_ref[1], m) * rows, rows)
        out_ref[m] = mixed_s[pl.ds(at, rows), :].astype(bf16)


def mixer_finish(place, ends, local, reach, gate, gain, count):
    vm = pl.BlockSpec(memory_space=pltpu.VMEM)
    return pl.pallas_call(
        finish_kernel,
        out_shape=jax.ShapeDtypeStruct((count, local.shape[0] // count, local.shape[1]), bf16),
        in_specs=[pl.BlockSpec(memory_space=pltpu.SMEM)] + [vm] * 5,
        out_specs=vm,
        scratch_shapes=[pltpu.VMEM(local.shape, f32)],
        compiler_params=pltpu.CompilerParams(vmem_limit_bytes=24 * 1024 * 1024),
        cost_estimate=pl.CostEstimate(flops=4_000_000_000, bytes_accessed=2_000_000, transcendentals=0),
        name="mixer_finish",
    )(place, ends, local, reach, gate, gain.reshape(1, -1))


def route_kernel(place_ref, x_ref, gain_ref, gw_ref, ew_ref, routes_ref, *outs):
    send_refs, info_ref = outs[:-1], outs[-1]
    tokens, width = x_ref.shape
    experts, part, share = send_refs[0].shape
    per_group = experts // GROUPS
    x = x_ref[...].astype(f32)
    scale = lax.rsqrt(jnp.mean(x * x, axis=-1, keepdims=True) + norm_eps)
    normed = (x * scale * gain_ref[...]).astype(bf16)
    group_exp = jnp.exp(mm(gw_ref[...], normed, NT))
    group_prob = group_exp / jnp.sum(group_exp, axis=0, keepdims=True)
    logit = mm(ew_ref[...], normed, NT)
    top = routes_ref.shape[0]
    ids = [routes_ref[k : k + 1, :] for k in range(top)]
    match = [iota((experts, tokens), 0) == i for i in ids]
    chosen = [jnp.sum(jnp.where(m, logit, 0.0), axis=0, keepdims=True) for m in match]
    group = [
        jnp.sum(
            jnp.where(iota((GROUPS, tokens), 0) == i // per_group, group_prob, 0.0),
            axis=0, keepdims=True,
        )
        for i in ids
    ]
    weights = [group[k] * jax.nn.sigmoid(chosen[k] - chosen[top - 1 - k]) for k in range(top)]
    counts = sum(m.astype(f32) for m in match)
    earlier = (iota((tokens, tokens), 0) < iota((tokens, tokens), 1)).astype(bf16)
    before = mm(counts.astype(bf16), earlier)
    placed = [jnp.sum(jnp.where(m, before, 0.0), axis=0, keepdims=True) for m in match]
    rows = weights + placed + [i.astype(f32) for i in ids]
    rows += [jnp.zeros((1, tokens), f32)] * (8 - len(rows))
    info_ref[...] = jnp.transpose(jnp.concatenate(rows, axis=0))
    own = pl.multiple_of(place_ref[0] * share, share)
    mine = (
        x_ref[:, pl.ds(own, share)].astype(f32) * scale * gain_ref[:, pl.ds(own, share)]
    ).astype(bf16)
    slots = iota((experts * part, tokens), 0)
    for j, send_ref in enumerate(send_refs):
        hit = None
        for i, p in zip(ids, placed):
            p = p.astype(jnp.int32)
            inside = jnp.logical_and(p >= j * part, p < (j + 1) * part)
            h = jnp.logical_and(slots == i * part + p - j * part, inside)
            hit = h if hit is None else jnp.logical_or(hit, h)
        send_ref[...] = mm(hit.astype(bf16), mine).astype(bf16).reshape(experts, part, share)


def route(place, x, gain, gw, ew, routes, parts, part, share):
    experts, tokens = ew.shape[0], x.shape[0]
    vm = pl.BlockSpec(memory_space=pltpu.VMEM)
    return pl.pallas_call(
        route_kernel,
        out_shape=[jax.ShapeDtypeStruct((experts, part, share), bf16)] * parts
        + [jax.ShapeDtypeStruct((tokens, 8), f32)],
        in_specs=[pl.BlockSpec(memory_space=pltpu.SMEM)] + [vm] * 5,
        out_specs=[vm] * (parts + 1),
        compiler_params=pltpu.CompilerParams(vmem_limit_bytes=24 * 1024 * 1024),
        cost_estimate=pl.CostEstimate(flops=4_000_000_000, bytes_accessed=1_000_000, transcendentals=0),
        name="route",
    )(place, x, gain.reshape(1, -1), gw, ew, routes)


def combine_kernel(info_ref, *refs, top):
    homes, out_ref = refs[:-1], refs[-1]
    tokens = info_ref.shape[0]
    experts, part, share = homes[0].shape
    slots = iota((tokens, experts * part), 1)
    total = jnp.zeros((tokens, share), f32)
    for k in range(top):
        p = info_ref[:, top + k : top + k + 1].astype(jnp.int32)
        i = info_ref[:, 2 * top + k : 2 * top + k + 1].astype(jnp.int32)
        rows = jnp.zeros((tokens, share), f32)
        for j, home in enumerate(homes):
            inside = jnp.logical_and(p >= j * part, p < (j + 1) * part)
            h = jnp.logical_and(slots == i * part + p - j * part, inside)
            rows += mm(h.astype(bf16), home[...].reshape(experts * part, share))
        total += info_ref[:, k : k + 1] * rows
    out_ref[...] = total.astype(bf16)


def combine(info, homes, top):
    vm = pl.BlockSpec(memory_space=pltpu.VMEM)
    return pl.pallas_call(
        functools.partial(combine_kernel, top=top),
        out_shape=jax.ShapeDtypeStruct((info.shape[0], homes[0].shape[2]), bf16),
        in_specs=[vm] * (1 + len(homes)),
        out_specs=vm,
        compiler_params=pltpu.CompilerParams(vmem_limit_bytes=24 * 1024 * 1024),
        cost_estimate=pl.CostEstimate(flops=1_000_000_000, bytes_accessed=1_000_000, transcendentals=0),
        name="combine",
    )(info, *homes)


def tile_of(size, most):
    return most if size % most == 0 else size


def hidden_kernel(place_ref, *refs, masks):
    xs, (wg_ref, wu_ref, out_ref) = refs[: len(masks)], refs[len(masks) :]
    share = xs[0].shape[1]
    gate = up = None
    for m, x in zip(masks, xs):
        at = pl.ds(pl.multiple_of(lax.bitwise_xor(place_ref[0], m) * share, share), share)
        g, u = mm(x[...], wg_ref[0, at, :]), mm(x[...], wu_ref[0, at, :])
        gate, up = (g, u) if gate is None else (gate + g, up + u)
    out_ref[...] = (gate * jax.nn.sigmoid(gate) * up).astype(bf16)


def hidden(place, masks, xs, wg, wu):
    rows, share = xs[0].shape
    _, width, units = wg.shape
    tile = tile_of(units, 256)
    weight = pl.BlockSpec((1, width, tile), lambda f, p: (0, 0, f))
    return pl.pallas_call(
        functools.partial(hidden_kernel, masks=masks),
        grid_spec=pltpu.PrefetchScalarGridSpec(
            num_scalar_prefetch=1,
            grid=(units // tile,),
            in_specs=[pl.BlockSpec((rows, share), lambda f, p: (0, 0))] * len(xs) + [weight] * 2,
            out_specs=pl.BlockSpec((rows, tile), lambda f, p: (0, f)),
        ),
        out_shape=jax.ShapeDtypeStruct((rows, units), bf16),
        compiler_params=pltpu.CompilerParams(vmem_limit_bytes=32 * 1024 * 1024),
        cost_estimate=pl.CostEstimate(
            flops=4 * rows * width * units, bytes_accessed=4 * width * units, transcendentals=0
        ),
        name="hidden",
    )(place, *xs, wg, wu)


def down_kernel(place_ref, h_ref, w_ref, out_ref):
    out_ref[0] = mm(h_ref[...], w_ref[0]).astype(bf16)


def down(place, masks, h, wd, share):
    rows, units = h.shape
    masks = tuple(masks)

    def column(i, p):
        mask = jnp.int32(masks[-1])
        for j in range(len(masks) - 2, -1, -1):
            mask = jnp.where(i == j, jnp.int32(masks[j]), mask)
        return 0, 0, lax.bitwise_xor(p[0], mask)

    return pl.pallas_call(
        down_kernel,
        grid_spec=pltpu.PrefetchScalarGridSpec(
            num_scalar_prefetch=1,
            grid=(len(masks),),
            in_specs=[
                pl.BlockSpec((rows, units), lambda i, p: (0, 0)),
                pl.BlockSpec((1, units, share), column),
            ],
            out_specs=pl.BlockSpec((1, rows, share), lambda i, p: (i, 0, 0)),
        ),
        out_shape=jax.ShapeDtypeStruct((len(masks), rows, share), bf16),
        compiler_params=pltpu.CompilerParams(vmem_limit_bytes=24 * 1024 * 1024),
        cost_estimate=pl.CostEstimate(
            flops=2 * rows * units * share * len(masks),
            bytes_accessed=2 * units * share * len(masks), transcendentals=0,
        ),
        name="down",
    )(place, h, wd)


def project_kernel(*refs):
    out_ref = refs[-1]
    count = (len(refs) - 1) // 2
    total = None
    for x, w in zip(refs[:count], refs[count:-1]):
        p = mm(x[...], w[...]).astype(bf16).astype(f32)
        total = p if total is None else total + p
    out_ref[...] = total.astype(bf16)


def project(xs, ws):
    rows, lanes = xs[0].shape
    width = ws[0].shape[1]
    tile = tile_of(width, 512)
    return pl.pallas_call(
        project_kernel,
        grid=(width // tile,),
        in_specs=[pl.BlockSpec((rows, lanes), lambda i: (0, 0))] * len(xs)
        + [pl.BlockSpec((lanes, tile), lambda i: (0, i))] * len(ws),
        out_specs=pl.BlockSpec((rows, tile), lambda i: (0, i)),
        out_shape=jax.ShapeDtypeStruct((rows, width), bf16),
        compiler_params=pltpu.CompilerParams(vmem_limit_bytes=24 * 1024 * 1024),
        cost_estimate=pl.CostEstimate(
            flops=2 * rows * lanes * width * len(xs),
            bytes_accessed=2 * lanes * width * len(xs), transcendentals=0,
        ),
        name="project",
    )(*xs, *ws)


def swap(x, mask):
    count = lax.axis_size("tp")
    return lax.ppermute(x, "tp", [(i, i ^ mask) for i in range(count)])


def gathered(x, far=None):
    masks, blocks = [0], [x]
    mask = lax.axis_size("tp") // 2
    if far is not None:
        masks, blocks, mask = [0, mask], [x, far], mask // 2
    while mask:
        blocks += [swap(b, mask) for b in blocks]
        masks += [m ^ mask for m in masks]
        mask //= 2
    return tuple(masks), blocks


def local(
    receptance, key_matrix, value_matrix, decay_data_term, correction_rate_data,
    output_gate_input, decay_channel_offset, correction_rate_offset, extra_head_log_decay,
    head_norm_gain, mixer_output_weight, expert_layer_input, feedforward_norm_gain,
    group_router_weight, expert_router_weight, routes, expert_gate_weight, expert_up_weight,
    expert_down_weight,
):
    ep, tp = lax.axis_size("ep"), lax.axis_size("tp")
    place = lax.axis_index("tp").reshape(1).astype(jnp.int32)
    turn = lax.axis_index("ep").reshape(1).astype(jnp.int32)
    tokens, width = expert_layer_input.shape
    experts = expert_router_weight.shape[1]
    share = width // tp
    capacity = 4 * tokens // ep
    part = capacity // PARTS

    *sends, info = route(
        place, expert_layer_input, feedforward_norm_gain, group_router_weight.T,
        expert_router_weight.T, routes.T, PARTS, part, share,
    )
    arrived = [lax.all_to_all(s, "ep", split_axis=0, concat_axis=0, tiled=True) for s in sends]
    masks, blocks = [0], [mixer_output_weight]
    top_mask = tp // 2
    far = swap(mixer_output_weight, top_mask)

    local_read, reached, end = mixer_local(
        receptance, key_matrix, value_matrix, decay_data_term, correction_rate_data,
        decay_channel_offset, correction_rate_offset, extra_head_log_decay.T,
    )
    arrived, far, end = lax.optimization_barrier((arrived, far, end))
    weight_masks, weight_blocks = gathered(mixer_output_weight, far)
    ends = lax.all_to_all(
        jnp.broadcast_to(end[None], (ep,) + end.shape), "ep", split_axis=0, concat_axis=0, tiled=True
    )

    waiting = []
    for piece in arrived:
        masks, blocks = gathered(piece.reshape(experts * part, share))
        h = hidden(place, masks, blocks, expert_gate_weight, expert_up_weight)
        todo, bit = list(range(tp)), 1
        odd = [m for m in todo if m & bit]
        even = [m for m in todo if not m & bit]
        send = down(place, odd, h, expert_down_weight, share)
        keep = down(place, even, h, expert_down_weight, share)
        while True:
            got = swap(send, bit)
            bit *= 2
            if bit >= tp:
                break
            total = (keep.astype(f32) + got.astype(f32)).astype(bf16)
            total = total.reshape((-1, 2) + total.shape[1:])
            keep, send = total[:, 0], total[:, 1]
        waiting.append((keep, got))

    mixed = mixer_finish(
        jnp.concatenate([turn, place]), ends, local_read, reached, output_gate_input, head_norm_gain, tp
    )
    pieces = [mixed[m] if m == 0 else swap(mixed[m], m) for m in weight_masks]
    token_mixer_output = project(pieces, weight_blocks)
    waiting, token_mixer_output = lax.optimization_barrier((waiting, token_mixer_output))
    homes = []
    for keep, got in waiting:
        total = (keep.astype(f32) + got.astype(f32)).astype(bf16).reshape(experts, part, share)
        homes.append(lax.all_to_all(total, "ep", split_axis=0, concat_axis=0, tiled=True))
    expert_out = combine(info, homes, routes.shape[1])
    return (token_mixer_output, expert_out)


def solution(mesh):
    in_specs = (
        P("ep", "tp"), P("ep", "tp"), P("ep", "tp"), P("ep", "tp"), P("ep", "tp"), P("ep", "tp"),
        P("tp"), P("tp"), P("ep", "tp"), P("tp"), P("tp", None), P("ep", None), P(), P(), P(),
        P("ep", None), P("ep", None, "tp"), P("ep", None, "tp"), P("ep", "tp", None),
    )
    out_specs = (P(("ep", "tp"), None), P("ep", "tp"))
    return jax.shard_map(local, mesh=mesh, in_specs=in_specs, out_specs=out_specs, check_vma=False)
```

time: 769 us -> 125 us (0.16)
  other arithmetic: 347 us -> 2.84 us
  local copies, waits for them, and re-layouts: 220 us -> 17.6 us
  matrix products: 61.2 us -> 0 us
  blocking collectives: 67.4 us -> 20.7 us
  Pallas kernels: 0 us -> 39.8 us
  waiting for transfers between devices: 38.2 us -> 23.1 us
  between operations: 14.2 us -> 0.86 us
    while x26 -> x0, local copies, waits for them, and re-layouts: 172 us -> none
    another operation x50 -> x0, other arithmetic: 167 us -> none  [the longest x40 158 us: block_advance(): jax.scipy.linalg.solve_triangular(left_side, right_side, lower=True, unit...]
    while x16 -> x0, other arithmetic: 162 us -> none
    all_gather x2 -> x0, blocking collectives: 67.4 us -> none  [carried_in(): lax.all_gather(part.astype(kind), axis)]
    dot_general x72 -> x0, matrix products: 58.1 us -> none  [the longest x1 10.7 us: finish_experts(): jnp.einsum('sxcf,xfd->dsxc', expert_hidden, expert_down_weight, preferred...]
    pallas_call x0 -> x8, Pallas kernels: none -> 39.8 us  [the longest x1 19.5 us: mixer_local(): pl.pallas_call(mixer_kernel, out_shape=(jax.ShapeDtypeStruct((rows, lanes...]
    reduce_scatter x2 -> x0, waiting for transfers between devices: 24.3 us -> none  [the longest x1 13.4 us: mixer_part(): lax.psum_scatter(jnp.dot(mixed_hidden, mixer_output_weight, preferred_ele...]
    all_to_all x0 -> x1, blocking collectives: none -> 20.7 us  [local(): lax.all_to_all(total, 'ep', split_axis=0, concat_axis=0, tiled=True)]
  transfers between devices with their start and end apart: 5 -> 13, of which waited for: 3 -> 6; matrix products, arithmetic and copies ran while one was open for 79% -> 3% of each run, Pallas kernels for 0% -> 23%
where the time goes in v1:
time: 125 us
  Pallas kernels  39.8 us (32%)
  waiting for transfers between devices  23.1 us (18%)
  blocking collectives  20.7 us (17%)
  starting transfers between devices  19.6 us (16%)
  local copies, waits for them, and re-layouts  17.6 us (14%)
  other arithmetic  2.84 us (2%)
    all_to_all x1, blocking collectives, local(): lax.all_to_all(total, 'ep', split_axis=0, concat_axis=0, tiled=True)  20.7 us
    pallas_call x1, Pallas kernels, mixer_local(): pl.pallas_call(mixer_kernel, out_shape=(jax.ShapeDtypeStruct((rows, lanes...  19.5 us
    ppermute x11, waiting for transfers between devices, swap(): return lax.ppermute(x, 'tp', [(i, i ^ mask) for i in range(count)])  15.8 us
    unnamed x54, local copies, waits for them, and re-layouts  15.7 us
    all_to_all x1, starting transfers between devices, local(): lax.all_to_all(s, 'ep', split_axis=0, concat_axis=0, tiled=True)  7.28 us
    all_to_all x1, waiting for transfers between devices, local(): lax.all_to_all(jnp.broadcast_to(end[None], (ep,) + end.shape), 'ep', spli...  7.25 us
    ppermute x11, starting transfers between devices, swap(): return lax.ppermute(x, 'tp', [(i, i ^ mask) for i in range(count)])  6.73 us
    pallas_call x1, Pallas kernels, hidden(): pl.pallas_call(functools.partial(hidden_kernel, masks=masks), grid_spec=p...  6.26 us
  transfers between devices with their start and end apart: 13, of which 6 were waited for; matrix products, arithmetic and copies ran while one was open for 3% of the time, Pallas kernels for 23%

profile of v1, /device:TPU:0, one launch (start us, length us, event | category | flops | bytes accessed | tf_op | source)
XLA Modules:
  0.0 124.5 jit_solution(7477447442769528674)
XLA Ops:
  0.6 0.0 copy-start.7
  0.6 1.0 copy-done.7
  1.7 0.8 copy-done.14
  2.4 0.7 copy-done.15
  3.2 0.7 copy-done.16
  3.9 0.7 copy-done.18
  4.6 1.7 %route.1 = (bf16[8,64,512]{2,1,0:T(8,128)(2,1)}, f32[128,8]{1,0:T(8,128)S(1)}) custom-call(s32[1]{0:T(128)} %bitcast.place_ref, bf16[128,2048]{1,0:T(8,128)(2,1)S(1)} %copy-done.7, f32[1,2048]{1,0:T(1,128)S(1)} %bitcast.31, bf16[4,2048]{1,0:T(4,128)(2,1)S(1)} %bitcast.30, bf16[8,2048]{1,0:T(8,128)(2,1)S(1)} %bitcast.29, s32[2,128]{1,0:T(2,128)S(1)} %bitcast.33), custom_call_target="tpu_custom_call" | custom-call | flops 4000000000 | bytes 1000000 | tf_op jit(solution)/shard_map/route/pallas_call | solution.py:297
  6.3 7.3 %all-to-all-start = ((bf16[8,64,512]{2,1,0:T(8,128)(2,1)}), bf16[8,64,512]{2,1,0:T(8,128)(2,1)S(1)}, u32[]{:S(2)}, u32[]{:S(2)}) async-start(bf16[8,64,512]{2,1,0:T(8,128)(2,1)} %get-tuple-element.13), calls=%async_computation | async-start | bytes 1048576 | tf_op jit(solution)/shard_map/all_to_all | solution.py:479
  13.6 1.6 %collective-permute-start = (bf16[256,2048]{1,0:T(8,128)(2,1)S(1)}, bf16[256,2048]{1,0:T(8,128)(2,1)S(1)}, u32[]{:S(2)}, u32[]{:S(2)}) collective-permute-start(bf16[256,2048]{1,0:T(8,128)(2,1)S(1)} %copy-done.2), channel_id=1, source_target_pairs={{0,2},{1,3},{2,0},{3,1},{4,6},{5,7},{6,4},{7,5},{8,10},{9,11},{10,... | collective-permute-start | bytes 3145736 | tf_op jit(solution)/shard_map/ppermute | solution.py:444
  15.1 0.0 copy-done.17
  15.2 0.0 copy-done.19
  15.2 0.0 copy-done.20
  15.2 0.0 copy-start.11
  15.2 0.9 copy-done.11
  16.1 0.9 copy-done.12
  17.1 19.5 %mixer_local.1 = (f32[512,256]{1,0:T(8,128)S(1)}, bf16[512,256]{1,0:T(8,128)(2,1)S(1)}, bf16[128,256]{1,0:T(8,128)(2,1)S(1)}) custom-call(bf16[512,256]{1,0:T(8,128)(2,1)S(1)} %copy-done.8, bf16[512,256]{1,0:T(8,128)(2,1)S(1)} %copy-done.9, bf16[512,256]{1,0:T(8,128)(2,1)S(1)} %copy-done.10, bf16[512,256]{1,0:T(8,128)(2,1)S(1)} %copy-done.11, ...), custom_call_target="tpu_custom_call" | custom-call | flops 30000001024 | bytes 4000000 | tf_op jit(solution)/shard_map/mixer_local/pallas_call | solution.py:192
  36.6 0.8 copy-done.22
  37.3 0.7 copy-done.24
  38.1 0.0 all-to-all-done
  38.1 0.2 collective-permute-done.refs_5_
  38.2 1.5 %collective-permute-start.1 = (bf16[512,512]{1,0:T(8,128)(2,1)S(1)}, bf16[512,512]{1,0:T(8,128)(2,1)S(1)}, u32[]{:S(2)}, u32[]{:S(2)}) collective-permute-start(bf16[512,512]{1,0:T(8,128)(2,1)S(1)} %bitcast.26), channel_id=1, source_target_pairs={{0,2},{1,3},{2,0},{3,1},{4,6},{5,7},{6,4},{7,5},{8,10},{9,11},{10,... | collective-permute-start | bytes 1572872 | tf_op jit(solution)/shard_map/ppermute | solution.py:444
  39.8 0.0 collective-permute-start.2
  39.8 0.8 copy-done.3
  40.6 10.7 %collective-permute-done.1.refs_1_ = bf16[512,512]{1,0:T(8,128)(2,1)S(1)} collective-permute-done((bf16[512,512]{1,0:T(8,128)(2,1)S(1)}, bf16[512,512]{1,0:T(8,128)(2,1)S(1)}, u32[]{:S(2)}, u32[]{:S(2)}) %collective-permute-start.1) | collective-permute-done | bytes 524320 | tf_op jit(solution)/shard_map/ppermute | solution.py:444
  51.3 0.0 collective-permute-start.3
  51.3 0.0 collective-permute-done.2.refs_2_
  51.3 1.9 %collective-permute-done.3.refs_3_ = bf16[512,512]{1,0:T(8,128)(2,1)S(1)} collective-permute-done((bf16[512,512]{1,0:T(8,128)(2,1)S(1)}, bf16[512,512]{1,0:T(8,128)(2,1)S(1)}, u32[]{:S(2)}, u32[]{:S(2)}) %collective-permute-start.3) | collective-permute-done | bytes 524320 | tf_op jit(solution)/shard_map/ppermute | solution.py:444
  53.2 1.0 copy-done.4
  54.2 2.2 %copy-done.5 = bf16[1,2048,1024]{2,1,0:T(8,128)(2,1)S(1)} copy-done((bf16[1,2048,1024]{2,1,0:T(8,128)(2,1)S(1)}, bf16[1,2048,1024]{2,1,0:T(8,128)(2,1)}, u32[]{:S(2)}) %copy-start.5) | copy-done | bytes 4194328
  56.4 2.2 %copy-done.6 = bf16[1,2048,1024]{2,1,0:T(8,128)(2,1)S(1)} copy-done((bf16[1,2048,1024]{2,1,0:T(8,128)(2,1)S(1)}, bf16[1,2048,1024]{2,1,0:T(8,128)(2,1)}, u32[]{:S(2)}) %copy-start.6) | copy-done | bytes 4194328
  58.6 6.3 %hidden.1.h_ref = bf16[512,1024]{1,0:T(8,128)(2,1)S(1)} custom-call(s32[1]{0:T(128)} %bitcast.place_ref, bf16[512,512]{1,0:T(8,128)(2,1)S(1)} %bitcast.28, bf16[512,512]{1,0:T(8,128)(2,1)S(1)} %collective-permute-done.1.refs_1_, bf16[512,512]{1,0:T(8,128)(2,1)S(1)} %collective-permute-done.2.refs_2_, bf16[512,512]{1,0:T(8,128)(2,1)S(1)} %collective-permute-done.3.refs_3_, ...), custom_call_target="tpu_custom_call" | custom-call | flops 4294967296 | bytes 8388608 | tf_op jit(solution)/shard_map/hidden/pallas_call | solution.py:360
  64.9 2.5 %down.3 = bf16[2,512,512]{2,1,0:T(8,128)(2,1)} custom-call(s32[1]{0:T(128)} %bitcast.place_ref, bf16[512,1024]{1,0:T(8,128)(2,1)S(1)} %hidden.1.h_ref, bf16[1,1024,2048]{2,1,0:T(8,128)(2,1)S(1)} %copy-done), custom_call_target="tpu_custom_call" | custom-call | flops 1073741824 | bytes 2097152 | tf_op jit(solution)/shard_map/down/pallas_call | solution.py:391
  67.3 0.1 collective-permute-start.4
  67.5 0.8 broadcast_in_dim.2
  68.3 5.6 %all-to-all-start.1 = ((bf16[8,128,256]{2,1,0:T(8,128)(2,1)}), bf16[8,128,256]{2,1,0:T(8,128)(2,1)}, u32[]{:S(2)}, u32[]{:S(2)}) async-start(bf16[8,128,256]{2,1,0:T(8,128)(2,1)} %broadcast_in_dim.2), calls=%async_computation.1 | async-start | bytes 1048576 | tf_op jit(solution)/shard_map/all_to_all | solution.py:490
  73.9 0.1 collective-permute-start.9
  74.0 0.1 pad_add_fusion.place_ref
  74.1 0.4 collective-permute-start.10
  74.5 2.2 %copy-done.1 = bf16[1,1024,2048]{2,1,0:T(8,128)(2,1)S(1)} copy-done((bf16[1,1024,2048]{2,1,0:T(8,128)(2,1)S(1)}, bf16[1,1024,2048]{2,1,0:T(8,128)(2,1)}, u32[]{:S(2)}) %copy-start.1) | copy-done | bytes 4194328
  76.7 1.6 %down.2 = bf16[2,512,512]{2,1,0:T(8,128)(2,1)S(1)} custom-call(s32[1]{0:T(128)} %bitcast.place_ref, bf16[512,1024]{1,0:T(8,128)(2,1)S(1)} %hidden.1.h_ref, bf16[1,1024,2048]{2,1,0:T(8,128)(2,1)S(1)} %copy-done.1), custom_call_target="tpu_custom_call" | custom-call | flops 1073741824 | bytes 2097152 | tf_op jit(solution)/shard_map/down/pallas_call | solution.py:391
  78.3 0.0 copy-start.13
  78.3 0.0 copy-start.21
  78.3 0.0 copy-start.23
  78.4 0.0 copy-start.25
  78.4 0.0 collective-permute-done.4
  78.4 1.6 %fusion = bf16[1,2,512,512]{3,2,1,0:T(8,128)(2,1)S(1)} fusion(bf16[2,512,512]{2,1,0:T(8,128)(2,1)} %collective-permute-done.4, bf16[2,512,512]{2,1,0:T(8,128)(2,1)S(1)} %down.2), kind=kLoop, calls=%fused_computation.1 | loop fusion | flops 2097152 | bytes 3145728 | tf_op jit(solution)/shard_map/reshape | solution.py:509
  80.0 1.1 slice_bitcast_fusion
  81.0 0.8 collective-permute-start.5
  81.8 7.3 %all-to-all-done.1.ends_ref = bf16[8,128,256]{2,1,0:T(8,128)(2,1)} async-done(((bf16[8,128,256]{2,1,0:T(8,128)(2,1)}), bf16[8,128,256]{2,1,0:T(8,128)(2,1)}, u32[]{:S(2)}, u32[]{:S(2)}) %all-to-all-start.1) | async-done | bytes 524320 | tf_op jit(solution)/shard_map/all_to_all | solution.py:490
  89.0 0.0 copy-done.23
  89.1 3.1 %mixer_finish.1 = bf16[4,128,256]{2,1,0:T(8,128)(2,1)S(1)} custom-call(s32[2]{0:T(128)S(1)} %pad_add_fusion.place_ref, bf16[8,128,256]{2,1,0:T(8,128)(2,1)} %all-to-all-done.1.ends_ref, f32[512,256]{1,0:T(8,128)S(1)} %copy-done.23, bf16[512,256]{1,0:T(8,128)(2,1)S(1)} %copy-done.25, bf16[512,256]{1,0:T(8,128)(2,1)S(1)} %copy-done.13, f32[1,256]{1,0:T(1,128)S(1)} %bitcast.36), custom_call_target="tpu_custom_call" | custom-call | flops 4000000000 | bytes 2000000 | tf_op jit(solution)/shard_map/mixer_finish/pallas_call | solution.py:237
  92.2 0.8 collective-permute-start.6
  93.0 0.0 collective-permute-start.7
  93.0 0.0 collective-permute-done.9.refs_6_
  93.0 1.4 %collective-permute-start.8 = (bf16[128,256]{1,0:T(8,128)(2,1)S(1)}, bf16[128,256]{1,0:T(8,128)(2,1)S(1)}, u32[]{:S(2)}, u32[]{:S(2)}) collective-permute-start(bf16[128,256]{1,0:T(8,128)(2,1)S(1)} %get-tuple-element.26), channel_id=1, source_target_pairs={{0,3},{1,2},{2,1},{3,0},{4,7},{5,6},{6,5},{7,4},{8,11},{9,10},{10,... | collective-permute-start | bytes 196616 | tf_op jit(solution)/shard_map/ppermute | solution.py:444
  94.4 2.7 %collective-permute-done.6.refs_1_ = bf16[128,256]{1,0:T(8,128)(2,1)S(1)} collective-permute-done((bf16[128,256]{1,0:T(8,128)(2,1)S(1)}, bf16[128,256]{1,0:T(8,128)(2,1)S(1)}, u32[]{:S(2)}, u32[]{:S(2)}) %collective-permute-start.6) | collective-permute-done | bytes 65568 | tf_op jit(solution)/shard_map/ppermute | solution.py:444
  97.1 0.0 collective-permute-done.7.refs_2_
  97.1 0.3 collective-permute-done.8.refs_3_
  97.4 0.0 collective-permute-done.10.refs_7_
  97.4 4.1 %project.1 = bf16[128,2048]{1,0:T(8,128)(2,1)} custom-call(bf16[128,256]{1,0:T(8,128)(2,1)S(1)} %get-tuple-element.29.refs_0_, bf16[128,256]{1,0:T(8,128)(2,1)S(1)} %collective-permute-done.6.refs_1_, bf16[128,256]{1,0:T(8,128)(2,1)S(1)} %collective-permute-done.7.refs_2_, bf16[128,256]{1,0:T(8,128)(2,1)S(1)} %collective-permute-done.8.refs_3_, ...), custom_call_target="tpu_custom_call" | custom-call | flops 536870912 | bytes 4194304 | tf_op jit(solution)/shard_map/project/pallas_call | solution.py:426
  101.5 0.0 collective-permute-done.5
  101.5 1.2 add_convert_fusion.1
  102.7 20.7 %all_to_all.15.refs_0_ = bf16[8,64,512]{2,1,0:T(8,128)(2,1)S(1)} all-to-all(bf16[8,64,512]{2,1,0:T(8,128)(2,1)S(1)} %bitcast.37), channel_id=1, replica_groups=mesh['ep'=8,'tp'=4] {'ep'}, dimensions={0} | all-to-all | bytes 1048576 | tf_op jit(solution)/shard_map/all_to_all | solution.py:522
  123.5 1.1 combine.1
  (31 shorter events, 0.1 us)
Async XLA Ops:
  0.6 1.0 copy-start.7
  1.7 0.8 copy-start.14
  2.4 0.7 copy-start.15
  3.2 0.7 copy-start.16
  3.9 0.7 copy-start.18
  4.5 9.0 %copy-start.2 = (bf16[256,2048]{1,0:T(8,128)(2,1)S(1)}, bf16[256,2048]{1,0:T(8,128)(2,1)}, u32[]{:S(2)}) copy-start(bf16[256,2048]{1,0:T(8,128)(2,1)} %refs_4_.3) | copy-start | bytes 3145732
  4.5 10.6 %copy-start.8 = (bf16[512,256]{1,0:T(8,128)(2,1)S(1)}, bf16[512,256]{1,0:T(8,128)(2,1)}, u32[]{:S(2)}) copy-start(bf16[512,256]{1,0:T(8,128)(2,1)} %q_ref.1) | copy-start | bytes 786436
  4.5 10.6 %copy-start.9 = (bf16[512,256]{1,0:T(8,128)(2,1)S(1)}, bf16[512,256]{1,0:T(8,128)(2,1)}, u32[]{:S(2)}) copy-start(bf16[512,256]{1,0:T(8,128)(2,1)} %k_ref.1) | copy-start | bytes 786436
  4.5 10.6 %copy-start.10 = (bf16[512,256]{1,0:T(8,128)(2,1)S(1)}, bf16[512,256]{1,0:T(8,128)(2,1)}, u32[]{:S(2)}) copy-start(bf16[512,256]{1,0:T(8,128)(2,1)} %v_ref.1) | copy-start | bytes 786436
  4.5 10.6 %copy-start.17 = (f32[512,4]{0,1:T(4,128)S(1)}, f32[512,4]{0,1:T(4,128)}, u32[]{:S(2)}) copy-start(f32[512,4]{0,1:T(4,128)} %param.27) | copy-start | bytes 24580
  4.6 10.6 %copy-start.19 = (f32[256]{0:T(256)S(1)}, f32[256]{0:T(256)}, u32[]{:S(2)}) copy-start(f32[256]{0:T(256)} %param.25) | copy-start | bytes 3076
  4.6 10.6 %copy-start.20 = (f32[256]{0:T(256)S(1)}, f32[256]{0:T(256)}, u32[]{:S(2)}) copy-start(f32[256]{0:T(256)} %param.26) | copy-start | bytes 3076
  6.3 31.8 %all-to-all-start = ((bf16[8,64,512]{2,1,0:T(8,128)(2,1)}), bf16[8,64,512]{2,1,0:T(8,128)(2,1)S(1)}, u32[]{:S(2)}, u32[]{:S(2)}) async-start(bf16[8,64,512]{2,1,0:T(8,128)(2,1)} %get-tuple-element.13), calls=%async_computation | async-start | bytes 1048576 | tf_op jit(solution)/shard_map/all_to_all | solution.py:479
  13.6 24.7 %collective-permute-start = (bf16[256,2048]{1,0:T(8,128)(2,1)S(1)}, bf16[256,2048]{1,0:T(8,128)(2,1)S(1)}, u32[]{:S(2)}, u32[]{:S(2)}) collective-permute-start(bf16[256,2048]{1,0:T(8,128)(2,1)S(1)} %copy-done.2), channel_id=1, source_target_pairs={{0,2},{1,3},{2,0},{3,1},{4,6},{5,7},{6,4},{7,5},{8,10},{9,11},{10,... | collective-permute-start | bytes 3145736 | tf_op jit(solution)/shard_map/ppermute | solution.py:444
  15.2 1.0 copy-start.11
  16.1 0.9 copy-start.12
  36.5 0.8 copy-start.22
  37.3 0.7 copy-start.24
  38.2 26.6 %copy-start = (bf16[1,1024,2048]{2,1,0:T(8,128)(2,1)S(1)}, bf16[1,1024,2048]{2,1,0:T(8,128)(2,1)}, u32[]{:S(2)}) copy-start(bf16[1,1024,2048]{2,1,0:T(8,128)(2,1)} %w_ref.5) | copy-start | bytes 12582916
  38.2 13.0 %collective-permute-start.1 = (bf16[512,512]{1,0:T(8,128)(2,1)S(1)}, bf16[512,512]{1,0:T(8,128)(2,1)S(1)}, u32[]{:S(2)}, u32[]{:S(2)}) collective-permute-start(bf16[512,512]{1,0:T(8,128)(2,1)S(1)} %bitcast.26), channel_id=1, source_target_pairs={{0,2},{1,3},{2,0},{3,1},{4,6},{5,7},{6,4},{7,5},{8,10},{9,11},{10,... | collective-permute-start | bytes 1572872 | tf_op jit(solution)/shard_map/ppermute | solution.py:444
  39.8 11.5 %collective-permute-start.2 = (bf16[512,512]{1,0:T(8,128)(2,1)S(1)}, bf16[512,512]{1,0:T(8,128)(2,1)S(1)}, u32[]{:S(2)}, u32[]{:S(2)}) collective-permute-start(bf16[512,512]{1,0:T(8,128)(2,1)S(1)} %bitcast.27), channel_id=1, source_target_pairs={{0,1},{1,0},{2,3},{3,2},{4,5},{5,4},{6,7},{7,6},{8,9},{9,8},{10,11... | collective-permute-start | bytes 1572872 | tf_op jit(solution)/shard_map/ppermute | solution.py:444
  39.8 0.8 copy-start.3
  51.3 1.9 %collective-permute-start.3 = (bf16[512,512]{1,0:T(8,128)(2,1)S(1)}, bf16[512,512]{1,0:T(8,128)(2,1)S(1)}, u32[]{:S(2)}, u32[]{:S(2)}) collective-permute-start(bf16[512,512]{1,0:T(8,128)(2,1)S(1)} %collective-permute-done.1.refs_1_), channel_id=1, source_target_pairs={{0,1},{1,0},{2,3},{3,2},{4,5},{5,4},{6,7},{7,6},{8,9},{9,8},{10,11... | collective-permute-start | bytes 1572872 | tf_op jit(solution)/shard_map/ppermute | solution.py:444
  53.2 1.0 copy-start.4
  54.2 2.2 %copy-start.5 = (bf16[1,2048,1024]{2,1,0:T(8,128)(2,1)S(1)}, bf16[1,2048,1024]{2,1,0:T(8,128)(2,1)}, u32[]{:S(2)}) copy-start(bf16[1,2048,1024]{2,1,0:T(8,128)(2,1)} %refs_4_.2) | copy-start | bytes 12582916
  56.4 2.2 %copy-start.6 = (bf16[1,2048,1024]{2,1,0:T(8,128)(2,1)S(1)}, bf16[1,2048,1024]{2,1,0:T(8,128)(2,1)}, u32[]{:S(2)}) copy-start(bf16[1,2048,1024]{2,1,0:T(8,128)(2,1)} %refs_5_.1) | copy-start | bytes 12582916
  67.3 11.0 %collective-permute-start.4 = (bf16[2,512,512]{2,1,0:T(8,128)(2,1)}, bf16[2,512,512]{2,1,0:T(8,128)(2,1)}, u32[]{:S(2)}, u32[]{:S(2)}) collective-permute-start(bf16[2,512,512]{2,1,0:T(8,128)(2,1)} %down.3), channel_id=1, source_target_pairs={{0,1},{1,0},{2,3},{3,2},{4,5},{5,4},{6,7},{7,6},{8,9},{9,8},{10,11... | collective-permute-start | bytes 3145736 | tf_op jit(solution)/shard_map/ppermute | solution.py:444
  68.3 20.7 %all-to-all-start.1 = ((bf16[8,128,256]{2,1,0:T(8,128)(2,1)}), bf16[8,128,256]{2,1,0:T(8,128)(2,1)}, u32[]{:S(2)}, u32[]{:S(2)}) async-start(bf16[8,128,256]{2,1,0:T(8,128)(2,1)} %broadcast_in_dim.2), calls=%async_computation.1 | async-start | bytes 1048576 | tf_op jit(solution)/shard_map/all_to_all | solution.py:490
  73.9 19.1 %collective-permute-start.9 = (bf16[256,2048]{1,0:T(8,128)(2,1)S(1)}, bf16[256,2048]{1,0:T(8,128)(2,1)}, u32[]{:S(2)}, u32[]{:S(2)}) collective-permute-start(bf16[256,2048]{1,0:T(8,128)(2,1)S(1)} %copy-done.2), channel_id=1, source_target_pairs={{0,1},{1,0},{2,3},{3,2},{4,5},{5,4},{6,7},{7,6},{8,9},{9,8},{10,11... | collective-permute-start | bytes 3145736 | tf_op jit(solution)/shard_map/ppermute | solution.py:444
  74.1 23.3 %collective-permute-start.10 = (bf16[256,2048]{1,0:T(8,128)(2,1)S(1)}, bf16[256,2048]{1,0:T(8,128)(2,1)}, u32[]{:S(2)}, u32[]{:S(2)}) collective-permute-start(bf16[256,2048]{1,0:T(8,128)(2,1)S(1)} %collective-permute-done.refs_5_), channel_id=1, source_target_pairs={{0,1},{1,0},{2,3},{3,2},{4,5},{5,4},{6,7},{7,6},{8,9},{9,8},{10,11... | collective-permute-start | bytes 3145736 | tf_op jit(solution)/shard_map/ppermute | solution.py:444
  74.5 2.2 %copy-start.1 = (bf16[1,1024,2048]{2,1,0:T(8,128)(2,1)S(1)}, bf16[1,1024,2048]{2,1,0:T(8,128)(2,1)}, u32[]{:S(2)}) copy-start(bf16[1,1024,2048]{2,1,0:T(8,128)(2,1)} %w_ref.5) | copy-start | bytes 12582916
  78.3 10.7 %copy-start.13 = (bf16[512,256]{1,0:T(8,128)(2,1)S(1)}, bf16[512,256]{1,0:T(8,128)(2,1)}, u32[]{:S(2)}) copy-start(bf16[512,256]{1,0:T(8,128)(2,1)} %gate_ref.1) | copy-start | bytes 786436
  78.3 10.7 %copy-start.21 = (f32[256]{0:T(256)S(1)}, f32[256]{0:T(256)}, u32[]{:S(2)}) copy-start(f32[256]{0:T(256)} %param.28) | copy-start | bytes 3076
  78.3 10.7 %copy-start.23 = (f32[512,256]{1,0:T(8,128)S(1)}, f32[512,256]{1,0:T(8,128)}, u32[]{:S(2)}) copy-start(f32[512,256]{1,0:T(8,128)} %copy-done.22) | copy-start | bytes 1572868
  78.4 10.7 %copy-start.25 = (bf16[512,256]{1,0:T(8,128)(2,1)S(1)}, bf16[512,256]{1,0:T(8,128)(2,1)}, u32[]{:S(2)}) copy-start(bf16[512,256]{1,0:T(8,128)(2,1)} %copy-done.24) | copy-start | bytes 786436
  81.0 20.5 %collective-permute-start.5 = (bf16[1,512,512]{2,1,0:T(8,128)(2,1)}, bf16[1,512,512]{2,1,0:T(8,128)(2,1)}, u32[]{:S(2)}, u32[]{:S(2)}) collective-permute-start(bf16[1,512,512]{2,1,0:T(8,128)(2,1)} %get-tuple-element.24), channel_id=1, source_target_pairs={{0,2},{1,3},{2,0},{3,1},{4,6},{5,7},{6,4},{7,5},{8,10},{9,11},{10,... | collective-permute-start | bytes 1572872 | tf_op jit(solution)/shard_map/ppermute | solution.py:444
  92.1 9.4 %copy-start.26 = (bf16[1,512,512]{2,1,0:T(8,128)(2,1)S(1)}, bf16[1,512,512]{2,1,0:T(8,128)(2,1)}, u32[]{:S(2)}) copy-start(bf16[1,512,512]{2,1,0:T(8,128)(2,1)} %get-tuple-element.22) | copy-start | bytes 1572868
  92.2 4.9 %collective-permute-start.6 = (bf16[128,256]{1,0:T(8,128)(2,1)S(1)}, bf16[128,256]{1,0:T(8,128)(2,1)S(1)}, u32[]{:S(2)}, u32[]{:S(2)}) collective-permute-start(bf16[128,256]{1,0:T(8,128)(2,1)S(1)} %get-tuple-element.28), channel_id=1, source_target_pairs={{0,2},{1,3},{2,0},{3,1},{4,6},{5,7},{6,4},{7,5},{8,10},{9,11},{10,... | collective-permute-start | bytes 196616 | tf_op jit(solution)/shard_map/ppermute | solution.py:444
  93.0 4.1 %collective-permute-start.7 = (bf16[128,256]{1,0:T(8,128)(2,1)S(1)}, bf16[128,256]{1,0:T(8,128)(2,1)S(1)}, u32[]{:S(2)}, u32[]{:S(2)}) collective-permute-start(bf16[128,256]{1,0:T(8,128)(2,1)S(1)} %get-tuple-element.27), channel_id=1, source_target_pairs={{0,1},{1,0},{2,3},{3,2},{4,5},{5,4},{6,7},{7,6},{8,9},{9,8},{10,11... | collective-permute-start | bytes 196616 | tf_op jit(solution)/shard_map/ppermute | solution.py:444
  93.0 4.4 %collective-permute-start.8 = (bf16[128,256]{1,0:T(8,128)(2,1)S(1)}, bf16[128,256]{1,0:T(8,128)(2,1)S(1)}, u32[]{:S(2)}, u32[]{:S(2)}) collective-permute-start(bf16[128,256]{1,0:T(8,128)(2,1)S(1)} %get-tuple-element.26), channel_id=1, source_target_pairs={{0,3},{1,2},{2,1},{3,0},{4,7},{5,6},{6,5},{7,4},{8,11},{9,10},{10,... | collective-permute-start | bytes 196616 | tf_op jit(solution)/shard_map/ppermute | solution.py:444

commit v2 on v1

--- a/solution.py
+++ b/solution.py
@@ -8,7 +8,7 @@
 
 HEAD_DIM = 64
 GROUPS = 4
-PARTS = 1
+VMEM_LIMIT = 16 * 1024 * 1024
 key_eps = 1e-06
 group_eps = 0.00064
 norm_eps = 1e-06
@@ -18,6 +18,10 @@
 NN = (((1,), (0,)), ((), ()))
 NT = (((1,), (1,)), ((), ()))
 TN = (((0,), (0,)), ((), ()))
+
+
+def hbm(*arrays):
+    return [pltpu.with_memory_space_constraint(a, pltpu.HBM) for a in arrays]
 
 
 def mm(a, b, dims=NN):
@@ -63,10 +67,14 @@
 
 
 def mixer_kernel(
-    q_ref, k_ref, v_ref, w_ref, a_ref, wo_ref, ao_ref, ex_ref,
-    local_ref, reach_ref, end_ref,
-    u_s, r_s, c_s, ld_s, pair_s, diag_s, tri_s, ue_s, qe_s, kh_s, rh_s, up_s, qp_s, g_s, et_s,
+    first_part, last_part, q_ref, k_ref, v_ref, w_ref, a_ref, wo_ref, ao_ref, ex_ref, *refs
 ):
+    refs = list(refs)
+    start_ref = None if first_part else refs.pop(0)
+    local_ref, reach_ref, end_ref = refs[:3]
+    (
+        u_s, r_s, ld_s, pair_s, diag_s, tri_s, ue_s, qe_s, kh_s, rh_s, up_s, qp_s, g_s, et_s,
+    ) = refs[3:]
     rows, lanes = q_ref.shape
     C = HEAD_DIM
     chunks = rows // C
@@ -124,15 +132,27 @@
         )
         return 0
 
-    lax.fori_loop(0, chunks, first, 0, unroll=2)
-
-    dparts = thirds(diag_s[...].reshape(chunks * BASE, lanes))
+    lax.fori_loop(0, chunks, first, 0, unroll=4)
+
+    dall = diag_s[...].reshape(chunks * BASE, lanes)
+    dparts = thirds(dall)
     t = jnp.where(
         iota((chunks, BASE, lanes), 1) == iota((chunks, BASE, lanes), 2) % BASE, 1.0, 0.0
     ).astype(f32)
     for j in range(BASE - 1):
-        pick = jnp.logical_and(base_mask, rr % BASE == j).astype(bf16)
-        col = sum(mm(p, pick) for p in dparts).reshape(chunks, BASE, lanes)
+        if lanes % 128:
+            pick = jnp.logical_and(base_mask, rr % BASE == j).astype(bf16)
+            col = sum(mm(p, pick) for p in dparts)
+        else:
+            near = iota((chunks * BASE, 128), 1) // BASE * BASE + j
+            col = jnp.concatenate(
+                [
+                    jnp.take_along_axis(dall[:, p : p + 128], near, axis=1, mode="promise_in_bounds")
+                    for p in range(0, lanes, 128)
+                ],
+                axis=1,
+            )
+        col = col.reshape(chunks, BASE, lanes)
         t = t - col * t[:, j : j + 1, :]
     tri_s[...] = t
 
@@ -166,7 +186,7 @@
         g_s[i] = mm(vt, spread(kh_s[at, :], hm)) - mm(zat, spread(rh_s[at, :], hm))
         return 0
 
-    lax.fori_loop(0, chunks, second, 0, unroll=2)
+    lax.fori_loop(0, chunks, second, 0, unroll=4)
 
     def third(i, x):
         at = pl.ds(pl.multiple_of(i * C, C), C)
@@ -180,40 +200,65 @@
         g = g_s[i]
         return x * et_s[pl.ds(i, 1), :] + jnp.concatenate([g, jnp.zeros_like(g)], axis=0) - corr
 
-    x0 = jnp.concatenate([jnp.zeros((HEAD_DIM, lanes), f32), pickv.astype(f32)], axis=0)
-    x = lax.fori_loop(0, chunks, third, x0, unroll=2)
-    end_ref[...] = x.astype(bf16)
-
-
-def mixer_local(q, k, v, w, a, wo, ao, ex):
+    if first_part:
+        x0 = jnp.concatenate([jnp.zeros((HEAD_DIM, lanes), f32), pickv.astype(f32)], axis=0)
+    else:
+        x0 = start_ref[...]
+    x = lax.fori_loop(0, chunks, third, x0, unroll=4)
+    if last_part:
+        end_ref[...] = jnp.broadcast_to(x.astype(bf16)[None], end_ref.shape)
+    else:
+        end_ref[...] = x
+
+
+def mixer_local(part, parts, copies, start, q, k, v, w, a, wo, ao, ex):
     rows, lanes = q.shape
+    rows //= parts
     chunks = rows // HEAD_DIM
+    heads = ex.shape[0]
     V = pltpu.VMEM
-    return pl.pallas_call(
-        mixer_kernel,
-        out_shape=(
-            jax.ShapeDtypeStruct((rows, lanes), f32),
-            jax.ShapeDtypeStruct((rows, lanes), bf16),
-            jax.ShapeDtypeStruct((2 * HEAD_DIM, lanes), bf16),
-        ),
+    block = pl.BlockSpec((rows, lanes), lambda i: (part, 0))
+    vector = pl.BlockSpec((1, lanes), lambda i: (0, 0))
+    state = pl.BlockSpec((2 * HEAD_DIM, lanes), lambda i: (0, 0))
+    out = pl.BlockSpec((rows, lanes), lambda i: (0, 0))
+    last = part == parts - 1
+    ends = (copies, 2 * HEAD_DIM, lanes)
+    return pl.pallas_call(
+        functools.partial(mixer_kernel, part == 0, last),
+        grid=(1,),
+        in_specs=[block] * 5
+        + [vector] * 2
+        + [pl.BlockSpec((heads, rows), lambda i: (0, part))]
+        + ([] if start is None else [state]),
+        out_specs=[out, out, pl.BlockSpec(ends, lambda i: (0, 0, 0)) if last else state],
+        out_shape=[
+            pltpu.HBM((rows, lanes), f32),
+            pltpu.HBM((rows, lanes), bf16),
+            pltpu.HBM(ends, bf16) if last else jax.ShapeDtypeStruct(ends[1:], f32),
+        ],
         scratch_shapes=[
-            V((rows, lanes), f32), V((rows, lanes), f32), V((8, 128), f32), V((rows, lanes), f32),
+            V((rows, lanes), f32), V((rows, lanes), f32), V((rows, lanes), f32),
             V((chunks, 4, lanes, lanes), bf16), V((chunks, BASE, lanes), f32), V((chunks, BASE, lanes), f32),
             V((rows, lanes), bf16), V((rows, lanes), f32), V((rows, lanes), bf16), V((rows, lanes), bf16),
             V((chunks, lanes, lanes), bf16), V((rows, lanes), bf16), V((chunks, HEAD_DIM, lanes), f32),
             V((chunks, lanes), f32),
         ],
-        compiler_params=pltpu.CompilerParams(vmem_limit_bytes=40 * 1024 * 1024),
-        cost_estimate=pl.CostEstimate(flops=30_000_000_000, bytes_accessed=4_000_000, transcendentals=0),
+        compiler_params=pltpu.CompilerParams(vmem_limit_bytes=VMEM_LIMIT),
+        cost_estimate=pl.CostEstimate(flops=10_000_000_000, bytes_accessed=2_000_000, transcendentals=0),
         name="mixer_local",
-    )(q, k, v, w, a, wo.reshape(1, -1), ao.reshape(1, -1), ex)
-
-
-def finish_kernel(place_ref, ends_ref, local_ref, reach_ref, gate_ref, gain_ref, out_ref, mixed_s):
+    )(
+        *hbm(q, k, v, w, a, wo.reshape(1, -1), ao.reshape(1, -1), ex),
+        *([] if start is None else [start]),
+    )
+
+
+def finish_kernel(place_ref, ends_ref, gate_ref, gain_ref, *refs):
+    out_ref, mixed_s = refs[-2:]
+    parts = (len(refs) - 2) // 2
     devices, _, lanes = ends_ref.shape
     hm = head_mask(lanes)
     ones_bd = hm.astype(bf16)
-    place = place_ref[0]
+    place = place_ref[1]
 
     def hop(e, s):
         pbd = spread(ends_ref[e, HEAD_DIM:, :], hm)
@@ -221,34 +266,47 @@
         return jnp.where(e < place, new, s)
 
     s = lax.fori_loop(0, devices - 1, hop, jnp.zeros((HEAD_DIM, lanes), f32), unroll=True)
-    head_out = local_ref[...] + mm(reach_ref[...], spread(s.astype(bf16), hm), NT)
-    centred = head_out - exact_right(head_out, ones_bd, halves) * (1.0 / HEAD_DIM)
-    var = exact_right(centred * centred, ones_bd, halves) * (1.0 / HEAD_DIM)
-    gate = jax.nn.sigmoid(gate_ref[...].astype(f32))
-    mixed_s[...] = centred * lax.rsqrt(var + group_eps) * gain_ref[...] * gate
+    sbd = spread(s.astype(bf16), hm)
+    gain = gain_ref[...]
+    for j, (local_ref, reach_ref) in enumerate(zip(refs[:parts], refs[parts : 2 * parts])):
+        rows = local_ref.shape[0]
+        at = pl.ds(j * rows, rows)
+        head_out = local_ref[...] + mm(reach_ref[...], sbd, NT)
+        centred = head_out - exact_right(head_out, ones_bd, halves) * (1.0 / HEAD_DIM)
+        var = exact_right(centred * centred, ones_bd, halves) * (1.0 / HEAD_DIM)
+        gate = jax.nn.sigmoid(gate_ref[at, :].astype(f32))
+        mixed_s[at, :] = centred * lax.rsqrt(var + group_eps) * gain * gate
     count, rows, _ = out_ref.shape
     for m in range(count):
-        at = pl.multiple_of(lax.bitwise_xor(place_ref[1], m) * rows, rows)
+        at = pl.multiple_of(lax.bitwise_xor(place_ref[0], m) * rows, rows)
         out_ref[m] = mixed_s[pl.ds(at, rows), :].astype(bf16)
 
 
-def mixer_finish(place, ends, local, reach, gate, gain, count):
-    vm = pl.BlockSpec(memory_space=pltpu.VMEM)
+def whole(shape):
+    return pl.BlockSpec(shape, lambda i: (0,) * len(shape))
+
+
+def mixer_finish(place, ends, gate, gain, local, reach, count):
+    rows, lanes = gate.shape
+    gain = gain.reshape(1, -1)
+    out = (count, rows // count, lanes)
     return pl.pallas_call(
         finish_kernel,
-        out_shape=jax.ShapeDtypeStruct((count, local.shape[0] // count, local.shape[1]), bf16),
-        in_specs=[pl.BlockSpec(memory_space=pltpu.SMEM)] + [vm] * 5,
-        out_specs=vm,
-        scratch_shapes=[pltpu.VMEM(local.shape, f32)],
-        compiler_params=pltpu.CompilerParams(vmem_limit_bytes=24 * 1024 * 1024),
+        grid=(1,),
+        out_shape=jax.ShapeDtypeStruct(out, bf16),
+        in_specs=[pl.BlockSpec(memory_space=pltpu.SMEM)]
+        + [whole(x.shape) for x in (ends, gate, gain, *local, *reach)],
+        out_specs=whole(out),
+        scratch_shapes=[pltpu.VMEM(gate.shape, f32)],
+        compiler_params=pltpu.CompilerParams(vmem_limit_bytes=VMEM_LIMIT),
         cost_estimate=pl.CostEstimate(flops=4_000_000_000, bytes_accessed=2_000_000, transcendentals=0),
         name="mixer_finish",
-    )(place, ends, local, reach, gate, gain.reshape(1, -1))
+    )(place, *hbm(ends, gate, gain, *local, *reach))
 
 
 def route_kernel(place_ref, x_ref, gain_ref, gw_ref, ew_ref, routes_ref, *outs):
     send_refs, info_ref = outs[:-1], outs[-1]
-    tokens, width = x_ref.shape
+    tokens, _ = x_ref.shape
     experts, part, share = send_refs[0].shape
     per_group = experts // GROUPS
     x = x_ref[...].astype(f32)
@@ -293,92 +351,187 @@
 
 def route(place, x, gain, gw, ew, routes, parts, part, share):
     experts, tokens = ew.shape[0], x.shape[0]
-    vm = pl.BlockSpec(memory_space=pltpu.VMEM)
+    gain = gain.reshape(1, -1)
     return pl.pallas_call(
         route_kernel,
-        out_shape=[jax.ShapeDtypeStruct((experts, part, share), bf16)] * parts
-        + [jax.ShapeDtypeStruct((tokens, 8), f32)],
-        in_specs=[pl.BlockSpec(memory_space=pltpu.SMEM)] + [vm] * 5,
-        out_specs=[vm] * (parts + 1),
-        compiler_params=pltpu.CompilerParams(vmem_limit_bytes=24 * 1024 * 1024),
+        grid=(1,),
+        out_shape=[pltpu.HBM((experts, part, share), bf16)] * parts + [pltpu.HBM((tokens, 8), f32)],
+        in_specs=[pl.BlockSpec(memory_space=pltpu.SMEM)]
+        + [whole(a.shape) for a in (x, gain, gw, ew, routes)],
+        out_specs=[whole((experts, part, share))] * parts + [whole((tokens, 8))],
+        compiler_params=pltpu.CompilerParams(vmem_limit_bytes=VMEM_LIMIT),
         cost_estimate=pl.CostEstimate(flops=4_000_000_000, bytes_accessed=1_000_000, transcendentals=0),
         name="route",
-    )(place, x, gain.reshape(1, -1), gw, ew, routes)
-
-
-def combine_kernel(info_ref, *refs, top):
-    homes, out_ref = refs[:-1], refs[-1]
+    )(place, *hbm(x, gain, gw, ew, routes))
+
+
+def combine_kernel(place_ref, info_ref, *refs, top):
+    homes, out_ref, home_s = refs[:-2], refs[-2], refs[-1]
     tokens = info_ref.shape[0]
-    experts, part, share = homes[0].shape
-    slots = iota((tokens, experts * part), 1)
+    part, share = homes[0].shape
+    for j, home in enumerate(homes):
+        home_s[j * part : (j + 1) * part, :] = home[...]
+    home = home_s[...]
+    slots = iota((tokens, home.shape[0]), 1)
     total = jnp.zeros((tokens, share), f32)
     for k in range(top):
         p = info_ref[:, top + k : top + k + 1].astype(jnp.int32)
         i = info_ref[:, 2 * top + k : 2 * top + k + 1].astype(jnp.int32)
-        rows = jnp.zeros((tokens, share), f32)
-        for j, home in enumerate(homes):
-            inside = jnp.logical_and(p >= j * part, p < (j + 1) * part)
-            h = jnp.logical_and(slots == i * part + p - j * part, inside)
-            rows += mm(h.astype(bf16), home[...].reshape(experts * part, share))
-        total += info_ref[:, k : k + 1] * rows
+        hit = slots == lax.bitwise_xor(i, place_ref[1]) * part + p
+        total += info_ref[:, k : k + 1] * mm(hit.astype(bf16), home)
     out_ref[...] = total.astype(bf16)
 
 
-def combine(info, homes, top):
+def combine(place, info, homes, top):
+    part, share = homes[0].shape
+    out = (info.shape[0], share)
     vm = pl.BlockSpec(memory_space=pltpu.VMEM)
     return pl.pallas_call(
         functools.partial(combine_kernel, top=top),
-        out_shape=jax.ShapeDtypeStruct((info.shape[0], homes[0].shape[2]), bf16),
-        in_specs=[vm] * (1 + len(homes)),
+        out_shape=jax.ShapeDtypeStruct(out, bf16),
+        in_specs=[pl.BlockSpec(memory_space=pltpu.SMEM)] + [vm] * (1 + len(homes)),
         out_specs=vm,
-        compiler_params=pltpu.CompilerParams(vmem_limit_bytes=24 * 1024 * 1024),
+        scratch_shapes=[pltpu.VMEM((part * len(homes), share), bf16)],
+        compiler_params=pltpu.CompilerParams(vmem_limit_bytes=VMEM_LIMIT),
         cost_estimate=pl.CostEstimate(flops=1_000_000_000, bytes_accessed=1_000_000, transcendentals=0),
         name="combine",
-    )(info, *homes)
+    )(place, info, *homes)
+
+
+def merge_kernel(keep_ref, got_ref, *outs, offset):
+    part = outs[0].shape[0]
+    for j, out_ref in enumerate(outs):
+        at = j * part
+        total = keep_ref[0, offset + at : offset + at + part, :].astype(f32)
+        total += got_ref[0, at : at + part, :].astype(f32)
+        out_ref[...] = total.astype(bf16)
+
+
+def merge(keep, got, offset, part):
+    _, rows, share = got.shape
+    vm = pl.BlockSpec(memory_space=pltpu.VMEM)
+    return pl.pallas_call(
+        functools.partial(merge_kernel, offset=offset),
+        out_shape=[jax.ShapeDtypeStruct((part, share), bf16)] * (rows // part),
+        in_specs=[vm] * 2,
+        out_specs=[vm] * (rows // part),
+        compiler_params=pltpu.CompilerParams(vmem_limit_bytes=VMEM_LIMIT),
+        cost_estimate=pl.CostEstimate(flops=100_000_000, bytes_accessed=1_000_000, transcendentals=0),
+        name="merge",
+    )(keep, got)
+
+
+def split_kernel(keep_ref, got_ref, keep_out, *outs):
+    blocks, rows, _ = keep_out.shape
+    half = rows // len(outs)
+    for j in range(blocks):
+        mine = keep_ref[2 * j].astype(f32) + got_ref[2 * j].astype(f32)
+        keep_out[j] = mine.astype(bf16)
+        away = (keep_ref[2 * j + 1].astype(f32) + got_ref[2 * j + 1].astype(f32)).astype(bf16)
+        for n, out_ref in enumerate(outs):
+            out_ref[j] = away[n * half : (n + 1) * half]
+
+
+def split(keep, got, pieces):
+    blocks, rows, share = keep.shape
+    vm = pl.BlockSpec(memory_space=pltpu.VMEM)
+    return pl.pallas_call(
+        split_kernel,
+        out_shape=[jax.ShapeDtypeStruct((blocks // 2, rows, share), bf16)]
+        + [jax.ShapeDtypeStruct((blocks // 2, rows // pieces, share), bf16)] * pieces,
+        in_specs=[vm] * 2,
+        out_specs=[vm] * (1 + pieces),
+        compiler_params=pltpu.CompilerParams(vmem_limit_bytes=VMEM_LIMIT),
+        cost_estimate=pl.CostEstimate(flops=100_000_000, bytes_accessed=1_000_000, transcendentals=0),
+        name="split",
+    )(keep, got)
 
 
 def tile_of(size, most):
     return most if size % most == 0 else size
 
 
-def hidden_kernel(place_ref, *refs, masks):
-    xs, (wg_ref, wu_ref, out_ref) = refs[: len(masks)], refs[len(masks) :]
-    share = xs[0].shape[1]
-    gate = up = None
-    for m, x in zip(masks, xs):
-        at = pl.ds(pl.multiple_of(lax.bitwise_xor(place_ref[0], m) * share, share), share)
-        g, u = mm(x[...], wg_ref[0, at, :]), mm(x[...], wu_ref[0, at, :])
-        gate, up = (g, u) if gate is None else (gate + g, up + u)
-    out_ref[...] = (gate * jax.nn.sigmoid(gate) * up).astype(bf16)
-
-
-def hidden(place, masks, xs, wg, wu):
+def experts_kernel(place_ref, *refs, masks, sends, sources):
+    count = len(masks)
+    xs = refs[:count]
+    wg_hbm, wu_hbm, wd_hbm, h_ref, send_ref, wg, wu, wd, gate_sem, down_sem = refs[count:]
+    rows, share = xs[0].shape
+    tiles, _, _, tile = wg.shape
+
+    def rows_of(m):
+        return pl.ds(pl.multiple_of(lax.bitwise_xor(place_ref[0], m) * share, share), share)
+
+    loads = {}
+    for f in range(tiles):
+        for n, m in enumerate(masks):
+            columns = pl.ds(f * tile, tile)
+            loads[f, n] = [
+                pltpu.make_async_copy(
+                    src.at[0, rows_of(m), columns], dst.at[f, n], gate_sem.at[i, f, n]
+                )
+                for i, (src, dst) in enumerate(((wg_hbm, wg), (wu_hbm, wu)))
+            ]
+            for load in loads[f, n]:
+                load.start()
+    downs = [
+        pltpu.make_async_copy(wd_hbm.at[0, :, rows_of(m)], wd.at[n], down_sem.at[n])
+        for n, m in enumerate(sends)
+    ]
+    for load in downs:
+        load.start()
+    for f in range(tiles):
+        gate = up = None
+        for n, x in enumerate(xs):
+            for load in loads[f, n]:
+                load.wait()
+            x = x[...]
+            g, u = mm(x, wg[f, n]), mm(x, wu[f, n])
+            gate, up = (g, u) if gate is None else (gate + g, up + u)
+        h = (gate * jax.nn.sigmoid(gate) * up).astype(bf16)
+        part = rows // sources
+        for s in range(sources):
+            at = pl.multiple_of(lax.bitwise_xor(place_ref[1], s) * part, part)
+            h_ref[pl.ds(at, part), f * tile : (f + 1) * tile] = h[s * part : (s + 1) * part]
+    h = h_ref[...]
+    for n, load in enumerate(downs):
+        load.wait()
+        send_ref[n] = mm(h, wd[n]).astype(bf16)
+
+
+def run_experts(place, masks, sends, xs, wg, wu, wd, sources):
     rows, share = xs[0].shape
     _, width, units = wg.shape
     tile = tile_of(units, 256)
-    weight = pl.BlockSpec((1, width, tile), lambda f, p: (0, 0, f))
-    return pl.pallas_call(
-        functools.partial(hidden_kernel, masks=masks),
-        grid_spec=pltpu.PrefetchScalarGridSpec(
-            num_scalar_prefetch=1,
-            grid=(units // tile,),
-            in_specs=[pl.BlockSpec((rows, share), lambda f, p: (0, 0))] * len(xs) + [weight] * 2,
-            out_specs=pl.BlockSpec((rows, tile), lambda f, p: (0, f)),
-        ),
-        out_shape=jax.ShapeDtypeStruct((rows, units), bf16),
-        compiler_params=pltpu.CompilerParams(vmem_limit_bytes=32 * 1024 * 1024),
+    tiles = units // tile
+    vm = pl.BlockSpec(memory_space=pltpu.VMEM)
+    held = pltpu.VMEM((tiles, len(masks), share, tile), bf16)
+    return pl.pallas_call(
+        functools.partial(experts_kernel, masks=masks, sends=tuple(sends), sources=sources),
+        in_specs=[pl.BlockSpec(memory_space=pltpu.SMEM)]
+        + [vm] * len(xs)
+        + [pl.BlockSpec(memory_space=pltpu.HBM)] * 3,
+        out_specs=[vm] * 2,
+        out_shape=[
+            jax.ShapeDtypeStruct((rows, units), bf16),
+            jax.ShapeDtypeStruct((len(sends), rows, share), bf16),
+        ],
+        scratch_shapes=[
+            held, held, pltpu.VMEM((len(sends), units, share), bf16),
+            pltpu.SemaphoreType.DMA((2, tiles, len(masks))), pltpu.SemaphoreType.DMA((len(sends),)),
+        ],
+        compiler_params=pltpu.CompilerParams(vmem_limit_bytes=VMEM_LIMIT),
         cost_estimate=pl.CostEstimate(
             flops=4 * rows * width * units, bytes_accessed=4 * width * units, transcendentals=0
         ),
-        name="hidden",
-    )(place, *xs, wg, wu)
-
-
-def down_kernel(place_ref, h_ref, w_ref, out_ref):
+        name="experts",
+    )(place, *xs, *hbm(wg, wu, wd))
+
+
+def keep_kernel(place_ref, h_ref, w_ref, out_ref):
     out_ref[0] = mm(h_ref[...], w_ref[0]).astype(bf16)
 
 
-def down(place, masks, h, wd, share):
+def keep_down(place, masks, h, wd, share):
     rows, units = h.shape
     masks = tuple(masks)
 
@@ -389,7 +542,7 @@
         return 0, 0, lax.bitwise_xor(p[0], mask)
 
     return pl.pallas_call(
-        down_kernel,
+        keep_kernel,
         grid_spec=pltpu.PrefetchScalarGridSpec(
             num_scalar_prefetch=1,
             grid=(len(masks),),
@@ -400,13 +553,13 @@
             out_specs=pl.BlockSpec((1, rows, share), lambda i, p: (i, 0, 0)),
         ),
         out_shape=jax.ShapeDtypeStruct((len(masks), rows, share), bf16),
-        compiler_params=pltpu.CompilerParams(vmem_limit_bytes=24 * 1024 * 1024),
+        compiler_params=pltpu.CompilerParams(vmem_limit_bytes=VMEM_LIMIT),
         cost_estimate=pl.CostEstimate(
             flops=2 * rows * units * share * len(masks),
             bytes_accessed=2 * units * share * len(masks), transcendentals=0,
         ),
-        name="down",
-    )(place, h, wd)
+        name="keep_down",
+    )(place, h, *hbm(wd))
 
 
 def project_kernel(*refs):
@@ -430,7 +583,7 @@
         + [pl.BlockSpec((lanes, tile), lambda i: (0, i))] * len(ws),
         out_specs=pl.BlockSpec((rows, tile), lambda i: (0, i)),
         out_shape=jax.ShapeDtypeStruct((rows, width), bf16),
-        compiler_params=pltpu.CompilerParams(vmem_limit_bytes=24 * 1024 * 1024),
+        compiler_params=pltpu.CompilerParams(vmem_limit_bytes=VMEM_LIMIT),
         cost_estimate=pl.CostEstimate(
             flops=2 * rows * lanes * width * len(xs),
             bytes_accessed=2 * lanes * width * len(xs), transcendentals=0,
@@ -444,13 +597,21 @@
     return lax.ppermute(x, "tp", [(i, i ^ mask) for i in range(count)])
 
 
+def hop(x, mask):
+    count = lax.axis_size("ep")
+    return lax.ppermute(x, "ep", [(i, i ^ mask) for i in range(count)])
+
+
 def gathered(x, far=None):
     masks, blocks = [0], [x]
     mask = lax.axis_size("tp") // 2
     if far is not None:
         masks, blocks, mask = [0, mask], [x, far], mask // 2
     while mask:
-        blocks += [swap(b, mask) for b in blocks]
+        more = []
+        for b in blocks:
+            more.append(swap(b, mask))
+        blocks += more
         masks += [m ^ mask for m in masks]
         mask //= 2
     return tuple(masks), blocks
@@ -466,61 +627,64 @@
     ep, tp = lax.axis_size("ep"), lax.axis_size("tp")
     place = lax.axis_index("tp").reshape(1).astype(jnp.int32)
     turn = lax.axis_index("ep").reshape(1).astype(jnp.int32)
+    both = jnp.concatenate([place, turn])
     tokens, width = expert_layer_input.shape
     experts = expert_router_weight.shape[1]
     share = width // tp
     capacity = 4 * tokens // ep
-    part = capacity // PARTS
-
-    *sends, info = route(
+
+    weight_far = swap(mixer_output_weight, tp // 2)
+    send, info = route(
         place, expert_layer_input, feedforward_norm_gain, group_router_weight.T,
-        expert_router_weight.T, routes.T, PARTS, part, share,
+        expert_router_weight.T, routes.T, 1, capacity, share,
     )
-    arrived = [lax.all_to_all(s, "ep", split_axis=0, concat_axis=0, tiled=True) for s in sends]
-    masks, blocks = [0], [mixer_output_weight]
-    top_mask = tp // 2
-    far = swap(mixer_output_weight, top_mask)
-
-    local_read, reached, end = mixer_local(
+    arrived = lax.all_to_all(send, "ep", split_axis=0, concat_axis=0, tiled=True)
+
+    mixer_args = (
         receptance, key_matrix, value_matrix, decay_data_term, correction_rate_data,
         decay_channel_offset, correction_rate_offset, extra_head_log_decay.T,
     )
-    arrived, far, end = lax.optimization_barrier((arrived, far, end))
-    weight_masks, weight_blocks = gathered(mixer_output_weight, far)
-    ends = lax.all_to_all(
-        jnp.broadcast_to(end[None], (ep,) + end.shape), "ep", split_axis=0, concat_axis=0, tiled=True
+    local_a, reach_a, state = mixer_local(0, 2, ep, None, *mixer_args)
+    arrived, state = lax.optimization_barrier((arrived, state))
+    rows_in = arrived.reshape(experts * capacity, share)
+    far = swap(rows_in, tp // 2)
+    local_b, reach_b, end = mixer_local(1, 2, ep, state, *mixer_args)
+    far, weight_far, local_b = lax.optimization_barrier((far, weight_far, local_b))
+    weight_masks, weight_blocks = gathered(mixer_output_weight, weight_far)
+    ends = lax.all_to_all(end, "ep", split_axis=0, concat_axis=0, tiled=True)
+
+    masks, blocks = gathered(rows_in, far)
+    odd = [m for m in range(tp) if m & 1]
+    even = [m for m in range(tp) if not m & 1]
+    h, send = run_experts(
+        both, masks, odd, blocks, expert_gate_weight, expert_up_weight, expert_down_weight, ep
     )
-
-    waiting = []
-    for piece in arrived:
-        masks, blocks = gathered(piece.reshape(experts * part, share))
-        h = hidden(place, masks, blocks, expert_gate_weight, expert_up_weight)
-        todo, bit = list(range(tp)), 1
-        odd = [m for m in todo if m & bit]
-        even = [m for m in todo if not m & bit]
-        send = down(place, odd, h, expert_down_weight, share)
-        keep = down(place, even, h, expert_down_weight, share)
-        while True:
+    keep = keep_down(place, even, h, expert_down_weight, share)
+    bit = 1
+    got = swap(send, bit)
+    while 2 * bit < tp:
+        bit *= 2
+        if 2 * bit < tp:
+            keep, send = split(keep, got, 1)
             got = swap(send, bit)
-            bit *= 2
-            if bit >= tp:
-                break
-            total = (keep.astype(f32) + got.astype(f32)).astype(bf16)
-            total = total.reshape((-1, 2) + total.shape[1:])
-            keep, send = total[:, 0], total[:, 1]
-        waiting.append((keep, got))
+        else:
+            keep, near, away = split(keep, got, 2)
+    half = near.shape[1]
+    away = swap(away, bit)
+    near = swap(near, bit)
+    away = merge(keep, away, half, capacity)
+    away = [hop(x, ep // 2 + m) for m, x in enumerate(away)]
+    near = merge(keep, near, 0, capacity)
+    near = [near[0]] + [hop(x, m) for m, x in enumerate(near) if m]
+    homes = near + away
 
     mixed = mixer_finish(
-        jnp.concatenate([turn, place]), ends, local_read, reached, output_gate_input, head_norm_gain, tp
+        both, ends, output_gate_input, head_norm_gain,
+        (local_a, local_b), (reach_a, reach_b), tp,
     )
     pieces = [mixed[m] if m == 0 else swap(mixed[m], m) for m in weight_masks]
     token_mixer_output = project(pieces, weight_blocks)
-    waiting, token_mixer_output = lax.optimization_barrier((waiting, token_mixer_output))
-    homes = []
-    for keep, got in waiting:
-        total = (keep.astype(f32) + got.astype(f32)).astype(bf16).reshape(experts, part, share)
-        homes.append(lax.all_to_all(total, "ep", split_axis=0, concat_axis=0, tiled=True))
-    expert_out = combine(info, homes, routes.shape[1])
+    expert_out = combine(both, info, homes, routes.shape[1])
     return (token_mixer_output, expert_out)
 
 

time: 125 us -> 110 us (0.88)
  blocking collectives: 20.7 us -> 0 us
  local copies, waits for them, and re-layouts: 17.6 us -> 1 us
  starting transfers between devices: 19.6 us -> 31.7 us
  Pallas kernels: 39.8 us -> 48 us
  waiting for transfers between devices: 23.1 us -> 27.8 us
  other arithmetic: 2.84 us -> 0.07 us
    all_to_all x1 -> x0, blocking collectives: 20.7 us -> none  [local(): lax.all_to_all(total, 'ep', split_axis=0, concat_axis=0, tiled=True)]
    unnamed x54 -> x8, local copies, waits for them, and re-layouts: 15.7 us -> 0.99 us
    ppermute x0 -> x7, starting transfers between devices: none -> 11.2 us  [hop(): return lax.ppermute(x, 'ep', [(i, i ^ mask) for i in range(count)])]
    pallas_call x6 -> x9, Pallas kernels: 34.6 us -> 42.4 us  [the longest x2 20.6 us: mixer_local(): pl.pallas_call(functools.partial(mixer_kernel, part == 0, last), grid=(1,...]
    ppermute x11 -> x12, waiting for transfers between devices: 15.8 us -> 20.8 us  [swap(): return lax.ppermute(x, 'tp', [(i, i ^ mask) for i in range(count)])]
    all_to_all x2, waiting for transfers between devices: 7.25 us -> 5.31 us  [the longest x1 2.7 us: local(): lax.all_to_all(send, 'ep', split_axis=0, concat_axis=0, tiled=True)]
    ppermute x0 -> x7, waiting for transfers between devices: none -> 1.69 us  [hop(): return lax.ppermute(x, 'ep', [(i, i ^ mask) for i in range(count)])]
    reshape x1 -> x0, other arithmetic: 1.59 us -> none  [local(): total = total.reshape((-1, 2) + total.shape[1:])]
  transfers between devices with their start and end apart: 13 -> 21, of which waited for: 6 -> 6; matrix products, arithmetic and copies ran while one was open for 3% -> 0% of each run, Pallas kernels for 23% -> 40%
where the time goes in v2:
time: 110 us; the launch traced here: 109 us
  Pallas kernels  48 us (44%)
  starting transfers between devices  31.7 us (29%)
  waiting for transfers between devices  27.8 us (25%)
    ppermute x12, waiting for transfers between devices, swap(): return lax.ppermute(x, 'tp', [(i, i ^ mask) for i in range(count)])  20.8 us
    pallas_call x2, Pallas kernels, mixer_local(): pl.pallas_call(functools.partial(mixer_kernel, part == 0, last), grid=(1,...  20.6 us
    ppermute x7, starting transfers between devices, hop(): return lax.ppermute(x, 'ep', [(i, i ^ mask) for i in range(count)])  11.2 us
    pallas_call x1, Pallas kernels, run_experts(): pl.pallas_call(functools.partial(experts_kernel, masks=masks, sends=tuple...  10.9 us
    ppermute x12, starting transfers between devices, swap(): return lax.ppermute(x, 'tp', [(i, i ^ mask) for i in range(count)])  7.52 us
    all_to_all x1, starting transfers between devices, local(): lax.all_to_all(send, 'ep', split_axis=0, concat_axis=0, tiled=True)  7.28 us
    all_to_all x1, starting transfers between devices, local(): ends = lax.all_to_all(end, 'ep', split_axis=0, concat_axis=0, tiled=True)  5.65 us
    pallas_call x1, Pallas kernels, project(): pl.pallas_call(project_kernel, grid=(width // tile,), in_specs=[pl.BlockS...  3.97 us
  transfers between devices with their start and end apart: 21, of which 6 were waited for; matrix products, arithmetic and copies ran while one was open for 0% of the time, Pallas kernels for 40%

profile of v2, /device:TPU:0, one launch (start us, length us, event | category | flops | bytes accessed | tf_op | source)
XLA Modules:
  0.0 109.3 jit_solution(9086070084668527034)
XLA Ops:
  0.6 0.0 copy-start
  0.6 2.9 %route.1 = (bf16[8,64,512]{2,1,0:T(8,128)(2,1)}, f32[128,8]{1,0:T(8,128)}) custom-call(s32[1]{0:T(128)} %bitcast.place_ref, bf16[128,2048]{1,0:T(8,128)(2,1)} %x_ref.1, f32[1,2048]{1,0:T(1,128)} %bitcast.24, bf16[4,2048]{1,0:T(4,128)(2,1)} %bitcast.23, bf16[8,2048]{1,0:T(8,128)(2,1)} %bitcast.22, s32[2,128]{1,0:T(2,128)} %bitcast.27), custom_call_target="tpu_custom_call" | custom-call | flops 4000000000 | bytes 1000000 | tf_op jit(solution)/shard_map/route/pallas_call | solution.py:355
  3.5 7.3 %all-to-all-start = ((bf16[8,64,512]{2,1,0:T(8,128)(2,1)}), bf16[8,64,512]{2,1,0:T(8,128)(2,1)S(1)}, u32[]{:S(2)}, u32[]{:S(2)}) async-start(bf16[8,64,512]{2,1,0:T(8,128)(2,1)} %get-tuple-element.28), calls=%async_computation | async-start | bytes 1048576 | tf_op jit(solution)/shard_map/all_to_all | solution.py:641
  10.8 0.0 copy-done
  10.8 1.6 %collective-permute-start.1 = (bf16[256,2048]{1,0:T(8,128)(2,1)S(1)}, bf16[256,2048]{1,0:T(8,128)(2,1)S(1)}, u32[]{:S(2)}, u32[]{:S(2)}) collective-permute-start(bf16[256,2048]{1,0:T(8,128)(2,1)S(1)} %copy-done), channel_id=1, source_target_pairs={{0,2},{1,3},{2,0},{3,1},{4,6},{5,7},{6,4},{7,5},{8,10},{9,11},{10,... | collective-permute-start | bytes 3145736 | tf_op jit(solution)/shard_map/ppermute | solution.py:597
  12.4 10.2 %mixer_local.2 = (f32[256,256]{1,0:T(8,128)}, bf16[256,256]{1,0:T(8,128)(2,1)}, f32[128,256]{1,0:T(8,128)S(1)}) custom-call(bf16[512,256]{1,0:T(8,128)(2,1)} %q_ref.3, bf16[512,256]{1,0:T(8,128)(2,1)} %k_ref.3, bf16[512,256]{1,0:T(8,128)(2,1)} %v_ref.3, bf16[512,256]{1,0:T(8,128)(2,1)} %w_ref.4, bf16[512,256]{1,0:T(8,128)(2,1)} %a_ref.3, f32[1,256]{1,0:T(1,128)} %bitcast.28, ...), custom_call_target="tpu_custom_call" | custom-call | flops 10000000000 | bytes 2000000 | tf_op jit(solution)/shard_map/mixer_local/pallas_call | solution.py:226
  22.6 2.7 %all-to-all-done = bf16[8,64,512]{2,1,0:T(8,128)(2,1)S(1)} async-done(((bf16[8,64,512]{2,1,0:T(8,128)(2,1)}), bf16[8,64,512]{2,1,0:T(8,128)(2,1)S(1)}, u32[]{:S(2)}, u32[]{:S(2)}) %all-to-all-start) | async-done | bytes 524320 | tf_op jit(solution)/shard_map/all_to_all | solution.py:641
  25.3 1.5 %collective-permute-start = (bf16[512,512]{1,0:T(8,128)(2,1)S(1)}, bf16[512,512]{1,0:T(8,128)(2,1)S(1)}, u32[]{:S(2)}, u32[]{:S(2)}) collective-permute-start(bf16[512,512]{1,0:T(8,128)(2,1)S(1)} %bitcast.19), channel_id=1, source_target_pairs={{0,2},{1,3},{2,0},{3,1},{4,6},{5,7},{6,4},{7,5},{8,10},{9,11},{10,... | collective-permute-start | bytes 1572872 | tf_op jit(solution)/shard_map/ppermute | solution.py:597
  26.8 0.0 collective-permute-start.7
  26.8 10.4 %mixer_local.3 = (f32[256,256]{1,0:T(8,128)}, bf16[256,256]{1,0:T(8,128)(2,1)}, bf16[8,128,256]{2,1,0:T(8,128)(2,1)}) custom-call(bf16[512,256]{1,0:T(8,128)(2,1)} %q_ref.3, bf16[512,256]{1,0:T(8,128)(2,1)} %k_ref.3, bf16[512,256]{1,0:T(8,128)(2,1)} %v_ref.3, bf16[512,256]{1,0:T(8,128)(2,1)} %w_ref.4, bf16[512,256]{1,0:T(8,128)(2,1)} %a_ref.3, ...), custom_call_target="tpu_custom_call" | custom-call | flops 10000000000 | bytes 2000000 | tf_op jit(solution)/shard_map/mixer_local/pallas_call | solution.py:226
  37.2 0.0 collective-permute-done.1.refs_5_
  37.2 9.5 %collective-permute-done.refs_1_ = bf16[512,512]{1,0:T(8,128)(2,1)S(1)} collective-permute-done((bf16[512,512]{1,0:T(8,128)(2,1)S(1)}, bf16[512,512]{1,0:T(8,128)(2,1)S(1)}, u32[]{:S(2)}, u32[]{:S(2)}) %collective-permute-start) | collective-permute-done | bytes 524320 | tf_op jit(solution)/shard_map/ppermute | solution.py:597
  46.7 0.0 collective-permute-start.8
  46.7 0.1 pad_add_fusion.place_ref
  46.8 5.7 %all-to-all-start.1 = ((bf16[8,128,256]{2,1,0:T(8,128)(2,1)}), bf16[8,128,256]{2,1,0:T(8,128)(2,1)}, u32[]{:S(2)}, u32[]{:S(2)}) async-start(bf16[8,128,256]{2,1,0:T(8,128)(2,1)} %get-tuple-element.31), calls=%async_computation.1 | async-start | bytes 1048576 | tf_op jit(solution)/shard_map/all_to_all | solution.py:654
  52.4 0.0 collective-permute-done.7.refs_2_
  52.5 0.0 collective-permute-done.8.refs_3_
  52.5 10.9 %experts.1 = (bf16[512,1024]{1,0:T(8,128)(2,1)S(1)}, bf16[2,512,512]{2,1,0:T(8,128)(2,1)}) custom-call(s32[2]{0:T(128)S(1)} %pad_add_fusion.place_ref, bf16[512,512]{1,0:T(8,128)(2,1)S(1)} %bitcast.21, bf16[512,512]{1,0:T(8,128)(2,1)S(1)} %collective-permute-done.refs_1_, bf16[512,512]{1,0:T(8,128)(2,1)} %collective-permute-done.7.refs_2_, ...), custom_call_target="tpu_custom_call" | custom-call | flops 4294967296 | bytes 8388608 | tf_op jit(solution)/shard_map/experts/pallas_call | solution.py:508
  63.4 0.0 copy-start.1
  63.4 1.0 copy-done.1
  64.4 0.2 collective-permute-start.9
  64.6 0.3 collective-permute-start.5
  64.9 0.2 collective-permute-start.6
  65.1 2.6 %all-to-all-done.1.ends_ref = bf16[8,128,256]{2,1,0:T(8,128)(2,1)} async-done(((bf16[8,128,256]{2,1,0:T(8,128)(2,1)}), bf16[8,128,256]{2,1,0:T(8,128)(2,1)}, u32[]{:S(2)}, u32[]{:S(2)}) %all-to-all-start.1) | async-done | bytes 524320 | tf_op jit(solution)/shard_map/all_to_all | solution.py:654
  67.7 0.0 copy-start.2
  67.7 3.6 %mixer_finish.1 = bf16[4,128,256]{2,1,0:T(8,128)(2,1)S(1)} custom-call(s32[2]{0:T(128)S(1)} %pad_add_fusion.place_ref, bf16[8,128,256]{2,1,0:T(8,128)(2,1)} %all-to-all-done.1.ends_ref, bf16[512,256]{1,0:T(8,128)(2,1)} %gate_ref.1, f32[1,256]{1,0:T(1,128)} %bitcast.32, f32[256,256]{1,0:T(8,128)} %get-tuple-element.32.refs_0_, ...), custom_call_target="tpu_custom_call" | custom-call | flops 4000000000 | bytes 2000000 | tf_op jit(solution)/shard_map/mixer_finish/pallas_call | solution.py:293
  71.3 0.0 copy-done.2
  71.3 2.7 %keep_down.1.keep_ref = bf16[2,512,512]{2,1,0:T(8,128)(2,1)S(1)} custom-call(s32[1]{0:T(128)} %bitcast.place_ref, bf16[512,1024]{1,0:T(8,128)(2,1)S(1)} %copy-done.2, bf16[1,1024,2048]{2,1,0:T(8,128)(2,1)} %w_ref.5), custom_call_target="tpu_custom_call" | custom-call | flops 1073741824 | bytes 2097152 | tf_op jit(solution)/shard_map/keep_down/pallas_call | solution.py:544
  74.0 0.0 copy-start.3
  74.0 0.0 collective-permute-done.9.got_ref
  74.0 1.6 %split.1 = (bf16[1,512,512]{2,1,0:T(8,128)(2,1)S(1)}, bf16[1,256,512]{2,1,0:T(8,128)(2,1)S(1)}, bf16[1,256,512]{2,1,0:T(8,128)(2,1)S(1)}) custom-call(bf16[2,512,512]{2,1,0:T(8,128)(2,1)S(1)} %keep_down.1.keep_ref, bf16[2,512,512]{2,1,0:T(8,128)(2,1)} %collective-permute-done.9.got_ref), custom_call_target="tpu_custom_call" | custom-call | flops 100000000 | bytes 1000000 | tf_op jit(solution)/shard_map/split/pallas_call | solution.py:438
  75.6 1.6 %collective-permute-start.10 = (bf16[1,256,512]{2,1,0:T(8,128)(2,1)S(1)}, bf16[1,256,512]{2,1,0:T(8,128)(2,1)S(1)}, u32[]{:S(2)}, u32[]{:S(2)}) collective-permute-start(bf16[1,256,512]{2,1,0:T(8,128)(2,1)S(1)} %get-tuple-element.44), channel_id=1, source_target_pairs={{0,2},{1,3},{2,0},{3,1},{4,6},{5,7},{6,4},{7,5},{8,10},{9,11},{10,... | collective-permute-start | bytes 786440 | tf_op jit(solution)/shard_map/ppermute | solution.py:597
  77.2 0.5 collective-permute-start.14
  77.8 1.6 %collective-permute-start.2 = (bf16[128,256]{1,0:T(8,128)(2,1)S(1)}, bf16[128,256]{1,0:T(8,128)(2,1)S(1)}, u32[]{:S(2)}, u32[]{:S(2)}) collective-permute-start(bf16[128,256]{1,0:T(8,128)(2,1)S(1)} %get-tuple-element.56), channel_id=1, source_target_pairs={{0,2},{1,3},{2,0},{3,1},{4,6},{5,7},{6,4},{7,5},{8,10},{9,11},{10,... | collective-permute-start | bytes 196616 | tf_op jit(solution)/shard_map/ppermute | solution.py:597
  79.3 0.0 collective-permute-done.5.refs_6_
  79.4 0.0 collective-permute-start.3
  79.4 5.5 %collective-permute-done.10.got_ref = bf16[1,256,512]{2,1,0:T(8,128)(2,1)S(1)} collective-permute-done((bf16[1,256,512]{2,1,0:T(8,128)(2,1)S(1)}, bf16[1,256,512]{2,1,0:T(8,128)(2,1)S(1)}, u32[]{:S(2)}, u32[]{:S(2)}) %collective-permute-start.10) | collective-permute-done | bytes 262176 | tf_op jit(solution)/shard_map/ppermute | solution.py:597
  84.9 0.0 collective-permute-start.4
  84.9 0.1 merge.2
  85.0 5.8 %collective-permute-done.2.refs_1_ = bf16[128,256]{1,0:T(8,128)(2,1)S(1)} collective-permute-done((bf16[128,256]{1,0:T(8,128)(2,1)S(1)}, bf16[128,256]{1,0:T(8,128)(2,1)S(1)}, u32[]{:S(2)}, u32[]{:S(2)}) %collective-permute-start.2) | collective-permute-done | bytes 65568 | tf_op jit(solution)/shard_map/ppermute | solution.py:597
  90.7 1.8 %collective-permute-start.11 = (bf16[64,512]{1,0:T(8,128)(2,1)S(1)}, bf16[64,512]{1,0:T(8,128)(2,1)S(1)}, u32[]{:S(2)}, u32[]{:S(2)}) collective-permute-start(bf16[64,512]{1,0:T(8,128)(2,1)S(1)} %get-tuple-element.46), channel_id=1, source_target_pairs={{0,4},{4,0},{8,12},{12,8},{16,20},{20,16},{24,28},{28,24},{1,5},{5... | collective-permute-start | bytes 196616 | tf_op jit(solution)/shard_map/ppermute | solution.py:602
  92.5 0.0 collective-permute-done.14.got_ref
  92.5 0.1 collective-permute-start.12
  92.6 0.1 merge.3
  92.6 0.0 collective-permute-done.3.refs_2_
  92.6 1.7 %collective-permute-start.13 = (bf16[64,512]{1,0:T(8,128)(2,1)S(1)}, bf16[64,512]{1,0:T(8,128)(2,1)S(1)}, u32[]{:S(2)}, u32[]{:S(2)}) collective-permute-start(bf16[64,512]{1,0:T(8,128)(2,1)S(1)} %get-tuple-element.48), channel_id=1, source_target_pairs={{0,12},{4,8},{8,4},{12,0},{16,28},{20,24},{24,20},{28,16},{1,13},{... | collective-permute-start | bytes 196616 | tf_op jit(solution)/shard_map/ppermute | solution.py:602
  94.4 0.0 collective-permute-done.4.refs_3_
  94.4 1.3 %collective-permute-start.15 = (bf16[64,512]{1,0:T(8,128)(2,1)S(1)}, bf16[64,512]{1,0:T(8,128)(2,1)S(1)}, u32[]{:S(2)}, u32[]{:S(2)}) collective-permute-start(bf16[64,512]{1,0:T(8,128)(2,1)S(1)} %get-tuple-element.50), channel_id=1, source_target_pairs={{0,16},{4,20},{8,24},{12,28},{16,0},{20,4},{24,8},{28,12},{1,17},{... | collective-permute-start | bytes 196616 | tf_op jit(solution)/shard_map/ppermute | solution.py:602
  95.7 0.0 collective-permute-done.6.refs_7_
  95.7 2.8 %collective-permute-start.16 = (bf16[64,512]{1,0:T(8,128)(2,1)S(1)}, bf16[64,512]{1,0:T(8,128)(2,1)S(1)}, u32[]{:S(2)}, u32[]{:S(2)}) collective-permute-start(bf16[64,512]{1,0:T(8,128)(2,1)S(1)} %get-tuple-element.51), channel_id=1, source_target_pairs={{0,20},{4,16},{8,28},{12,24},{16,4},{20,0},{24,12},{28,8},{1,21},{... | collective-permute-start | bytes 196616 | tf_op jit(solution)/shard_map/ppermute | solution.py:602
  98.5 0.0 collective-permute-done.11.refs_1_
  98.5 2.1 %collective-permute-start.17 = (bf16[64,512]{1,0:T(8,128)(2,1)S(1)}, bf16[64,512]{1,0:T(8,128)(2,1)S(1)}, u32[]{:S(2)}, u32[]{:S(2)}) collective-permute-start(bf16[64,512]{1,0:T(8,128)(2,1)S(1)} %get-tuple-element.52), channel_id=1, source_target_pairs={{0,24},{4,28},{8,16},{12,20},{16,8},{20,12},{24,0},{28,4},{1,25},{... | collective-permute-start | bytes 196616 | tf_op jit(solution)/shard_map/ppermute | solution.py:602
  100.6 0.0 collective-permute-done.12.refs_2_
  100.6 1.4 %collective-permute-start.18 = (bf16[64,512]{1,0:T(8,128)(2,1)S(1)}, bf16[64,512]{1,0:T(8,128)(2,1)S(1)}, u32[]{:S(2)}, u32[]{:S(2)}) collective-permute-start(bf16[64,512]{1,0:T(8,128)(2,1)S(1)} %get-tuple-element.53), channel_id=1, source_target_pairs={{0,28},{4,24},{8,20},{12,16},{16,12},{20,8},{24,4},{28,0},{1,29},{... | collective-permute-start | bytes 196616 | tf_op jit(solution)/shard_map/ppermute | solution.py:602
  102.0 4.0 %project.1 = bf16[128,2048]{1,0:T(8,128)(2,1)} custom-call(bf16[128,256]{1,0:T(8,128)(2,1)S(1)} %get-tuple-element.57.refs_0_, bf16[128,256]{1,0:T(8,128)(2,1)S(1)} %collective-permute-done.2.refs_1_, bf16[128,256]{1,0:T(8,128)(2,1)S(1)} %collective-permute-done.3.refs_2_, bf16[128,256]{1,0:T(8,128)(2,1)S(1)} %collective-permute-done.4.refs_3_, ...), custom_call_target="tpu_custom_call" | custom-call | flops 536870912 | bytes 4194304 | tf_op jit(solution)/shard_map/project/pallas_call | solution.py:579
  106.0 0.0 collective-permute-done.13.refs_3_
  106.0 0.0 collective-permute-done.15.refs_4_
  106.0 0.0 collective-permute-done.16.refs_5_
  106.0 0.0 collective-permute-done.17.refs_6_
  106.0 1.7 %collective-permute-done.18.refs_7_ = bf16[64,512]{1,0:T(8,128)(2,1)S(1)} collective-permute-done((bf16[64,512]{1,0:T(8,128)(2,1)S(1)}, bf16[64,512]{1,0:T(8,128)(2,1)S(1)}, u32[]{:S(2)}, u32[]{:S(2)}) %collective-permute-start.18) | collective-permute-done | bytes 65568 | tf_op jit(solution)/shard_map/ppermute | solution.py:602
  107.7 0.0 copy-done.3
  107.7 1.6 %combine.1 = bf16[128,512]{1,0:T(8,128)(2,1)} custom-call(s32[2]{0:T(128)S(1)} %pad_add_fusion.place_ref, f32[128,8]{1,0:T(8,128)S(1)} %copy-done.3, bf16[64,512]{1,0:T(8,128)(2,1)S(1)} %get-tuple-element.45.refs_0_, bf16[64,512]{1,0:T(8,128)(2,1)S(1)} %collective-permute-done.11.refs_1_, bf16[64,512]{1,0:T(8,128)(2,1)S(1)} %collective-permute-done.12.refs_2_, ...), custom_call_target="tpu_custom_call" | custom-call | flops 1000000000 | bytes 1000000 | tf_op jit(solution)/shard_map/combine/pallas_call | solution.py:389
  (1 shorter events, 0.0 us)
Async XLA Ops:
  0.6 10.2 %copy-start = (bf16[256,2048]{1,0:T(8,128)(2,1)S(1)}, bf16[256,2048]{1,0:T(8,128)(2,1)}, u32[]{:S(2)}) copy-start(bf16[256,2048]{1,0:T(8,128)(2,1)} %refs_4_.2) | copy-start | bytes 3145732
  3.5 21.8 %all-to-all-start = ((bf16[8,64,512]{2,1,0:T(8,128)(2,1)}), bf16[8,64,512]{2,1,0:T(8,128)(2,1)S(1)}, u32[]{:S(2)}, u32[]{:S(2)}) async-start(bf16[8,64,512]{2,1,0:T(8,128)(2,1)} %get-tuple-element.28), calls=%async_computation | async-start | bytes 1048576 | tf_op jit(solution)/shard_map/all_to_all | solution.py:641
  10.8 26.4 %collective-permute-start.1 = (bf16[256,2048]{1,0:T(8,128)(2,1)S(1)}, bf16[256,2048]{1,0:T(8,128)(2,1)S(1)}, u32[]{:S(2)}, u32[]{:S(2)}) collective-permute-start(bf16[256,2048]{1,0:T(8,128)(2,1)S(1)} %copy-done), channel_id=1, source_target_pairs={{0,2},{1,3},{2,0},{3,1},{4,6},{5,7},{6,4},{7,5},{8,10},{9,11},{10,... | collective-permute-start | bytes 3145736 | tf_op jit(solution)/shard_map/ppermute | solution.py:597
  25.3 21.4 %collective-permute-start = (bf16[512,512]{1,0:T(8,128)(2,1)S(1)}, bf16[512,512]{1,0:T(8,128)(2,1)S(1)}, u32[]{:S(2)}, u32[]{:S(2)}) collective-permute-start(bf16[512,512]{1,0:T(8,128)(2,1)S(1)} %bitcast.19), channel_id=1, source_target_pairs={{0,2},{1,3},{2,0},{3,1},{4,6},{5,7},{6,4},{7,5},{8,10},{9,11},{10,... | collective-permute-start | bytes 1572872 | tf_op jit(solution)/shard_map/ppermute | solution.py:597
  26.8 25.7 %collective-permute-start.7 = (bf16[512,512]{1,0:T(8,128)(2,1)S(1)}, bf16[512,512]{1,0:T(8,128)(2,1)}, u32[]{:S(2)}, u32[]{:S(2)}) collective-permute-start(bf16[512,512]{1,0:T(8,128)(2,1)S(1)} %bitcast.20), channel_id=1, source_target_pairs={{0,1},{1,0},{2,3},{3,2},{4,5},{5,4},{6,7},{7,6},{8,9},{9,8},{10,11... | collective-permute-start | bytes 1572872 | tf_op jit(solution)/shard_map/ppermute | solution.py:597
  46.7 5.7 %collective-permute-start.8 = (bf16[512,512]{1,0:T(8,128)(2,1)S(1)}, bf16[512,512]{1,0:T(8,128)(2,1)}, u32[]{:S(2)}, u32[]{:S(2)}) collective-permute-start(bf16[512,512]{1,0:T(8,128)(2,1)S(1)} %collective-permute-done.refs_1_), channel_id=1, source_target_pairs={{0,1},{1,0},{2,3},{3,2},{4,5},{5,4},{6,7},{7,6},{8,9},{9,8},{10,11... | collective-permute-start | bytes 1572872 | tf_op jit(solution)/shard_map/ppermute | solution.py:597
  46.8 20.9 %all-to-all-start.1 = ((bf16[8,128,256]{2,1,0:T(8,128)(2,1)}), bf16[8,128,256]{2,1,0:T(8,128)(2,1)}, u32[]{:S(2)}, u32[]{:S(2)}) async-start(bf16[8,128,256]{2,1,0:T(8,128)(2,1)} %get-tuple-element.31), calls=%async_computation.1 | async-start | bytes 1048576 | tf_op jit(solution)/shard_map/all_to_all | solution.py:654
  63.4 1.0 copy-start.1
  64.4 9.7 %collective-permute-start.9 = (bf16[2,512,512]{2,1,0:T(8,128)(2,1)}, bf16[2,512,512]{2,1,0:T(8,128)(2,1)}, u32[]{:S(2)}, u32[]{:S(2)}) collective-permute-start(bf16[2,512,512]{2,1,0:T(8,128)(2,1)} %get-tuple-element.42), channel_id=1, source_target_pairs={{0,1},{1,0},{2,3},{3,2},{4,5},{5,4},{6,7},{7,6},{8,9},{9,8},{10,11... | collective-permute-start | bytes 3145736 | tf_op jit(solution)/shard_map/ppermute | solution.py:597
  64.6 14.8 %collective-permute-start.5 = (bf16[256,2048]{1,0:T(8,128)(2,1)S(1)}, bf16[256,2048]{1,0:T(8,128)(2,1)S(1)}, u32[]{:S(2)}, u32[]{:S(2)}) collective-permute-start(bf16[256,2048]{1,0:T(8,128)(2,1)S(1)} %copy-done), channel_id=1, source_target_pairs={{0,1},{1,0},{2,3},{3,2},{4,5},{5,4},{6,7},{7,6},{8,9},{9,8},{10,11... | collective-permute-start | bytes 3145736 | tf_op jit(solution)/shard_map/ppermute | solution.py:597
  64.9 30.8 %collective-permute-start.6 = (bf16[256,2048]{1,0:T(8,128)(2,1)S(1)}, bf16[256,2048]{1,0:T(8,128)(2,1)}, u32[]{:S(2)}, u32[]{:S(2)}) collective-permute-start(bf16[256,2048]{1,0:T(8,128)(2,1)S(1)} %collective-permute-done.1.refs_5_), channel_id=1, source_target_pairs={{0,1},{1,0},{2,3},{3,2},{4,5},{5,4},{6,7},{7,6},{8,9},{9,8},{10,11... | collective-permute-start | bytes 3145736 | tf_op jit(solution)/shard_map/ppermute | solution.py:597
  67.7 3.6 %copy-start.2 = (bf16[512,1024]{1,0:T(8,128)(2,1)S(1)}, bf16[512,1024]{1,0:T(8,128)(2,1)}, u32[]{:S(2)}) copy-start(bf16[512,1024]{1,0:T(8,128)(2,1)} %copy-done.1) | copy-start | bytes 3145732
  74.0 33.7 %copy-start.3 = (f32[128,8]{1,0:T(8,128)S(1)}, f32[128,8]{1,0:T(8,128)}, u32[]{:S(2)}) copy-start(f32[128,8]{1,0:T(8,128)} %get-tuple-element.39.info_ref) | copy-start | bytes 12292
  75.6 9.2 %collective-permute-start.10 = (bf16[1,256,512]{2,1,0:T(8,128)(2,1)S(1)}, bf16[1,256,512]{2,1,0:T(8,128)(2,1)S(1)}, u32[]{:S(2)}, u32[]{:S(2)}) collective-permute-start(bf16[1,256,512]{2,1,0:T(8,128)(2,1)S(1)} %get-tuple-element.44), channel_id=1, source_target_pairs={{0,2},{1,3},{2,0},{3,1},{4,6},{5,7},{6,4},{7,5},{8,10},{9,11},{10,... | collective-permute-start | bytes 786440 | tf_op jit(solution)/shard_map/ppermute | solution.py:597
  77.2 15.2 %collective-permute-start.14 = (bf16[1,256,512]{2,1,0:T(8,128)(2,1)S(1)}, bf16[1,256,512]{2,1,0:T(8,128)(2,1)S(1)}, u32[]{:S(2)}, u32[]{:S(2)}) collective-permute-start(bf16[1,256,512]{2,1,0:T(8,128)(2,1)S(1)} %get-tuple-element.49), channel_id=1, source_target_pairs={{0,2},{1,3},{2,0},{3,1},{4,6},{5,7},{6,4},{7,5},{8,10},{9,11},{10,... | collective-permute-start | bytes 786440 | tf_op jit(solution)/shard_map/ppermute | solution.py:597
  77.8 13.0 %collective-permute-start.2 = (bf16[128,256]{1,0:T(8,128)(2,1)S(1)}, bf16[128,256]{1,0:T(8,128)(2,1)S(1)}, u32[]{:S(2)}, u32[]{:S(2)}) collective-permute-start(bf16[128,256]{1,0:T(8,128)(2,1)S(1)} %get-tuple-element.56), channel_id=1, source_target_pairs={{0,2},{1,3},{2,0},{3,1},{4,6},{5,7},{6,4},{7,5},{8,10},{9,11},{10,... | collective-permute-start | bytes 196616 | tf_op jit(solution)/shard_map/ppermute | solution.py:597
  79.4 13.3 %collective-permute-start.3 = (bf16[128,256]{1,0:T(8,128)(2,1)S(1)}, bf16[128,256]{1,0:T(8,128)(2,1)S(1)}, u32[]{:S(2)}, u32[]{:S(2)}) collective-permute-start(bf16[128,256]{1,0:T(8,128)(2,1)S(1)} %get-tuple-element.55), channel_id=1, source_target_pairs={{0,1},{1,0},{2,3},{3,2},{4,5},{5,4},{6,7},{7,6},{8,9},{9,8},{10,11... | collective-permute-start | bytes 196616 | tf_op jit(solution)/shard_map/ppermute | solution.py:597
  84.9 9.5 %collective-permute-start.4 = (bf16[128,256]{1,0:T(8,128)(2,1)S(1)}, bf16[128,256]{1,0:T(8,128)(2,1)S(1)}, u32[]{:S(2)}, u32[]{:S(2)}) collective-permute-start(bf16[128,256]{1,0:T(8,128)(2,1)S(1)} %get-tuple-element.54), channel_id=1, source_target_pairs={{0,3},{1,2},{2,1},{3,0},{4,7},{5,6},{6,5},{7,4},{8,11},{9,10},{10,... | collective-permute-start | bytes 196616 | tf_op jit(solution)/shard_map/ppermute | solution.py:597
  90.7 7.8 %collective-permute-start.11 = (bf16[64,512]{1,0:T(8,128)(2,1)S(1)}, bf16[64,512]{1,0:T(8,128)(2,1)S(1)}, u32[]{:S(2)}, u32[]{:S(2)}) collective-permute-start(bf16[64,512]{1,0:T(8,128)(2,1)S(1)} %get-tuple-element.46), channel_id=1, source_target_pairs={{0,4},{4,0},{8,12},{12,8},{16,20},{20,16},{24,28},{28,24},{1,5},{5... | collective-permute-start | bytes 196616 | tf_op jit(solution)/shard_map/ppermute | solution.py:602
  92.5 8.1 %collective-permute-start.12 = (bf16[64,512]{1,0:T(8,128)(2,1)S(1)}, bf16[64,512]{1,0:T(8,128)(2,1)S(1)}, u32[]{:S(2)}, u32[]{:S(2)}) collective-permute-start(bf16[64,512]{1,0:T(8,128)(2,1)S(1)} %get-tuple-element.47), channel_id=1, source_target_pairs={{0,8},{4,12},{8,0},{12,4},{16,24},{20,28},{24,16},{28,20},{1,9},{5... | collective-permute-start | bytes 196616 | tf_op jit(solution)/shard_map/ppermute | solution.py:602
  92.6 13.4 %collective-permute-start.13 = (bf16[64,512]{1,0:T(8,128)(2,1)S(1)}, bf16[64,512]{1,0:T(8,128)(2,1)S(1)}, u32[]{:S(2)}, u32[]{:S(2)}) collective-permute-start(bf16[64,512]{1,0:T(8,128)(2,1)S(1)} %get-tuple-element.48), channel_id=1, source_target_pairs={{0,12},{4,8},{8,4},{12,0},{16,28},{20,24},{24,20},{28,16},{1,13},{... | collective-permute-start | bytes 196616 | tf_op jit(solution)/shard_map/ppermute | solution.py:602
  94.4 11.6 %collective-permute-start.15 = (bf16[64,512]{1,0:T(8,128)(2,1)S(1)}, bf16[64,512]{1,0:T(8,128)(2,1)S(1)}, u32[]{:S(2)}, u32[]{:S(2)}) collective-permute-start(bf16[64,512]{1,0:T(8,128)(2,1)S(1)} %get-tuple-element.50), channel_id=1, source_target_pairs={{0,16},{4,20},{8,24},{12,28},{16,0},{20,4},{24,8},{28,12},{1,17},{... | collective-permute-start | bytes 196616 | tf_op jit(solution)/shard_map/ppermute | solution.py:602
  95.7 10.3 %collective-permute-start.16 = (bf16[64,512]{1,0:T(8,128)(2,1)S(1)}, bf16[64,512]{1,0:T(8,128)(2,1)S(1)}, u32[]{:S(2)}, u32[]{:S(2)}) collective-permute-start(bf16[64,512]{1,0:T(8,128)(2,1)S(1)} %get-tuple-element.51), channel_id=1, source_target_pairs={{0,20},{4,16},{8,28},{12,24},{16,4},{20,0},{24,12},{28,8},{1,21},{... | collective-permute-start | bytes 196616 | tf_op jit(solution)/shard_map/ppermute | solution.py:602
  98.5 7.5 %collective-permute-start.17 = (bf16[64,512]{1,0:T(8,128)(2,1)S(1)}, bf16[64,512]{1,0:T(8,128)(2,1)S(1)}, u32[]{:S(2)}, u32[]{:S(2)}) collective-permute-start(bf16[64,512]{1,0:T(8,128)(2,1)S(1)} %get-tuple-element.52), channel_id=1, source_target_pairs={{0,24},{4,28},{8,16},{12,20},{16,8},{20,12},{24,0},{28,4},{1,25},{... | collective-permute-start | bytes 196616 | tf_op jit(solution)/shard_map/ppermute | solution.py:602
  100.6 7.1 %collective-permute-start.18 = (bf16[64,512]{1,0:T(8,128)(2,1)S(1)}, bf16[64,512]{1,0:T(8,128)(2,1)S(1)}, u32[]{:S(2)}, u32[]{:S(2)}) collective-permute-start(bf16[64,512]{1,0:T(8,128)(2,1)S(1)} %get-tuple-element.53), channel_id=1, source_target_pairs={{0,28},{4,24},{8,20},{12,16},{16,12},{20,8},{24,4},{28,0},{1,29},{... | collective-permute-start | bytes 196616 | tf_op jit(solution)/shard_map/ppermute | solution.py:602

commit v3 on v2

--- a/solution.py
+++ b/solution.py
@@ -67,9 +67,20 @@
 
 
 def mixer_kernel(
-    first_part, last_part, q_ref, k_ref, v_ref, w_ref, a_ref, wo_ref, ao_ref, ex_ref, *refs
+    base, first_part, last_part, q_in, k_in, v_in, w_in, a_in, wo_ref, ao_ref, ex_ref, *refs
 ):
     refs = list(refs)
+    *refs, q_ref, k_ref, v_ref, w_ref, a_ref, in_sem = refs
+    loads = [
+        pltpu.make_async_copy(src.at[pl.ds(base, dst.shape[0]), :], dst, in_sem.at[n])
+        for n, (src, dst) in enumerate(
+            ((k_in, k_ref), (a_in, a_ref), (w_in, w_ref), (q_in, q_ref), (v_in, v_ref))
+        )
+    ]
+    for load in loads:
+        load.start()
+    for load in loads:
+        load.wait()
     start_ref = None if first_part else refs.pop(0)
     local_ref, reach_ref, end_ref = refs[:3]
     (
@@ -87,7 +98,7 @@
     u_s[...] = u
     r_s[...] = u * jax.nn.sigmoid(a_ref[...].astype(f32) + ao_ref[...])
     owner = (iota((heads, lanes), 1) // HEAD_DIM == iota((heads, lanes), 0)).astype(bf16)
-    exb = sum(mm(p, owner, TN) for p in thirds(ex_ref[...]))
+    exb = sum(mm(p, owner, TN) for p in thirds(ex_ref[...]))[base : base + rows]
     pre = w_ref[...].astype(f32) + wo_ref[...]
     ld_s[...] = exb - jax.nn.sigmoid(pre) * 0.6065306597126334
 
@@ -132,7 +143,7 @@
         )
         return 0
 
-    lax.fori_loop(0, chunks, first, 0, unroll=4)
+    lax.fori_loop(0, chunks, first, 0, unroll=True)
 
     dall = diag_s[...].reshape(chunks * BASE, lanes)
     dparts = thirds(dall)
@@ -186,7 +197,7 @@
         g_s[i] = mm(vt, spread(kh_s[at, :], hm)) - mm(zat, spread(rh_s[at, :], hm))
         return 0
 
-    lax.fori_loop(0, chunks, second, 0, unroll=4)
+    lax.fori_loop(0, chunks, second, 0, unroll=True)
 
     def third(i, x):
         at = pl.ds(pl.multiple_of(i * C, C), C)
@@ -204,31 +215,31 @@
         x0 = jnp.concatenate([jnp.zeros((HEAD_DIM, lanes), f32), pickv.astype(f32)], axis=0)
     else:
         x0 = start_ref[...]
-    x = lax.fori_loop(0, chunks, third, x0, unroll=4)
+    x = lax.fori_loop(0, chunks, third, x0, unroll=True)
     if last_part:
         end_ref[...] = jnp.broadcast_to(x.astype(bf16)[None], end_ref.shape)
     else:
         end_ref[...] = x
 
 
-def mixer_local(part, parts, copies, start, q, k, v, w, a, wo, ao, ex):
-    rows, lanes = q.shape
-    rows //= parts
-    chunks = rows // HEAD_DIM
+def mixer_local(part, copies, start, q, k, v, w, a, wo, ao, ex):
+    total, lanes = q.shape
+    cut = -(-(total // HEAD_DIM) * 5 // 8)
+    base, chunks = ((0, cut), (cut, total // HEAD_DIM - cut))[part]
+    base, rows = base * HEAD_DIM, chunks * HEAD_DIM
     heads = ex.shape[0]
     V = pltpu.VMEM
-    block = pl.BlockSpec((rows, lanes), lambda i: (part, 0))
     vector = pl.BlockSpec((1, lanes), lambda i: (0, 0))
     state = pl.BlockSpec((2 * HEAD_DIM, lanes), lambda i: (0, 0))
     out = pl.BlockSpec((rows, lanes), lambda i: (0, 0))
-    last = part == parts - 1
+    last = part == 1
     ends = (copies, 2 * HEAD_DIM, lanes)
     return pl.pallas_call(
-        functools.partial(mixer_kernel, part == 0, last),
+        functools.partial(mixer_kernel, base, part == 0, last),
         grid=(1,),
-        in_specs=[block] * 5
+        in_specs=[pl.BlockSpec(memory_space=pltpu.HBM)] * 5
         + [vector] * 2
-        + [pl.BlockSpec((heads, rows), lambda i: (0, part))]
+        + [pl.BlockSpec((heads, total), lambda i: (0, 0))]
         + ([] if start is None else [state]),
         out_specs=[out, out, pl.BlockSpec(ends, lambda i: (0, 0, 0)) if last else state],
         out_shape=[
@@ -242,7 +253,9 @@
             V((rows, lanes), bf16), V((rows, lanes), f32), V((rows, lanes), bf16), V((rows, lanes), bf16),
             V((chunks, lanes, lanes), bf16), V((rows, lanes), bf16), V((chunks, HEAD_DIM, lanes), f32),
             V((chunks, lanes), f32),
-        ],
+        ]
+        + [V((rows, lanes), bf16)] * 5
+        + [pltpu.SemaphoreType.DMA((5,))],
         compiler_params=pltpu.CompilerParams(vmem_limit_bytes=VMEM_LIMIT),
         cost_estimate=pl.CostEstimate(flops=10_000_000_000, bytes_accessed=2_000_000, transcendentals=0),
         name="mixer_local",
@@ -267,10 +280,11 @@
 
     s = lax.fori_loop(0, devices - 1, hop, jnp.zeros((HEAD_DIM, lanes), f32), unroll=True)
     sbd = spread(s.astype(bf16), hm)
-    gain = gain_ref[...]
-    for j, (local_ref, reach_ref) in enumerate(zip(refs[:parts], refs[parts : 2 * parts])):
+    gain, begin = gain_ref[...], 0
+    for local_ref, reach_ref in zip(refs[:parts], refs[parts : 2 * parts]):
         rows = local_ref.shape[0]
-        at = pl.ds(j * rows, rows)
+        at = pl.ds(begin, rows)
+        begin += rows
         head_out = local_ref[...] + mm(reach_ref[...], sbd, NT)
         centred = head_out - exact_right(head_out, ones_bd, halves) * (1.0 / HEAD_DIM)
         var = exact_right(centred * centred, ones_bd, halves) * (1.0 / HEAD_DIM)
@@ -644,11 +658,11 @@
         receptance, key_matrix, value_matrix, decay_data_term, correction_rate_data,
         decay_channel_offset, correction_rate_offset, extra_head_log_decay.T,
     )
-    local_a, reach_a, state = mixer_local(0, 2, ep, None, *mixer_args)
+    local_a, reach_a, state = mixer_local(0, ep, None, *mixer_args)
     arrived, state = lax.optimization_barrier((arrived, state))
     rows_in = arrived.reshape(experts * capacity, share)
     far = swap(rows_in, tp // 2)
-    local_b, reach_b, end = mixer_local(1, 2, ep, state, *mixer_args)
+    local_b, reach_b, end = mixer_local(1, ep, state, *mixer_args)
     far, weight_far, local_b = lax.optimization_barrier((far, weight_far, local_b))
     weight_masks, weight_blocks = gathered(mixer_output_weight, weight_far)
     ends = lax.all_to_all(end, "ep", split_axis=0, concat_axis=0, tiled=True)

time: 110 us -> 110 us (level)
  Pallas kernels: 48 us -> 49.8 us
  waiting for transfers between devices: 27.8 us -> 26.4 us
    all_to_all x1, waiting for transfers between devices: 2.7 us -> 0.01 us  [local(): lax.all_to_all(send, 'ep', split_axis=0, concat_axis=0, tiled=True)]
    pallas_call x2, Pallas kernels: 20.6 us -> 22.5 us  [mixer_local(): pl.pallas_call(functools.partial(mixer_kernel, base, part == 0, last), gr...]
    ppermute x12, waiting for transfers between devices: 20.8 us -> 22 us  [swap(): return lax.ppermute(x, 'tp', [(i, i ^ mask) for i in range(count)])]
  transfers between devices with their start and end apart: 21 -> 21, of which waited for: 6 -> 6; matrix products, arithmetic and copies ran while one was open for 0% -> 0% of each run, Pallas kernels for 40% -> 41%
where the time goes in v3:
time: 110 us; the launch traced here: 109 us
  Pallas kernels  49.8 us (45%)
  starting transfers between devices  31.3 us (28%)
  waiting for transfers between devices  26.4 us (24%)
    pallas_call x2, Pallas kernels, mixer_local(): pl.pallas_call(functools.partial(mixer_kernel, base, part == 0, last), gr...  22.5 us
    ppermute x12, waiting for transfers between devices, swap(): return lax.ppermute(x, 'tp', [(i, i ^ mask) for i in range(count)])  22 us
    ppermute x7, starting transfers between devices, hop(): return lax.ppermute(x, 'ep', [(i, i ^ mask) for i in range(count)])  11.2 us
    pallas_call x1, Pallas kernels, run_experts(): pl.pallas_call(functools.partial(experts_kernel, masks=masks, sends=tuple...  10.9 us
    all_to_all x1, starting transfers between devices, local(): lax.all_to_all(send, 'ep', split_axis=0, concat_axis=0, tiled=True)  7.28 us
    ppermute x12, starting transfers between devices, swap(): return lax.ppermute(x, 'tp', [(i, i ^ mask) for i in range(count)])  7.12 us
    all_to_all x1, starting transfers between devices, local(): ends = lax.all_to_all(end, 'ep', split_axis=0, concat_axis=0, tiled=True)  5.65 us
    pallas_call x1, Pallas kernels, project(): pl.pallas_call(project_kernel, grid=(width // tile,), in_specs=[pl.BlockS...  3.98 us
  transfers between devices with their start and end apart: 21, of which 6 were waited for; matrix products, arithmetic and copies ran while one was open for 0% of the time, Pallas kernels for 41%

profile of v3, /device:TPU:0, one launch (start us, length us, event | category | flops | bytes accessed | tf_op | source)
XLA Modules:
  0.0 109.3 jit_solution(8692436651348881564)
XLA Ops:
  0.6 0.0 copy-start
  0.6 2.9 %route.1 = (bf16[8,64,512]{2,1,0:T(8,128)(2,1)}, f32[128,8]{1,0:T(8,128)}) custom-call(s32[1]{0:T(128)} %bitcast.place_ref, bf16[128,2048]{1,0:T(8,128)(2,1)} %x_ref.1, f32[1,2048]{1,0:T(1,128)} %bitcast.24, bf16[4,2048]{1,0:T(4,128)(2,1)} %bitcast.23, bf16[8,2048]{1,0:T(8,128)(2,1)} %bitcast.22, s32[2,128]{1,0:T(2,128)} %bitcast.27), custom_call_target="tpu_custom_call" | custom-call | flops 4000000000 | bytes 1000000 | tf_op jit(solution)/shard_map/route/pallas_call | solution.py:369
  3.5 7.3 %all-to-all-start = ((bf16[8,64,512]{2,1,0:T(8,128)(2,1)}), bf16[8,64,512]{2,1,0:T(8,128)(2,1)S(1)}, u32[]{:S(2)}, u32[]{:S(2)}) async-start(bf16[8,64,512]{2,1,0:T(8,128)(2,1)} %get-tuple-element.28), calls=%async_computation | async-start | bytes 1048576 | tf_op jit(solution)/shard_map/all_to_all | solution.py:655
  10.8 0.0 copy-done
  10.8 1.6 %collective-permute-start.1 = (bf16[256,2048]{1,0:T(8,128)(2,1)S(1)}, bf16[256,2048]{1,0:T(8,128)(2,1)S(1)}, u32[]{:S(2)}, u32[]{:S(2)}) collective-permute-start(bf16[256,2048]{1,0:T(8,128)(2,1)S(1)} %copy-done), channel_id=1, source_target_pairs={{0,2},{1,3},{2,0},{3,1},{4,6},{5,7},{6,4},{7,5},{8,10},{9,11},{10,... | collective-permute-start | bytes 3145736 | tf_op jit(solution)/shard_map/ppermute | solution.py:611
  12.4 13.3 %mixer_local.2 = (f32[320,256]{1,0:T(8,128)}, bf16[320,256]{1,0:T(8,128)(2,1)}, f32[128,256]{1,0:T(8,128)S(1)}) custom-call(bf16[512,256]{1,0:T(8,128)(2,1)} %q_in.3, bf16[512,256]{1,0:T(8,128)(2,1)} %k_in.3, bf16[512,256]{1,0:T(8,128)(2,1)} %v_in.3, bf16[512,256]{1,0:T(8,128)(2,1)} %w_in.3, bf16[512,256]{1,0:T(8,128)(2,1)} %a_in.3, f32[1,256]{1,0:T(1,128)} %bitcast.28, ...), custom_call_target="tpu_custom_call" | custom-call | flops 10000000000 | bytes 2000000 | tf_op jit(solution)/shard_map/mixer_local/pallas_call | solution.py:237
  25.7 0.0 all-to-all-done
  25.7 1.1 %collective-permute-start = (bf16[512,512]{1,0:T(8,128)(2,1)S(1)}, bf16[512,512]{1,0:T(8,128)(2,1)S(1)}, u32[]{:S(2)}, u32[]{:S(2)}) collective-permute-start(bf16[512,512]{1,0:T(8,128)(2,1)S(1)} %bitcast.19), channel_id=1, source_target_pairs={{0,2},{1,3},{2,0},{3,1},{4,6},{5,7},{6,4},{7,5},{8,10},{9,11},{10,... | collective-permute-start | bytes 1572872 | tf_op jit(solution)/shard_map/ppermute | solution.py:611
  26.8 0.0 collective-permute-start.7
  26.8 9.2 %mixer_local.3 = (f32[192,256]{1,0:T(8,128)}, bf16[192,256]{1,0:T(8,128)(2,1)}, bf16[8,128,256]{2,1,0:T(8,128)(2,1)}) custom-call(bf16[512,256]{1,0:T(8,128)(2,1)} %q_in.3, bf16[512,256]{1,0:T(8,128)(2,1)} %k_in.3, bf16[512,256]{1,0:T(8,128)(2,1)} %v_in.3, bf16[512,256]{1,0:T(8,128)(2,1)} %w_in.3, bf16[512,256]{1,0:T(8,128)(2,1)} %a_in.3, ...), custom_call_target="tpu_custom_call" | custom-call | flops 10000000000 | bytes 2000000 | tf_op jit(solution)/shard_map/mixer_local/pallas_call | solution.py:237
  36.0 0.9 collective-permute-done.1.refs_5_
  36.9 9.8 %collective-permute-done.refs_1_ = bf16[512,512]{1,0:T(8,128)(2,1)S(1)} collective-permute-done((bf16[512,512]{1,0:T(8,128)(2,1)S(1)}, bf16[512,512]{1,0:T(8,128)(2,1)S(1)}, u32[]{:S(2)}, u32[]{:S(2)}) %collective-permute-start) | collective-permute-done | bytes 524320 | tf_op jit(solution)/shard_map/ppermute | solution.py:611
  46.7 0.0 collective-permute-start.8
  46.7 0.1 pad_add_fusion.place_ref
  46.8 5.7 %all-to-all-start.1 = ((bf16[8,128,256]{2,1,0:T(8,128)(2,1)}), bf16[8,128,256]{2,1,0:T(8,128)(2,1)}, u32[]{:S(2)}, u32[]{:S(2)}) async-start(bf16[8,128,256]{2,1,0:T(8,128)(2,1)} %get-tuple-element.31), calls=%async_computation.1 | async-start | bytes 1048576 | tf_op jit(solution)/shard_map/all_to_all | solution.py:668
  52.4 0.0 collective-permute-done.7.refs_2_
  52.5 0.0 collective-permute-done.8.refs_3_
  52.5 10.9 %experts.1 = (bf16[512,1024]{1,0:T(8,128)(2,1)S(1)}, bf16[2,512,512]{2,1,0:T(8,128)(2,1)}) custom-call(s32[2]{0:T(128)S(1)} %pad_add_fusion.place_ref, bf16[512,512]{1,0:T(8,128)(2,1)S(1)} %bitcast.21, bf16[512,512]{1,0:T(8,128)(2,1)S(1)} %collective-permute-done.refs_1_, bf16[512,512]{1,0:T(8,128)(2,1)} %collective-permute-done.7.refs_2_, ...), custom_call_target="tpu_custom_call" | custom-call | flops 4294967296 | bytes 8388608 | tf_op jit(solution)/shard_map/experts/pallas_call | solution.py:522
  63.4 0.0 copy-start.1
  63.4 1.0 copy-done.1
  64.4 0.2 collective-permute-start.9
  64.6 0.3 collective-permute-start.5
  64.9 0.2 collective-permute-start.6
  65.1 2.6 %all-to-all-done.1.ends_ref = bf16[8,128,256]{2,1,0:T(8,128)(2,1)} async-done(((bf16[8,128,256]{2,1,0:T(8,128)(2,1)}), bf16[8,128,256]{2,1,0:T(8,128)(2,1)}, u32[]{:S(2)}, u32[]{:S(2)}) %all-to-all-start.1) | async-done | bytes 524320 | tf_op jit(solution)/shard_map/all_to_all | solution.py:668
  67.7 0.0 copy-start.2
  67.7 3.5 %mixer_finish.1 = bf16[4,128,256]{2,1,0:T(8,128)(2,1)S(1)} custom-call(s32[2]{0:T(128)S(1)} %pad_add_fusion.place_ref, bf16[8,128,256]{2,1,0:T(8,128)(2,1)} %all-to-all-done.1.ends_ref, bf16[512,256]{1,0:T(8,128)(2,1)} %gate_ref.1, f32[1,256]{1,0:T(1,128)} %bitcast.32, f32[320,256]{1,0:T(8,128)} %get-tuple-element.32.refs_0_, ...), custom_call_target="tpu_custom_call" | custom-call | flops 4000000000 | bytes 2000000 | tf_op jit(solution)/shard_map/mixer_finish/pallas_call | solution.py:307
  71.3 0.0 copy-done.2
  71.3 2.7 %keep_down.1.keep_ref = bf16[2,512,512]{2,1,0:T(8,128)(2,1)S(1)} custom-call(s32[1]{0:T(128)} %bitcast.place_ref, bf16[512,1024]{1,0:T(8,128)(2,1)S(1)} %copy-done.2, bf16[1,1024,2048]{2,1,0:T(8,128)(2,1)} %w_ref.1), custom_call_target="tpu_custom_call" | custom-call | flops 1073741824 | bytes 2097152 | tf_op jit(solution)/shard_map/keep_down/pallas_call | solution.py:558
  74.0 0.0 copy-start.3
  74.0 0.0 collective-permute-done.9.got_ref
  74.0 1.6 %split.1 = (bf16[1,512,512]{2,1,0:T(8,128)(2,1)S(1)}, bf16[1,256,512]{2,1,0:T(8,128)(2,1)S(1)}, bf16[1,256,512]{2,1,0:T(8,128)(2,1)S(1)}) custom-call(bf16[2,512,512]{2,1,0:T(8,128)(2,1)S(1)} %keep_down.1.keep_ref, bf16[2,512,512]{2,1,0:T(8,128)(2,1)} %collective-permute-done.9.got_ref), custom_call_target="tpu_custom_call" | custom-call | flops 100000000 | bytes 1000000 | tf_op jit(solution)/shard_map/split/pallas_call | solution.py:452
  75.6 1.6 %collective-permute-start.10 = (bf16[1,256,512]{2,1,0:T(8,128)(2,1)S(1)}, bf16[1,256,512]{2,1,0:T(8,128)(2,1)S(1)}, u32[]{:S(2)}, u32[]{:S(2)}) collective-permute-start(bf16[1,256,512]{2,1,0:T(8,128)(2,1)S(1)} %get-tuple-element.44), channel_id=1, source_target_pairs={{0,2},{1,3},{2,0},{3,1},{4,6},{5,7},{6,4},{7,5},{8,10},{9,11},{10,... | collective-permute-start | bytes 786440 | tf_op jit(solution)/shard_map/ppermute | solution.py:611
  77.2 0.5 collective-permute-start.14
  77.7 1.6 %collective-permute-start.2 = (bf16[128,256]{1,0:T(8,128)(2,1)S(1)}, bf16[128,256]{1,0:T(8,128)(2,1)S(1)}, u32[]{:S(2)}, u32[]{:S(2)}) collective-permute-start(bf16[128,256]{1,0:T(8,128)(2,1)S(1)} %get-tuple-element.56), channel_id=1, source_target_pairs={{0,2},{1,3},{2,0},{3,1},{4,6},{5,7},{6,4},{7,5},{8,10},{9,11},{10,... | collective-permute-start | bytes 196616 | tf_op jit(solution)/shard_map/ppermute | solution.py:611
  79.3 0.0 collective-permute-done.5.refs_6_
  79.3 0.0 collective-permute-start.3
  79.3 5.5 %collective-permute-done.10.got_ref = bf16[1,256,512]{2,1,0:T(8,128)(2,1)S(1)} collective-permute-done((bf16[1,256,512]{2,1,0:T(8,128)(2,1)S(1)}, bf16[1,256,512]{2,1,0:T(8,128)(2,1)S(1)}, u32[]{:S(2)}, u32[]{:S(2)}) %collective-permute-start.10) | collective-permute-done | bytes 262176 | tf_op jit(solution)/shard_map/ppermute | solution.py:611
  84.8 0.0 collective-permute-start.4
  84.8 0.1 merge.2
  84.9 5.8 %collective-permute-done.2.refs_1_ = bf16[128,256]{1,0:T(8,128)(2,1)S(1)} collective-permute-done((bf16[128,256]{1,0:T(8,128)(2,1)S(1)}, bf16[128,256]{1,0:T(8,128)(2,1)S(1)}, u32[]{:S(2)}, u32[]{:S(2)}) %collective-permute-start.2) | collective-permute-done | bytes 65568 | tf_op jit(solution)/shard_map/ppermute | solution.py:611
  90.7 1.8 %collective-permute-start.11 = (bf16[64,512]{1,0:T(8,128)(2,1)S(1)}, bf16[64,512]{1,0:T(8,128)(2,1)S(1)}, u32[]{:S(2)}, u32[]{:S(2)}) collective-permute-start(bf16[64,512]{1,0:T(8,128)(2,1)S(1)} %get-tuple-element.46), channel_id=1, source_target_pairs={{0,4},{4,0},{8,12},{12,8},{16,20},{20,16},{24,28},{28,24},{1,5},{5... | collective-permute-start | bytes 196616 | tf_op jit(solution)/shard_map/ppermute | solution.py:616
  92.4 0.0 collective-permute-done.14.got_ref
  92.4 0.1 collective-permute-start.12
  92.5 0.1 merge.3
  92.6 0.0 collective-permute-done.3.refs_2_
  92.6 1.7 %collective-permute-start.13 = (bf16[64,512]{1,0:T(8,128)(2,1)S(1)}, bf16[64,512]{1,0:T(8,128)(2,1)S(1)}, u32[]{:S(2)}, u32[]{:S(2)}) collective-permute-start(bf16[64,512]{1,0:T(8,128)(2,1)S(1)} %get-tuple-element.48), channel_id=1, source_target_pairs={{0,12},{4,8},{8,4},{12,0},{16,28},{20,24},{24,20},{28,16},{1,13},{... | collective-permute-start | bytes 196616 | tf_op jit(solution)/shard_map/ppermute | solution.py:616
  94.3 0.0 collective-permute-done.4.refs_3_
  94.3 1.3 %collective-permute-start.15 = (bf16[64,512]{1,0:T(8,128)(2,1)S(1)}, bf16[64,512]{1,0:T(8,128)(2,1)S(1)}, u32[]{:S(2)}, u32[]{:S(2)}) collective-permute-start(bf16[64,512]{1,0:T(8,128)(2,1)S(1)} %get-tuple-element.50), channel_id=1, source_target_pairs={{0,16},{4,20},{8,24},{12,28},{16,0},{20,4},{24,8},{28,12},{1,17},{... | collective-permute-start | bytes 196616 | tf_op jit(solution)/shard_map/ppermute | solution.py:616
  95.6 0.0 collective-permute-done.6.refs_7_
  95.6 2.8 %collective-permute-start.16 = (bf16[64,512]{1,0:T(8,128)(2,1)S(1)}, bf16[64,512]{1,0:T(8,128)(2,1)S(1)}, u32[]{:S(2)}, u32[]{:S(2)}) collective-permute-start(bf16[64,512]{1,0:T(8,128)(2,1)S(1)} %get-tuple-element.51), channel_id=1, source_target_pairs={{0,20},{4,16},{8,28},{12,24},{16,4},{20,0},{24,12},{28,8},{1,21},{... | collective-permute-start | bytes 196616 | tf_op jit(solution)/shard_map/ppermute | solution.py:616
  98.4 0.0 collective-permute-done.11.refs_1_
  98.4 2.1 %collective-permute-start.17 = (bf16[64,512]{1,0:T(8,128)(2,1)S(1)}, bf16[64,512]{1,0:T(8,128)(2,1)S(1)}, u32[]{:S(2)}, u32[]{:S(2)}) collective-permute-start(bf16[64,512]{1,0:T(8,128)(2,1)S(1)} %get-tuple-element.52), channel_id=1, source_target_pairs={{0,24},{4,28},{8,16},{12,20},{16,8},{20,12},{24,0},{28,4},{1,25},{... | collective-permute-start | bytes 196616 | tf_op jit(solution)/shard_map/ppermute | solution.py:616
  100.6 0.0 collective-permute-done.12.refs_2_
  100.6 1.4 %collective-permute-start.18 = (bf16[64,512]{1,0:T(8,128)(2,1)S(1)}, bf16[64,512]{1,0:T(8,128)(2,1)S(1)}, u32[]{:S(2)}, u32[]{:S(2)}) collective-permute-start(bf16[64,512]{1,0:T(8,128)(2,1)S(1)} %get-tuple-element.53), channel_id=1, source_target_pairs={{0,28},{4,24},{8,20},{12,16},{16,12},{20,8},{24,4},{28,0},{1,29},{... | collective-permute-start | bytes 196616 | tf_op jit(solution)/shard_map/ppermute | solution.py:616
  102.0 4.0 %project.1 = bf16[128,2048]{1,0:T(8,128)(2,1)} custom-call(bf16[128,256]{1,0:T(8,128)(2,1)S(1)} %get-tuple-element.57.refs_0_, bf16[128,256]{1,0:T(8,128)(2,1)S(1)} %collective-permute-done.2.refs_1_, bf16[128,256]{1,0:T(8,128)(2,1)S(1)} %collective-permute-done.3.refs_2_, bf16[128,256]{1,0:T(8,128)(2,1)S(1)} %collective-permute-done.4.refs_3_, ...), custom_call_target="tpu_custom_call" | custom-call | flops 536870912 | bytes 4194304 | tf_op jit(solution)/shard_map/project/pallas_call | solution.py:593
  106.0 0.0 collective-permute-done.13.refs_3_
  106.0 0.0 collective-permute-done.15.refs_4_
  106.0 0.0 collective-permute-done.16.refs_5_
  106.0 0.0 collective-permute-done.17.refs_6_
  106.0 1.7 %collective-permute-done.18.refs_7_ = bf16[64,512]{1,0:T(8,128)(2,1)S(1)} collective-permute-done((bf16[64,512]{1,0:T(8,128)(2,1)S(1)}, bf16[64,512]{1,0:T(8,128)(2,1)S(1)}, u32[]{:S(2)}, u32[]{:S(2)}) %collective-permute-start.18) | collective-permute-done | bytes 65568 | tf_op jit(solution)/shard_map/ppermute | solution.py:616
  107.6 0.0 copy-done.3
  107.6 1.6 %combine.1 = bf16[128,512]{1,0:T(8,128)(2,1)} custom-call(s32[2]{0:T(128)S(1)} %pad_add_fusion.place_ref, f32[128,8]{1,0:T(8,128)S(1)} %copy-done.3, bf16[64,512]{1,0:T(8,128)(2,1)S(1)} %get-tuple-element.45.refs_0_, bf16[64,512]{1,0:T(8,128)(2,1)S(1)} %collective-permute-done.11.refs_1_, bf16[64,512]{1,0:T(8,128)(2,1)S(1)} %collective-permute-done.12.refs_2_, ...), custom_call_target="tpu_custom_call" | custom-call | flops 1000000000 | bytes 1000000 | tf_op jit(solution)/shard_map/combine/pallas_call | solution.py:403
  (1 shorter events, 0.0 us)
Async XLA Ops:
  0.6 10.2 %copy-start = (bf16[256,2048]{1,0:T(8,128)(2,1)S(1)}, bf16[256,2048]{1,0:T(8,128)(2,1)}, u32[]{:S(2)}) copy-start(bf16[256,2048]{1,0:T(8,128)(2,1)} %refs_4_.2) | copy-start | bytes 3145732
  3.5 22.2 %all-to-all-start = ((bf16[8,64,512]{2,1,0:T(8,128)(2,1)}), bf16[8,64,512]{2,1,0:T(8,128)(2,1)S(1)}, u32[]{:S(2)}, u32[]{:S(2)}) async-start(bf16[8,64,512]{2,1,0:T(8,128)(2,1)} %get-tuple-element.28), calls=%async_computation | async-start | bytes 1048576 | tf_op jit(solution)/shard_map/all_to_all | solution.py:655
  10.8 26.1 %collective-permute-start.1 = (bf16[256,2048]{1,0:T(8,128)(2,1)S(1)}, bf16[256,2048]{1,0:T(8,128)(2,1)S(1)}, u32[]{:S(2)}, u32[]{:S(2)}) collective-permute-start(bf16[256,2048]{1,0:T(8,128)(2,1)S(1)} %copy-done), channel_id=1, source_target_pairs={{0,2},{1,3},{2,0},{3,1},{4,6},{5,7},{6,4},{7,5},{8,10},{9,11},{10,... | collective-permute-start | bytes 3145736 | tf_op jit(solution)/shard_map/ppermute | solution.py:611
  25.7 21.0 %collective-permute-start = (bf16[512,512]{1,0:T(8,128)(2,1)S(1)}, bf16[512,512]{1,0:T(8,128)(2,1)S(1)}, u32[]{:S(2)}, u32[]{:S(2)}) collective-permute-start(bf16[512,512]{1,0:T(8,128)(2,1)S(1)} %bitcast.19), channel_id=1, source_target_pairs={{0,2},{1,3},{2,0},{3,1},{4,6},{5,7},{6,4},{7,5},{8,10},{9,11},{10,... | collective-permute-start | bytes 1572872 | tf_op jit(solution)/shard_map/ppermute | solution.py:611
  26.8 25.7 %collective-permute-start.7 = (bf16[512,512]{1,0:T(8,128)(2,1)S(1)}, bf16[512,512]{1,0:T(8,128)(2,1)}, u32[]{:S(2)}, u32[]{:S(2)}) collective-permute-start(bf16[512,512]{1,0:T(8,128)(2,1)S(1)} %bitcast.20), channel_id=1, source_target_pairs={{0,1},{1,0},{2,3},{3,2},{4,5},{5,4},{6,7},{7,6},{8,9},{9,8},{10,11... | collective-permute-start | bytes 1572872 | tf_op jit(solution)/shard_map/ppermute | solution.py:611
  46.7 5.7 %collective-permute-start.8 = (bf16[512,512]{1,0:T(8,128)(2,1)S(1)}, bf16[512,512]{1,0:T(8,128)(2,1)}, u32[]{:S(2)}, u32[]{:S(2)}) collective-permute-start(bf16[512,512]{1,0:T(8,128)(2,1)S(1)} %collective-permute-done.refs_1_), channel_id=1, source_target_pairs={{0,1},{1,0},{2,3},{3,2},{4,5},{5,4},{6,7},{7,6},{8,9},{9,8},{10,11... | collective-permute-start | bytes 1572872 | tf_op jit(solution)/shard_map/ppermute | solution.py:611
  46.8 20.9 %all-to-all-start.1 = ((bf16[8,128,256]{2,1,0:T(8,128)(2,1)}), bf16[8,128,256]{2,1,0:T(8,128)(2,1)}, u32[]{:S(2)}, u32[]{:S(2)}) async-start(bf16[8,128,256]{2,1,0:T(8,128)(2,1)} %get-tuple-element.31), calls=%async_computation.1 | async-start | bytes 1048576 | tf_op jit(solution)/shard_map/all_to_all | solution.py:668
  63.4 1.0 copy-start.1
  64.4 9.6 %collective-permute-start.9 = (bf16[2,512,512]{2,1,0:T(8,128)(2,1)}, bf16[2,512,512]{2,1,0:T(8,128)(2,1)}, u32[]{:S(2)}, u32[]{:S(2)}) collective-permute-start(bf16[2,512,512]{2,1,0:T(8,128)(2,1)} %get-tuple-element.42), channel_id=1, source_target_pairs={{0,1},{1,0},{2,3},{3,2},{4,5},{5,4},{6,7},{7,6},{8,9},{9,8},{10,11... | collective-permute-start | bytes 3145736 | tf_op jit(solution)/shard_map/ppermute | solution.py:611
  64.6 14.7 %collective-permute-start.5 = (bf16[256,2048]{1,0:T(8,128)(2,1)S(1)}, bf16[256,2048]{1,0:T(8,128)(2,1)S(1)}, u32[]{:S(2)}, u32[]{:S(2)}) collective-permute-start(bf16[256,2048]{1,0:T(8,128)(2,1)S(1)} %copy-done), channel_id=1, source_target_pairs={{0,1},{1,0},{2,3},{3,2},{4,5},{5,4},{6,7},{7,6},{8,9},{9,8},{10,11... | collective-permute-start | bytes 3145736 | tf_op jit(solution)/shard_map/ppermute | solution.py:611
  64.9 30.8 %collective-permute-start.6 = (bf16[256,2048]{1,0:T(8,128)(2,1)S(1)}, bf16[256,2048]{1,0:T(8,128)(2,1)}, u32[]{:S(2)}, u32[]{:S(2)}) collective-permute-start(bf16[256,2048]{1,0:T(8,128)(2,1)S(1)} %collective-permute-done.1.refs_5_), channel_id=1, source_target_pairs={{0,1},{1,0},{2,3},{3,2},{4,5},{5,4},{6,7},{7,6},{8,9},{9,8},{10,11... | collective-permute-start | bytes 3145736 | tf_op jit(solution)/shard_map/ppermute | solution.py:611
  67.7 3.6 %copy-start.2 = (bf16[512,1024]{1,0:T(8,128)(2,1)S(1)}, bf16[512,1024]{1,0:T(8,128)(2,1)}, u32[]{:S(2)}) copy-start(bf16[512,1024]{1,0:T(8,128)(2,1)} %copy-done.1) | copy-start | bytes 3145732
  74.0 33.7 %copy-start.3 = (f32[128,8]{1,0:T(8,128)S(1)}, f32[128,8]{1,0:T(8,128)}, u32[]{:S(2)}) copy-start(f32[128,8]{1,0:T(8,128)} %get-tuple-element.39.info_ref) | copy-start | bytes 12292
  75.6 9.2 %collective-permute-start.10 = (bf16[1,256,512]{2,1,0:T(8,128)(2,1)S(1)}, bf16[1,256,512]{2,1,0:T(8,128)(2,1)S(1)}, u32[]{:S(2)}, u32[]{:S(2)}) collective-permute-start(bf16[1,256,512]{2,1,0:T(8,128)(2,1)S(1)} %get-tuple-element.44), channel_id=1, source_target_pairs={{0,2},{1,3},{2,0},{3,1},{4,6},{5,7},{6,4},{7,5},{8,10},{9,11},{10,... | collective-permute-start | bytes 786440 | tf_op jit(solution)/shard_map/ppermute | solution.py:611
  77.2 15.3 %collective-permute-start.14 = (bf16[1,256,512]{2,1,0:T(8,128)(2,1)S(1)}, bf16[1,256,512]{2,1,0:T(8,128)(2,1)S(1)}, u32[]{:S(2)}, u32[]{:S(2)}) collective-permute-start(bf16[1,256,512]{2,1,0:T(8,128)(2,1)S(1)} %get-tuple-element.49), channel_id=1, source_target_pairs={{0,2},{1,3},{2,0},{3,1},{4,6},{5,7},{6,4},{7,5},{8,10},{9,11},{10,... | collective-permute-start | bytes 786440 | tf_op jit(solution)/shard_map/ppermute | solution.py:611
  77.7 13.0 %collective-permute-start.2 = (bf16[128,256]{1,0:T(8,128)(2,1)S(1)}, bf16[128,256]{1,0:T(8,128)(2,1)S(1)}, u32[]{:S(2)}, u32[]{:S(2)}) collective-permute-start(bf16[128,256]{1,0:T(8,128)(2,1)S(1)} %get-tuple-element.56), channel_id=1, source_target_pairs={{0,2},{1,3},{2,0},{3,1},{4,6},{5,7},{6,4},{7,5},{8,10},{9,11},{10,... | collective-permute-start | bytes 196616 | tf_op jit(solution)/shard_map/ppermute | solution.py:611
  79.3 13.3 %collective-permute-start.3 = (bf16[128,256]{1,0:T(8,128)(2,1)S(1)}, bf16[128,256]{1,0:T(8,128)(2,1)S(1)}, u32[]{:S(2)}, u32[]{:S(2)}) collective-permute-start(bf16[128,256]{1,0:T(8,128)(2,1)S(1)} %get-tuple-element.55), channel_id=1, source_target_pairs={{0,1},{1,0},{2,3},{3,2},{4,5},{5,4},{6,7},{7,6},{8,9},{9,8},{10,11... | collective-permute-start | bytes 196616 | tf_op jit(solution)/shard_map/ppermute | solution.py:611
  84.8 9.5 %collective-permute-start.4 = (bf16[128,256]{1,0:T(8,128)(2,1)S(1)}, bf16[128,256]{1,0:T(8,128)(2,1)S(1)}, u32[]{:S(2)}, u32[]{:S(2)}) collective-permute-start(bf16[128,256]{1,0:T(8,128)(2,1)S(1)} %get-tuple-element.54), channel_id=1, source_target_pairs={{0,3},{1,2},{2,1},{3,0},{4,7},{5,6},{6,5},{7,4},{8,11},{9,10},{10,... | collective-permute-start | bytes 196616 | tf_op jit(solution)/shard_map/ppermute | solution.py:611
  90.7 7.8 %collective-permute-start.11 = (bf16[64,512]{1,0:T(8,128)(2,1)S(1)}, bf16[64,512]{1,0:T(8,128)(2,1)S(1)}, u32[]{:S(2)}, u32[]{:S(2)}) collective-permute-start(bf16[64,512]{1,0:T(8,128)(2,1)S(1)} %get-tuple-element.46), channel_id=1, source_target_pairs={{0,4},{4,0},{8,12},{12,8},{16,20},{20,16},{24,28},{28,24},{1,5},{5... | collective-permute-start | bytes 196616 | tf_op jit(solution)/shard_map/ppermute | solution.py:616
  92.4 8.1 %collective-permute-start.12 = (bf16[64,512]{1,0:T(8,128)(2,1)S(1)}, bf16[64,512]{1,0:T(8,128)(2,1)S(1)}, u32[]{:S(2)}, u32[]{:S(2)}) collective-permute-start(bf16[64,512]{1,0:T(8,128)(2,1)S(1)} %get-tuple-element.47), channel_id=1, source_target_pairs={{0,8},{4,12},{8,0},{12,4},{16,24},{20,28},{24,16},{28,20},{1,9},{5... | collective-permute-start | bytes 196616 | tf_op jit(solution)/shard_map/ppermute | solution.py:616
  92.6 13.4 %collective-permute-start.13 = (bf16[64,512]{1,0:T(8,128)(2,1)S(1)}, bf16[64,512]{1,0:T(8,128)(2,1)S(1)}, u32[]{:S(2)}, u32[]{:S(2)}) collective-permute-start(bf16[64,512]{1,0:T(8,128)(2,1)S(1)} %get-tuple-element.48), channel_id=1, source_target_pairs={{0,12},{4,8},{8,4},{12,0},{16,28},{20,24},{24,20},{28,16},{1,13},{... | collective-permute-start | bytes 196616 | tf_op jit(solution)/shard_map/ppermute | solution.py:616
  94.3 11.6 %collective-permute-start.15 = (bf16[64,512]{1,0:T(8,128)(2,1)S(1)}, bf16[64,512]{1,0:T(8,128)(2,1)S(1)}, u32[]{:S(2)}, u32[]{:S(2)}) collective-permute-start(bf16[64,512]{1,0:T(8,128)(2,1)S(1)} %get-tuple-element.50), channel_id=1, source_target_pairs={{0,16},{4,20},{8,24},{12,28},{16,0},{20,4},{24,8},{28,12},{1,17},{... | collective-permute-start | bytes 196616 | tf_op jit(solution)/shard_map/ppermute | solution.py:616
  95.6 10.3 %collective-permute-start.16 = (bf16[64,512]{1,0:T(8,128)(2,1)S(1)}, bf16[64,512]{1,0:T(8,128)(2,1)S(1)}, u32[]{:S(2)}, u32[]{:S(2)}) collective-permute-start(bf16[64,512]{1,0:T(8,128)(2,1)S(1)} %get-tuple-element.51), channel_id=1, source_target_pairs={{0,20},{4,16},{8,28},{12,24},{16,4},{20,0},{24,12},{28,8},{1,21},{... | collective-permute-start | bytes 196616 | tf_op jit(solution)/shard_map/ppermute | solution.py:616
  98.4 7.5 %collective-permute-start.17 = (bf16[64,512]{1,0:T(8,128)(2,1)S(1)}, bf16[64,512]{1,0:T(8,128)(2,1)S(1)}, u32[]{:S(2)}, u32[]{:S(2)}) collective-permute-start(bf16[64,512]{1,0:T(8,128)(2,1)S(1)} %get-tuple-element.52), channel_id=1, source_target_pairs={{0,24},{4,28},{8,16},{12,20},{16,8},{20,12},{24,0},{28,4},{1,25},{... | collective-permute-start | bytes 196616 | tf_op jit(solution)/shard_map/ppermute | solution.py:616
  100.6 7.1 %collective-permute-start.18 = (bf16[64,512]{1,0:T(8,128)(2,1)S(1)}, bf16[64,512]{1,0:T(8,128)(2,1)S(1)}, u32[]{:S(2)}, u32[]{:S(2)}) collective-permute-start(bf16[64,512]{1,0:T(8,128)(2,1)S(1)} %get-tuple-element.53), channel_id=1, source_target_pairs={{0,28},{4,24},{8,20},{12,16},{16,12},{20,8},{24,4},{28,0},{1,29},{... | collective-permute-start | bytes 196616 | tf_op jit(solution)/shard_map/ppermute | solution.py:616
